TPU v7x, 256 devices: a 4x2x16 block of a 4x16x16 slice. The times are simulated.
256 devices in a mesh: grp: 2 (over y), sp: 32 (over z, core), tp: 4 (over x).
Axes of the slice: x: 4, y: 2, z: 16, core: 2. Of those that a mesh axis runs over, the one named last changes fastest.
The devices are a block of a 4x16x16 slice.
Arguments:
- queries: bfloat16 [14336, 1024], P(('grp', 'sp'), 'tp'), parts along dimension 0, may hold values from -6 to 6
- head_key_rows: bfloat16 [14336, 1024], P(('grp', 'sp'), 'tp'), parts along dimension 0, may hold values from -6 to 6
- head_value_rows: bfloat16 [14336, 2048], P(('grp', 'sp'), 'tp'), parts along dimension 0, may hold values from -6 to 6
- input_gate_logit: float32 [16, 14336], P('tp', ('grp', 'sp')), parts along dimension 1, may hold values from -6 to 300
- forget_gate_preact: float32 [16, 14336], P('tp', ('grp', 'sp')), parts along dimension 1, may hold values from 0 to 14
- forget_log_offset: float32 [16, 14336], P('tp', ('grp', 'sp')), parts along dimension 1, may hold values from -0.7 to 0
- per_head_norm_gain: bfloat16 [2048], P('tp'), may hold values from 0.099609375 to 1.8984375
- cell_output_matrix: bfloat16 [2048, 2048], P('tp', 'sp'), may hold values from -0.125 to 0.125
- layer_input_rows: bfloat16 [14336, 2048], P(('grp', 'sp', 'tp')), parts along dimension 0, may hold values from -6 to 6
- expert_norm_gain: bfloat16 [2048], replicated, may hold values from 0.099609375 to 1.8984375
- chosen_expert_index: int32 [14336, 2], P(('grp', 'sp', 'tp')), parts along dimension 0, may hold values from 0 to 31, all different within a row; in each aligned block of 56 rows (0 to 55, 56 to 111, ...) at most 7 rows name the same one
- chosen_expert_weight: float32 [14336, 2], P(('grp', 'sp', 'tp')), parts along dimension 0, may hold values from 0.2 to 1
- expert_gate_matrix: bfloat16 [32, 2048, 3584], P('sp', None, 'tp'), may hold values from -0.125 to 0.125
- expert_up_matrix: bfloat16 [32, 2048, 3584], P('sp', None, 'tp'), may hold values from -0.125 to 0.125
- expert_down_matrix: bfloat16 [32, 3584, 2048], P('sp', 'tp'), may hold values from -0.09375 to 0.09375
Outputs:
- layer_out: bfloat16 [14336, 2048], P(('grp', 'sp', 'tp')), parts along dimension 0
There are 2 independent parts, one for each index of `grp`. A program takes and returns all parts, laid end to end along the dimension named above; an argument that names none is the same for every part. Nothing has to cross between parts.
Inputs may be any that keep to these rules, and one draw needn't show every extreme that they name: `chosen_expert_index`: each row names 2 different experts. In the rows of one device no expert is named more than 7 times, and in every draw some expert is named exactly 7 times in the rows of some device.
All inputs are finite; a program needn't handle non-finite values.
Results may differ from a plain program's by a relative error of at most 0.013.
Values may be sent and summed in bfloat16 or wider, within the bound.
No kernel may reach another device: no remote copies, remote signals or barrier semaphores. Data moves between devices by JAX's collectives and lax.ppermute only.
A program may use at most 64 MiB of HBM per device.

v0:
```python
import jax
import jax.numpy as jnp
from jax import lax
from jax.sharding import Mesh
from jax.sharding import PartitionSpec as P


DK = 64
DV = 128
NEAR = ("near", "core")
SP = ("far", *NEAR)
GRP_SP = ("grp", *SP)
GRP_SP_TP = (*GRP_SP, "tp")

far_below = -1e30
norm_eps = 1e-06
HIGHEST = lax.Precision.HIGHEST


def shifted(x, axis, by):
    size = lax.axis_size(axis)
    return lax.ppermute(x, axis, [(i, (i + by) % size) for i in range(size)])


def traded(x, axis):
    return lax.all_to_all(x, axis, split_axis=0, concat_axis=0, tiled=True)


def strength_of(totals, peaks):
    size = totals.shape[0]
    shape = (size + 1, size, size)
    t, s, u = (lax.broadcasted_iota(jnp.int32, shape, d) for d in range(3))
    decay = jnp.sum(jnp.where((s < u) & (u < t), totals[None, None, :], 0.0), axis=2)
    earlier = s[:, :, 0] < t[:, :, 0]
    logs = jnp.where(earlier, decay + peaks[None, :], far_below)
    tops = jnp.max(logs, axis=1)
    return jnp.where(earlier, jnp.exp(logs - tops[:, None]), 0.0), tops


def with_header(body, *scalars):
    count, _, lanes = body.shape
    lines = [jnp.broadcast_to(x.reshape(count, 1, 1), (count, 1, lanes)) for x in scalars]
    lines.append(jnp.zeros((count, 8 - len(scalars), lanes), jnp.float32))
    return jnp.concatenate([body, *lines], axis=1)


def states_before(memory, totals, peaks):
    heads, dk, dv = memory.shape
    near = lax.axis_size(NEAR)
    far = lax.axis_size("far")
    rows = heads * dk // near
    per_head = near // heads
    sent = with_header(
        memory.reshape(near, rows, dv), jnp.repeat(totals, per_head), jnp.repeat(peaks, per_head)
    )
    got = traded(sent, NEAR)
    parts, total, peak = got[:, :rows], got[:, rows, 0], got[:, rows + 1, 0]
    size = total.shape[0]
    weight, tops = strength_of(total, peak)
    whole = jnp.sum(weight[size][:, None, None] * parts, axis=0)
    whole = with_header(whole[None], jnp.sum(total).reshape(1), tops[size].reshape(1))[0]
    group = lax.axis_index("far")
    before = []
    for back in range(far - 1, 0, -1):
        other = lax.ppermute(whole, "far", [(i, i + back) for i in range(far - back)])
        before.append(jnp.where(group >= back, other, jnp.zeros_like(other)))
    stack = jnp.stack(before)
    known = group >= jnp.arange(far - 1, 0, -1)
    all_total = jnp.concatenate([stack[:, rows, 0], total])
    all_peak = jnp.concatenate([jnp.where(known, stack[:, rows + 1, 0], far_below), peak])
    weight, tops = strength_of(all_total, all_peak)
    weight, tops = weight[far - 1 : -1], tops[far - 1 : -1]
    states = jnp.concatenate([stack[:, :rows], parts], axis=0)
    states = jnp.sum(weight[:, :, None, None] * states[None], axis=1)
    mine = traded(with_header(states, tops), NEAR)
    return mine[:, :rows].reshape(heads, dk, dv), mine[::per_head, rows, 0]


def gathered_columns(matrix):
    own = jnp.transpose(matrix)
    far, near = lax.axis_size("far"), lax.axis_size("near")
    level = jnp.stack([own] + [shifted(own, "far", far - i) for i in range(1, far)])
    chips = far * near
    wide = []
    for k in (-1, 0, 1, 2):
        if k:
            wide.append(shifted(level, ("far", "near"), chips - k))
        else:
            wide.append(level)
    mine = jnp.stack(wide, axis=1).reshape(chips, *own.shape)
    other = shifted(mine, "core", 1)
    core = lax.axis_index("core")
    both = jnp.stack([jnp.where(core == 0, mine, other), jnp.where(core == 0, other, mine)], axis=1)
    both = both.reshape(chips, -1, own.shape[1])
    both = jnp.concatenate([both, both], axis=0)
    at = lax.axis_index(("far", "near"))
    start = jnp.where(at == 0, 1, chips + 1 - at)
    whole = lax.dynamic_slice_in_dim(both, start, chips, axis=0)
    return whole.reshape(-1, own.shape[1])


def expert_part(rows_in, gate_w, up_w, down_w):
    gate = jnp.dot(rows_in, gate_w, preferred_element_type=jnp.float32)
    upward = jnp.dot(rows_in, up_w, preferred_element_type=jnp.float32)
    hidden = (jax.nn.silu(gate) * upward).astype(jnp.bfloat16)
    return jnp.dot(hidden, down_w, preferred_element_type=jnp.float32).astype(jnp.bfloat16)


def shards(
    queries,
    head_key_rows,
    head_value_rows,
    input_gate_logit,
    forget_gate_preact,
    forget_log_offset,
    per_head_norm_gain,
    cell_output_matrix,
    layer_input_rows,
    expert_norm_gain,
    chosen_expert_index,
    chosen_expert_weight,
    expert_gate_matrix,
    expert_up_matrix,
    expert_down_matrix,
):
    count = queries.shape[0]
    heads = input_gate_logit.shape[0]
    queries3 = queries.reshape(count, heads, DK)
    keys3 = head_key_rows.reshape(count, heads, DK)
    values3 = head_value_rows.reshape(count, heads, DV)
    rows_at = lax.broadcasted_iota(jnp.int32, (count, count), 0)
    cols_at = lax.broadcasted_iota(jnp.int32, (count, count), 1)
    causal = cols_at <= rows_at

    log_retention = jax.nn.log_sigmoid(forget_gate_preact) + forget_log_offset
    running = jnp.dot(log_retention, (rows_at <= cols_at).astype(jnp.float32), precision=HIGHEST)
    totals = running[:, -1]
    term_log = totals[:, None] - running + input_gate_logit
    own_peak = jnp.max(term_log, axis=1)
    factors = jnp.transpose(jnp.exp(term_log - own_peak[:, None]))
    weighted = values3.astype(jnp.float32) * factors[:, :, None]
    own_memory = jnp.einsum(
        "shd,she->hde", keys3.astype(jnp.float32), weighted, precision=HIGHEST
    )

    memory_in, peak_in = states_before(own_memory, totals, own_peak)

    decay_log = jnp.where(
        causal[None],
        running[:, :, None] - running[:, None, :] + input_gate_logit[:, None, :],
        far_below,
    )
    carried_log = running + peak_in[:, None]
    peak = jnp.maximum(carried_log, jnp.max(decay_log, axis=2))
    qk_scale = DK ** (-0.5)
    scores = (
        jnp.einsum("thd,shd->hts", queries3, keys3, preferred_element_type=jnp.float32) * qk_scale
    )
    strength = scores * jnp.exp(decay_log - peak[:, :, None])
    carried = jnp.exp(carried_log - peak)
    from_memory = (
        jnp.einsum("thd,hde->the", queries3.astype(jnp.float32), memory_in, precision=HIGHEST)
        * qk_scale
    )
    within = jnp.einsum(
        "hts,she->the", strength.astype(jnp.bfloat16), values3, preferred_element_type=jnp.float32
    )
    result = within + jnp.transpose(carried)[:, :, None] * from_memory
    result = result * lax.rsqrt(jnp.mean(result * result, axis=2, keepdims=True) + norm_eps)
    result = result * per_head_norm_gain.astype(jnp.float32).reshape(heads, -1)
    mixed = result.reshape(count, -1).astype(jnp.bfloat16)

    partial_value = lax.dot_general(
        mixed,
        gathered_columns(cell_output_matrix),
        (((1,), (1,)), ((), ())),
        preferred_element_type=jnp.float32,
    ).astype(jnp.bfloat16)
    rows, width = layer_input_rows.shape
    tiles = traded(partial_value.reshape(lax.axis_size("tp"), rows, width), "tp")
    residual = layer_input_rows.astype(jnp.float32) + jnp.sum(tiles.astype(jnp.float32), axis=0)
    normed = residual * lax.rsqrt(jnp.mean(residual * residual, axis=1, keepdims=True) + norm_eps)
    normed = (normed * expert_norm_gain.astype(jnp.float32)).astype(jnp.bfloat16)

    experts = lax.axis_size(SP)
    slots = (4 * rows + experts - 1) // experts
    expert_at = jnp.arange(experts, dtype=jnp.int32)[None, :]
    named = [
        (chosen_expert_index[:, k : k + 1] == expert_at).astype(jnp.bfloat16) for k in range(2)
    ]
    below = (
        lax.broadcasted_iota(jnp.int32, (rows, rows), 1)
        < lax.broadcasted_iota(jnp.int32, (rows, rows), 0)
    ).astype(jnp.bfloat16)
    ahead = [jnp.dot(below, n, preferred_element_type=jnp.float32) for n in named]
    first = jnp.sum(named[0].astype(jnp.float32), axis=0, keepdims=True)
    ahead[1] = ahead[1] + first
    picks = []
    for k in range(2):
        place = jnp.sum(named[k].astype(jnp.float32) * ahead[k], axis=1, keepdims=True)
        slot = chosen_expert_index[:, k : k + 1] * slots + place.astype(jnp.int32)
        target = lax.broadcasted_iota(jnp.int32, (rows, experts * slots), 1)
        picks.append((slot == target).astype(jnp.bfloat16))
    outgoing = lax.dot_general(
        picks[0] + picks[1],
        normed,
        (((0,), (0,)), ((), ())),
        preferred_element_type=jnp.float32,
    ).astype(jnp.bfloat16)

    arrived = traded(outgoing.reshape(experts, slots, width), SP)
    arrived = jnp.transpose(arrived, (1, 0, 2)).reshape(slots * experts, width)
    weights = (expert_gate_matrix[0], expert_up_matrix[0], expert_down_matrix[0])
    size = lax.axis_size("tp")
    half = arrived.shape[0] // 2
    left = shifted(arrived, "tp", 1)
    right = shifted(arrived, "tp", size - 1)
    own = expert_part(arrived, *weights)
    across = [shifted(left[:half], "tp", 1), shifted(right[half:], "tp", size - 1)]
    left, right, _ = lax.optimization_barrier((left, right, own))
    from_left = expert_part(left, *weights)
    parts = [own, shifted(from_left, "tp", size - 1)]
    right, _ = lax.optimization_barrier((right, from_left))
    from_right = expert_part(right, *weights)
    parts.append(shifted(from_right, "tp", 1))
    across, _ = lax.optimization_barrier((jnp.concatenate(across, axis=0), from_right))
    from_across = expert_part(across, *weights)
    parts.append(shifted(from_across, "tp", 2))
    total_out = sum(part.astype(jnp.float32) for part in parts)
    expert_out = total_out.astype(jnp.bfloat16).reshape(slots, experts, width)
    back = traded(jnp.transpose(expert_out, (1, 0, 2)), SP)
    flat_out = back.reshape(experts * slots, width)

    out = residual
    for k in range(2):
        picked = jnp.dot(picks[k], flat_out, preferred_element_type=jnp.float32)
        out = out + chosen_expert_weight[:, k : k + 1] * picked
    return out.astype(jnp.bfloat16)


def solution(mesh):
    sp = mesh.shape["sp"]
    torus = Mesh(
        mesh.devices.reshape(mesh.shape["grp"], sp // 8, 4, 2, mesh.shape["tp"]), GRP_SP_TP
    )
    return jax.shard_map(
        shards,
        mesh=torus,
        in_specs=(
            P(GRP_SP, "tp"),
            P(GRP_SP, "tp"),
            P(GRP_SP, "tp"),
            P("tp", GRP_SP),
            P("tp", GRP_SP),
            P("tp", GRP_SP),
            P("tp"),
            P("tp", SP),
            P(GRP_SP_TP, None),
            P(),
            P(GRP_SP_TP, None),
            P(GRP_SP_TP, None),
            P(SP, None, "tp"),
            P(SP, None, "tp"),
            P(SP, "tp", None),
        ),
        out_specs=P(GRP_SP_TP, None),
        check_vma=False,
    )
```

profile of v0, /device:TPU:40, one launch (start us, length us, event | category | flops | bytes accessed | tf_op | source)
XLA Modules:
  0.0 347.9 jit_solution(11321041395464253838)
XLA Ops:
  0.0 0.9 fusion.102
  1.1 0.9 fusion.148
  2.0 0.8 exponential_bitcast_fusion
  2.8 1.0 copy.78
  4.2 0.5 fusion.77
  4.8 0.8 maximum_maximum_fusion
  5.6 8.5 %all-to-all-start = ((f32[8,40,128]{2,1,0:T(8,128)}), f32[8,40,128]{2,1,0:T(8,128)S(1)}, u32[]{:S(2)}, u32[]{:S(2)}) async-start(f32[8,40,128]{2,1,0:T(8,128)} %maximum_maximum_fusion), calls=%async_computation | async-start | bytes 327680 | tf_op jit(solution)/shard_map/all_to_all | solution.py:26
  14.1 18.4 %collective-permute-start.3 = (bf16[64,512]{1,0:T(8,128)(2,1)}, bf16[64,512]{1,0:T(8,128)(2,1)S(1)}, u32[]{:S(2)}, u32[]{:S(2)}) collective-permute-start(bf16[64,512]{1,0:T(8,128)(2,1)} %bitcast.214), channel_id=1, source_target_pairs={{0,96},{32,0},{64,32},{96,64},{1,97},{33,1},{65,33},{97,65},{2,98}... | collective-permute-start | bytes 196616 | tf_op jit(solution)/shard_map/ppermute | solution.py:22
  32.5 5.5 %collective-permute-start.5 = (bf16[64,512]{1,0:T(8,128)(2,1)}, bf16[64,512]{1,0:T(8,128)(2,1)S(1)}, u32[]{:S(2)}, u32[]{:S(2)}) collective-permute-start(bf16[64,512]{1,0:T(8,128)(2,1)} %bitcast.216), channel_id=1, source_target_pairs={{0,32},{32,64},{64,96},{96,0},{1,33},{33,65},{65,97},{97,1},{2,34}... | collective-permute-start | bytes 196616 | tf_op jit(solution)/shard_map/ppermute | solution.py:22
  38.1 0.7 slice_bitcast_fusion.3
  38.8 0.6 slice_reduce_fusion.2
  39.7 0.6 slice.88
  40.5 0.7 pad.28.clone
  41.2 0.7 pad.27.clone
  42.1 7.7 %collective-permute-start.2 = (f32[40,128]{1,0:T(8,128)S(1)}, f32[40,128]{1,0:T(8,128)S(1)}, u32[]{:S(2)}, u32[]{:S(2)}) collective-permute-start(f32[40,128]{1,0:T(8,128)S(1)} %maximum_bitcast_fusion), channel_id=1, source_target_pairs={{0,32},{32,64},{64,96},{1,33},{33,65},{65,97},{2,34},{34,66},{66,9... | collective-permute-start | bytes 61448 | tf_op jit(solution)/shard_map/ppermute | solution.py:65
  50.0 5.3 %collective-permute-start.1 = (f32[40,128]{1,0:T(8,128)S(1)}, f32[40,128]{1,0:T(8,128)S(1)}, u32[]{:S(2)}, u32[]{:S(2)}) collective-permute-start(f32[40,128]{1,0:T(8,128)S(1)} %maximum_bitcast_fusion), channel_id=1, source_target_pairs={{0,64},{32,96},{1,65},{33,97},{2,66},{34,98},{3,67},{35,99},{4,68}... | collective-permute-start | bytes 61448 | tf_op jit(solution)/shard_map/ppermute | solution.py:65
  55.3 3.6 %collective-permute-start = (f32[40,128]{1,0:T(8,128)S(1)}, f32[40,128]{1,0:T(8,128)S(1)}, u32[]{:S(2)}, u32[]{:S(2)}) collective-permute-start(f32[40,128]{1,0:T(8,128)S(1)} %maximum_bitcast_fusion), channel_id=1, source_target_pairs={{0,96},{1,97},{2,98},{3,99},{4,100},{5,101},{6,102},{7,103},{8,104... | collective-permute-start | bytes 61448 | tf_op jit(solution)/shard_map/ppermute | solution.py:65
  59.0 1.4 collective-permute-done
  61.3 0.8 maximum_maximum_fusion.1
  62.1 5.4 %all-to-all-start.1 = ((f32[8,40,128]{2,1,0:T(8,128)}), f32[8,40,128]{2,1,0:T(8,128)S(1)}, u32[]{:S(2)}, u32[]{:S(2)}) async-start(f32[8,40,128]{2,1,0:T(8,128)} %maximum_maximum_fusion.1), calls=%async_computation.1 | async-start | bytes 327680 | tf_op jit(solution)/shard_map/all_to_all | solution.py:26
  67.5 0.9 fusion.149
  68.4 2.1 collective-permute-start.6
  70.5 4.9 %collective-permute-start.7 = (bf16[4,64,512]{2,1,0:T(8,128)(2,1)S(1)}, bf16[4,64,512]{2,1,0:T(8,128)(2,1)S(1)}, u32[]{:S(2)}, u32[]{:S(2)}) collective-permute-start(bf16[4,64,512]{2,1,0:T(8,128)(2,1)S(1)} %get-tuple-element.23), channel_id=1, source_target_pairs={{0,120},{8,0},{16,8},{24,16},{32,24},{40,32},{48,40},{56,48},{64,5... | collective-permute-start | bytes 786440 | tf_op jit(solution)/shard_map/ppermute | solution.py:22
  75.4 1.9 collective-permute-start.8
  77.3 0.4 fusion.69
  77.8 4.0 %collective-permute-done.6 = bf16[4,64,512]{2,1,0:T(8,128)(2,1)S(1)} collective-permute-done((bf16[4,64,512]{2,1,0:T(8,128)(2,1)S(1)}, bf16[4,64,512]{2,1,0:T(8,128)(2,1)S(1)}, u32[]{:S(2)}, u32[]{:S(2)}) %collective-permute-start.6) | collective-permute-done | bytes 262176 | tf_op jit(solution)/shard_map/ppermute | solution.py:22
  81.9 5.7 %collective-permute-done.7 = bf16[4,64,512]{2,1,0:T(8,128)(2,1)S(1)} collective-permute-done((bf16[4,64,512]{2,1,0:T(8,128)(2,1)S(1)}, bf16[4,64,512]{2,1,0:T(8,128)(2,1)S(1)}, u32[]{:S(2)}, u32[]{:S(2)}) %collective-permute-start.7) | collective-permute-done | bytes 262176 | tf_op jit(solution)/shard_map/ppermute | solution.py:22
  87.6 4.9 %collective-permute-done.8 = bf16[4,64,512]{2,1,0:T(8,128)(2,1)S(1)} collective-permute-done((bf16[4,64,512]{2,1,0:T(8,128)(2,1)S(1)}, bf16[4,64,512]{2,1,0:T(8,128)(2,1)S(1)}, u32[]{:S(2)}, u32[]{:S(2)}) %collective-permute-start.8) | collective-permute-done | bytes 262176 | tf_op jit(solution)/shard_map/ppermute | solution.py:22
  93.1 0.4 fusion.62
  93.5 1.6 multiply_reduce_fusion.2
  96.0 0.8 fusion.39
  96.8 1.8 convolution_convert_fusion
  98.6 4.6 %all-to-all-start.2 = ((bf16[4,56,2048]{2,1,0:T(8,128)(2,1)}), bf16[4,56,2048]{2,1,0:T(8,128)(2,1)S(1)}, u32[]{:S(2)}, u32[]{:S(2)}) async-start(bf16[4,56,2048]{2,1,0:T(8,128)(2,1)} %bitcast.36), calls=%async_computation.2 | async-start | bytes 1835008 | tf_op jit(solution)/shard_map/all_to_all | solution.py:26
  103.6 13.6 %all-to-all-done.2 = bf16[4,56,2048]{2,1,0:T(8,128)(2,1)S(1)} async-done(((bf16[4,56,2048]{2,1,0:T(8,128)(2,1)}), bf16[4,56,2048]{2,1,0:T(8,128)(2,1)S(1)}, u32[]{:S(2)}, u32[]{:S(2)}) %all-to-all-start.2) | async-done | bytes 917536 | tf_op jit(solution)/shard_map/all_to_all | solution.py:26
  117.6 0.5 convolution_convert_fusion.1
  118.4 64.4 %all_to_all.25 = bf16[32,7,2048]{2,1,0:T(8,128)(2,1)S(1)} all-to-all(bf16[32,7,2048]{2,1,0:T(8,128)(2,1)S(1)} %reshape.129), channel_id=1, replica_groups=mesh['grp'=2,'far'=4,'near'=4,'core'=2,'tp'=4] {'far','near','core'}, dimensions={0} | all-to-all | bytes 1835008 | tf_op jit(solution)/shard_map/all_to_all | solution.py:26
  182.8 0.6 copy.89
  183.4 0.7 collective-permute-start.10
  184.1 2.7 collective-permute-start.11
  186.8 2.0 fusion.22
  188.8 5.5 %fusion.24 = bf16[224,2048]{1,0:T(8,128)(2,1)S(1)} fusion(bf16[1,896,2048]{2,1,0:T(8,128)(2,1)} %param.29, bf16[224,2048]{1,0:T(8,128)(2,1)S(1)} %bitcast.204, bf16[1,2048,896]{2,1,0:T(8,128)(2,1)} %param.28, f32[224,896]{1,0:T(8,128)} %fusion.22), kind=kOutput, calls=%fused_computation.28 | convolution fusion | flops 1645830144 | bytes 9977856 | tf_op jit(solution)/shard_map/dot_general | solution.py:106
  194.3 12.8 %collective-permute-done.10 = bf16[224,2048]{1,0:T(8,128)(2,1)} collective-permute-done((bf16[224,2048]{1,0:T(8,128)(2,1)S(1)}, bf16[224,2048]{1,0:T(8,128)(2,1)}, u32[]{:S(2)}, u32[]{:S(2)}) %collective-permute-start.10) | collective-permute-done | bytes 917536 | tf_op jit(solution)/shard_map/ppermute | solution.py:22
  207.1 3.4 fusion.12
  210.5 6.5 %fusion.27 = bf16[224,2048]{1,0:T(8,128)(2,1)} fusion(bf16[1,896,2048]{2,1,0:T(8,128)(2,1)} %param.29, f32[224,896]{1,0:T(8,128)S(1)} %fusion.12, bf16[224,2048]{1,0:T(8,128)(2,1)} %collective-permute-done.10, bf16[1,2048,896]{2,1,0:T(8,128)(2,1)} %param.27), kind=kOutput, calls=%fused_computation.29 | convolution fusion | flops 1645830144 | bytes 9977856 | tf_op jit(solution)/shard_map/dot_general | solution.py:106
  217.0 3.0 collective-permute-start.12
  220.0 4.3 %fusion.18 = f32[224,896]{1,0:T(8,128)} fusion(bf16[224,2048]{1,0:T(8,128)(2,1)} %collective-permute-done.11, bf16[1,2048,896]{2,1,0:T(8,128)(2,1)} %param.27), kind=kOutput, calls=%fused_computation.20 | convolution fusion | flops 822083584 | bytes 5390336 | tf_op jit(solution)/shard_map/dot_general | solution.py:103
  224.3 1.0 slice.110
  225.5 1.1 slice.111
  226.6 3.5 %collective-permute-start.15 = (bf16[112,2048]{1,0:T(8,128)(2,1)S(1)}, bf16[112,2048]{1,0:T(8,128)(2,1)}, u32[]{:S(2)}, u32[]{:S(2)}) collective-permute-start(bf16[112,2048]{1,0:T(8,128)(2,1)S(1)} %slice.111), channel_id=1, source_target_pairs={{0,3},{1,0},{2,1},{3,2},{4,7},{5,4},{6,5},{7,6},{8,11},{9,8},{10,9... | collective-permute-start | bytes 1376264 | tf_op jit(solution)/shard_map/ppermute | solution.py:22
  230.1 6.7 %fusion.30 = bf16[224,2048]{1,0:T(8,128)(2,1)} fusion(bf16[1,896,2048]{2,1,0:T(8,128)(2,1)} %param.29, bf16[224,2048]{1,0:T(8,128)(2,1)} %collective-permute-done.11, bf16[1,2048,896]{2,1,0:T(8,128)(2,1)} %param.28, f32[224,896]{1,0:T(8,128)} %fusion.18), kind=kOutput, calls=%fused_computation.30 | convolution fusion | flops 1645830144 | bytes 9977856 | tf_op jit(solution)/shard_map/dot_general | solution.py:106
  236.8 0.9 collective-permute-done.14
  237.7 10.9 %collective-permute-done.15 = bf16[112,2048]{1,0:T(8,128)(2,1)} collective-permute-done((bf16[112,2048]{1,0:T(8,128)(2,1)S(1)}, bf16[112,2048]{1,0:T(8,128)(2,1)}, u32[]{:S(2)}, u32[]{:S(2)}) %collective-permute-start.15) | collective-permute-done | bytes 458784 | tf_op jit(solution)/shard_map/ppermute | solution.py:22
  248.7 1.1 pad_maximum_fusion.2
  249.7 4.0 %fusion.16 = f32[224,896]{1,0:T(8,128)} fusion(bf16[224,2048]{1,0:T(8,128)(2,1)S(1)} %pad_maximum_fusion.2, bf16[1,2048,896]{2,1,0:T(8,128)(2,1)} %param.27), kind=kOutput, calls=%fused_computation.18 | convolution fusion | flops 822083584 | bytes 5390336 | tf_op jit(solution)/shard_map/dot_general | solution.py:103
  253.8 6.4 %fusion.33 = bf16[224,2048]{1,0:T(8,128)(2,1)} fusion(bf16[1,896,2048]{2,1,0:T(8,128)(2,1)} %param.29, bf16[224,2048]{1,0:T(8,128)(2,1)S(1)} %pad_maximum_fusion.2, bf16[1,2048,896]{2,1,0:T(8,128)(2,1)} %param.28, f32[224,896]{1,0:T(8,128)} %fusion.16), kind=kOutput, calls=%fused_computation.31 | convolution fusion | flops 1645830144 | bytes 9977856 | tf_op jit(solution)/shard_map/dot_general | solution.py:106
  260.2 2.3 collective-permute-start.16
  262.5 19.8 %collective-permute-done.16 = bf16[224,2048]{1,0:T(8,128)(2,1)S(1)} collective-permute-done((bf16[224,2048]{1,0:T(8,128)(2,1)}, bf16[224,2048]{1,0:T(8,128)(2,1)S(1)}, u32[]{:S(2)}, u32[]{:S(2)}) %collective-permute-start.16) | collective-permute-done | bytes 917536 | tf_op jit(solution)/shard_map/ppermute | solution.py:22
  282.4 2.0 add_convert_fusion
  284.4 1.5 copy.108
  285.9 5.0 %all-to-all-start.4 = ((bf16[32,7,2048]{2,1,0:T(8,128)(2,1)}), bf16[32,7,2048]{2,1,0:T(8,128)(2,1)S(1)}, u32[]{:S(2)}, u32[]{:S(2)}) async-start(bf16[32,7,2048]{2,1,0:T(8,128)(2,1)} %bitcast.198), calls=%async_computation.4 | async-start | bytes 2097152 | tf_op jit(solution)/shard_map/all_to_all | solution.py:26
  291.0 55.3 %all-to-all-done.4 = bf16[32,7,2048]{2,1,0:T(8,128)(2,1)S(1)} async-done(((bf16[32,7,2048]{2,1,0:T(8,128)(2,1)}), bf16[32,7,2048]{2,1,0:T(8,128)(2,1)S(1)}, u32[]{:S(2)}, u32[]{:S(2)}) %all-to-all-start.4) | async-done | bytes 917536 | tf_op jit(solution)/shard_map/all_to_all | solution.py:26
  346.3 0.3 reshape.132
  346.6 0.3 convolution_multiply_fusion
  346.9 1.0 fusion.38
  (93 shorter events, 5.2 us)
Async XLA Ops:
  0.0 4.2 %copy-start = (bf16[224,512]{1,0:T(8,128)(2,1)S(1)}, bf16[224,512]{1,0:T(8,128)(2,1)}, u32[]{:S(2)}) copy-start(bf16[224,512]{1,0:T(8,128)(2,1)} %param.17) | copy-start | bytes 688132
  0.0 77.3 %copy-start.5 = (f32[4,224]{1,0:T(4,128)S(1)}, f32[4,224]{1,0:T(4,128)}, u32[]{:S(2)}) copy-start(f32[4,224]{1,0:T(4,128)} %param.18) | copy-start | bytes 10756
  0.0 77.7 %copy-start.4 = (bf16[224,256]{1,0:T(8,128)(2,1)S(1)}, bf16[224,256]{1,0:T(8,128)(2,1)}, u32[]{:S(2)}) copy-start(bf16[224,256]{1,0:T(8,128)(2,1)} %param.15) | copy-start | bytes 344068
  0.0 77.8 %copy-start.7 = (bf16[512]{0:T(512)(128)(2,1)S(1)}, bf16[512]{0:T(512)(128)(2,1)}, u32[]{:S(2)}) copy-start(bf16[512]{0:T(512)(128)(2,1)} %param.21) | copy-start | bytes 3076
  3.8 37.4 %copy-start.3 = (bf16[224,256]{0,1:T(8,128)(2,1)}, bf16[224,256]{0,1:T(8,128)(2,1)S(1)}, u32[]{:S(2)}) copy-start(bf16[224,256]{0,1:T(8,128)(2,1)S(1)} %copy.78) | copy-start | bytes 344068
  5.6 33.2 %all-to-all-start = ((f32[8,40,128]{2,1,0:T(8,128)}), f32[8,40,128]{2,1,0:T(8,128)S(1)}, u32[]{:S(2)}, u32[]{:S(2)}) async-start(f32[8,40,128]{2,1,0:T(8,128)} %maximum_maximum_fusion), calls=%async_computation | async-start | bytes 327680 | tf_op jit(solution)/shard_map/all_to_all | solution.py:26
  14.1 53.4 %collective-permute-start.3 = (bf16[64,512]{1,0:T(8,128)(2,1)}, bf16[64,512]{1,0:T(8,128)(2,1)S(1)}, u32[]{:S(2)}, u32[]{:S(2)}) collective-permute-start(bf16[64,512]{1,0:T(8,128)(2,1)} %bitcast.214), channel_id=1, source_target_pairs={{0,96},{32,0},{64,32},{96,64},{1,97},{33,1},{65,33},{97,65},{2,98}... | collective-permute-start | bytes 196616 | tf_op jit(solution)/shard_map/ppermute | solution.py:22
  32.5 35.0 %collective-permute-start.4 = (bf16[64,512]{1,0:T(8,128)(2,1)}, bf16[64,512]{1,0:T(8,128)(2,1)S(1)}, u32[]{:S(2)}, u32[]{:S(2)}) collective-permute-start(bf16[64,512]{1,0:T(8,128)(2,1)} %bitcast.215), channel_id=1, source_target_pairs={{0,64},{32,96},{64,0},{96,32},{1,65},{33,97},{65,1},{97,33},{2,66}... | collective-permute-start | bytes 196616 | tf_op jit(solution)/shard_map/ppermute | solution.py:22
  32.5 35.0 %collective-permute-start.5 = (bf16[64,512]{1,0:T(8,128)(2,1)}, bf16[64,512]{1,0:T(8,128)(2,1)S(1)}, u32[]{:S(2)}, u32[]{:S(2)}) collective-permute-start(bf16[64,512]{1,0:T(8,128)(2,1)} %bitcast.216), channel_id=1, source_target_pairs={{0,32},{32,64},{64,96},{96,0},{1,33},{33,65},{65,97},{97,1},{2,34}... | collective-permute-start | bytes 196616 | tf_op jit(solution)/shard_map/ppermute | solution.py:22
  38.1 54.4 %copy-start.2 = (pred[224,224]{1,0:T(8,128)(4,1)}, pred[224,224]{1,0:T(8,128)(4,1)S(1)}, u32[]{:S(2)}) copy-start(pred[224,224]{1,0:T(8,128)(4,1)S(1)} %iota_compare_fusion.1) | copy-start | bytes 150532
  42.1 13.3 %collective-permute-start.2 = (f32[40,128]{1,0:T(8,128)S(1)}, f32[40,128]{1,0:T(8,128)S(1)}, u32[]{:S(2)}, u32[]{:S(2)}) collective-permute-start(f32[40,128]{1,0:T(8,128)S(1)} %maximum_bitcast_fusion), channel_id=1, source_target_pairs={{0,32},{32,64},{64,96},{1,33},{33,65},{65,97},{2,34},{34,66},{66,9... | collective-permute-start | bytes 61448 | tf_op jit(solution)/shard_map/ppermute | solution.py:65
  50.0 9.0 %collective-permute-start.1 = (f32[40,128]{1,0:T(8,128)S(1)}, f32[40,128]{1,0:T(8,128)S(1)}, u32[]{:S(2)}, u32[]{:S(2)}) collective-permute-start(f32[40,128]{1,0:T(8,128)S(1)} %maximum_bitcast_fusion), channel_id=1, source_target_pairs={{0,64},{32,96},{1,65},{33,97},{2,66},{34,98},{3,67},{35,99},{4,68}... | collective-permute-start | bytes 61448 | tf_op jit(solution)/shard_map/ppermute | solution.py:65
  55.3 5.1 %collective-permute-start = (f32[40,128]{1,0:T(8,128)S(1)}, f32[40,128]{1,0:T(8,128)S(1)}, u32[]{:S(2)}, u32[]{:S(2)}) collective-permute-start(f32[40,128]{1,0:T(8,128)S(1)} %maximum_bitcast_fusion), channel_id=1, source_target_pairs={{0,96},{1,97},{2,98},{3,99},{4,100},{5,101},{6,102},{7,103},{8,104... | collective-permute-start | bytes 61448 | tf_op jit(solution)/shard_map/ppermute | solution.py:65
  62.1 30.7 %all-to-all-start.1 = ((f32[8,40,128]{2,1,0:T(8,128)}), f32[8,40,128]{2,1,0:T(8,128)S(1)}, u32[]{:S(2)}, u32[]{:S(2)}) async-start(f32[8,40,128]{2,1,0:T(8,128)} %maximum_maximum_fusion.1), calls=%async_computation.1 | async-start | bytes 327680 | tf_op jit(solution)/shard_map/all_to_all | solution.py:26
  68.4 13.5 %collective-permute-start.6 = (bf16[4,64,512]{2,1,0:T(8,128)(2,1)S(1)}, bf16[4,64,512]{2,1,0:T(8,128)(2,1)S(1)}, u32[]{:S(2)}, u32[]{:S(2)}) collective-permute-start(bf16[4,64,512]{2,1,0:T(8,128)(2,1)S(1)} %get-tuple-element.23), channel_id=1, source_target_pairs={{0,8},{8,16},{16,24},{24,32},{32,40},{40,48},{48,56},{56,64},{64,7... | collective-permute-start | bytes 786440 | tf_op jit(solution)/shard_map/ppermute | solution.py:22
  70.5 17.1 %collective-permute-start.7 = (bf16[4,64,512]{2,1,0:T(8,128)(2,1)S(1)}, bf16[4,64,512]{2,1,0:T(8,128)(2,1)S(1)}, u32[]{:S(2)}, u32[]{:S(2)}) collective-permute-start(bf16[4,64,512]{2,1,0:T(8,128)(2,1)S(1)} %get-tuple-element.23), channel_id=1, source_target_pairs={{0,120},{8,0},{16,8},{24,16},{32,24},{40,32},{48,40},{56,48},{64,5... | collective-permute-start | bytes 786440 | tf_op jit(solution)/shard_map/ppermute | solution.py:22
  75.4 17.1 %collective-permute-start.8 = (bf16[4,64,512]{2,1,0:T(8,128)(2,1)S(1)}, bf16[4,64,512]{2,1,0:T(8,128)(2,1)S(1)}, u32[]{:S(2)}, u32[]{:S(2)}) collective-permute-start(bf16[4,64,512]{2,1,0:T(8,128)(2,1)S(1)} %get-tuple-element.23), channel_id=1, source_target_pairs={{0,112},{8,120},{16,0},{24,8},{32,16},{40,24},{48,32},{56,40},{64,... | collective-permute-start | bytes 786440 | tf_op jit(solution)/shard_map/ppermute | solution.py:22
  92.6 2.8 collective-permute-start.9
  96.8 6.5 %copy-start.6 = (bf16[2048]{0:T(1024)(128)(2,1)S(1)}, bf16[2048]{0:T(1024)(128)(2,1)}, u32[]{:S(2)}) copy-start(bf16[2048]{0:T(1024)(128)(2,1)} %param.24) | copy-start | bytes 12292
  96.8 6.6 %copy-start.8 = (s32[56,2]{0,1:T(2,128)S(1)}, s32[56,2]{0,1:T(2,128)}, u32[]{:S(2)}) copy-start(s32[56,2]{0,1:T(2,128)} %param.25) | copy-start | bytes 1348
  96.8 20.6 %copy-start.1 = (bf16[56,2048]{1,0:T(8,128)(2,1)S(1)}, bf16[56,2048]{1,0:T(8,128)(2,1)}, u32[]{:S(2)}) copy-start(bf16[56,2048]{1,0:T(8,128)(2,1)} %param.23) | copy-start | bytes 688132
  98.6 18.7 %all-to-all-start.2 = ((bf16[4,56,2048]{2,1,0:T(8,128)(2,1)}), bf16[4,56,2048]{2,1,0:T(8,128)(2,1)S(1)}, u32[]{:S(2)}, u32[]{:S(2)}) async-start(bf16[4,56,2048]{2,1,0:T(8,128)(2,1)} %bitcast.36), calls=%async_computation.2 | async-start | bytes 1835008 | tf_op jit(solution)/shard_map/all_to_all | solution.py:26
  118.4 68.3 %copy-start.10 = (bf16[1,2048,896]{2,1,0:T(8,128)(2,1)S(1)}, bf16[1,2048,896]{2,1,0:T(8,128)(2,1)}, u32[]{:S(2)}) copy-start(bf16[1,2048,896]{2,1,0:T(8,128)(2,1)} %param.27) | copy-start | bytes 11010052
  183.4 23.7 %collective-permute-start.10 = (bf16[224,2048]{1,0:T(8,128)(2,1)S(1)}, bf16[224,2048]{1,0:T(8,128)(2,1)}, u32[]{:S(2)}, u32[]{:S(2)}) collective-permute-start(bf16[224,2048]{1,0:T(8,128)(2,1)S(1)} %bitcast.201), channel_id=1, source_target_pairs={{0,1},{1,2},{2,3},{3,0},{4,5},{5,6},{6,7},{7,4},{8,9},{9,10},{10,1... | collective-permute-start | bytes 2752520 | tf_op jit(solution)/shard_map/ppermute | solution.py:22
  184.1 23.0 %collective-permute-start.11 = (bf16[224,2048]{1,0:T(8,128)(2,1)S(1)}, bf16[224,2048]{1,0:T(8,128)(2,1)}, u32[]{:S(2)}, u32[]{:S(2)}) collective-permute-start(bf16[224,2048]{1,0:T(8,128)(2,1)S(1)} %bitcast.202), channel_id=1, source_target_pairs={{0,3},{1,0},{2,1},{3,2},{4,7},{5,4},{6,5},{7,6},{8,11},{9,8},{10,9... | collective-permute-start | bytes 2752520 | tf_op jit(solution)/shard_map/ppermute | solution.py:22
  217.0 45.5 %collective-permute-start.12 = (bf16[224,2048]{1,0:T(8,128)(2,1)}, bf16[224,2048]{1,0:T(8,128)(2,1)}, u32[]{:S(2)}, u32[]{:S(2)}) collective-permute-start(bf16[224,2048]{1,0:T(8,128)(2,1)} %fusion.27), channel_id=1, source_target_pairs={{0,3},{1,0},{2,1},{3,2},{4,7},{5,4},{6,5},{7,6},{8,11},{9,8},{10,9... | collective-permute-start | bytes 2752520 | tf_op jit(solution)/shard_map/ppermute | solution.py:22
  225.4 12.3 %collective-permute-start.14 = (bf16[112,2048]{1,0:T(8,128)(2,1)S(1)}, bf16[112,2048]{1,0:T(8,128)(2,1)S(1)}, u32[]{:S(2)}, u32[]{:S(2)}) collective-permute-start(bf16[112,2048]{1,0:T(8,128)(2,1)S(1)} %slice.110), channel_id=1, source_target_pairs={{0,1},{1,2},{2,3},{3,0},{4,5},{5,6},{6,7},{7,4},{8,9},{9,10},{10,1... | collective-permute-start | bytes 1376264 | tf_op jit(solution)/shard_map/ppermute | solution.py:22
  226.6 22.1 %collective-permute-start.15 = (bf16[112,2048]{1,0:T(8,128)(2,1)S(1)}, bf16[112,2048]{1,0:T(8,128)(2,1)}, u32[]{:S(2)}, u32[]{:S(2)}) collective-permute-start(bf16[112,2048]{1,0:T(8,128)(2,1)S(1)} %slice.111), channel_id=1, source_target_pairs={{0,3},{1,0},{2,1},{3,2},{4,7},{5,4},{6,5},{7,6},{8,11},{9,8},{10,9... | collective-permute-start | bytes 1376264 | tf_op jit(solution)/shard_map/ppermute | solution.py:22
  236.8 25.7 %collective-permute-start.13 = (bf16[224,2048]{1,0:T(8,128)(2,1)}, bf16[224,2048]{1,0:T(8,128)(2,1)}, u32[]{:S(2)}, u32[]{:S(2)}) collective-permute-start(bf16[224,2048]{1,0:T(8,128)(2,1)} %fusion.30), channel_id=1, source_target_pairs={{0,1},{1,2},{2,3},{3,0},{4,5},{5,6},{6,7},{7,4},{8,9},{9,10},{10,1... | collective-permute-start | bytes 2752520 | tf_op jit(solution)/shard_map/ppermute | solution.py:22
  260.2 30.8 %copy-start.9 = (f32[56,2]{0,1:T(2,128)S(1)}, f32[56,2]{0,1:T(2,128)}, u32[]{:S(2)}) copy-start(f32[56,2]{0,1:T(2,128)} %param.26) | copy-start | bytes 1348
  260.2 22.2 %collective-permute-start.16 = (bf16[224,2048]{1,0:T(8,128)(2,1)}, bf16[224,2048]{1,0:T(8,128)(2,1)S(1)}, u32[]{:S(2)}, u32[]{:S(2)}) collective-permute-start(bf16[224,2048]{1,0:T(8,128)(2,1)} %fusion.33), channel_id=1, source_target_pairs={{0,2},{1,3},{2,0},{3,1},{4,6},{5,7},{6,4},{7,5},{8,10},{9,11},{10,... | collective-permute-start | bytes 2752520 | tf_op jit(solution)/shard_map/ppermute | solution.py:22
  285.9 60.3 %all-to-all-start.4 = ((bf16[32,7,2048]{2,1,0:T(8,128)(2,1)}), bf16[32,7,2048]{2,1,0:T(8,128)(2,1)S(1)}, u32[]{:S(2)}, u32[]{:S(2)}) async-start(bf16[32,7,2048]{2,1,0:T(8,128)(2,1)} %bitcast.198), calls=%async_computation.4 | async-start | bytes 2097152 | tf_op jit(solution)/shard_map/all_to_all | solution.py:26
where the time goes:
time: 350 us; the launch traced here: 348 us
  waiting for transfers between devices  130 us (37%)
  starting transfers between devices  85.4 us (24%)
  blocking collectives  64.4 us (18%)
  matrix products  46.3 us (13%)
  other arithmetic  11.2 us (3%)
  local copies, waits for them, and re-layouts  10.4 us (3%)
    all_to_all x4, waiting for transfers between devices, traded(): return lax.all_to_all(x, axis, split_axis=0, concat_axis=0, tiled=True)  68.9 us
    all_to_all x1, blocking collectives, traded(): return lax.all_to_all(x, axis, split_axis=0, concat_axis=0, tiled=True)  64.4 us
    ppermute x14, waiting for transfers between devices, shifted(): return lax.ppermute(x, axis, [(i, (i + by) % size) for i in range(size)])  59.4 us
    ppermute x14, starting transfers between devices, shifted(): return lax.ppermute(x, axis, [(i, (i + by) % size) for i in range(size)])  45.3 us
    dot_general x4, matrix products, expert_part(): jnp.dot(hidden, down_w, preferred_element_type=jnp.float32)  25.2 us
    all_to_all x4, starting transfers between devices, traded(): return lax.all_to_all(x, axis, split_axis=0, concat_axis=0, tiled=True)  23.5 us
    ppermute x3, starting transfers between devices, states_before(): lax.ppermute(whole, 'far', [(i, i + back) for i in range(far - back)])  16.6 us
    dot_general x3, matrix products, expert_part(): gate = jnp.dot(rows_in, gate_w, preferred_element_type=jnp.float32)  10.4 us
  transfers between devices with their start and end apart: 21, of which 11 were waited for; matrix products, arithmetic and copies ran while one was open for 12% of the time, Pallas kernels for 0%

commit v1 on v0

--- a/solution.py
+++ b/solution.py
@@ -1,6 +1,8 @@
 import jax
 import jax.numpy as jnp
 from jax import lax
+from jax.experimental import pallas as pl
+from jax.experimental.pallas import tpu as pltpu
 from jax.sharding import Mesh
 from jax.sharding import PartitionSpec as P
 
@@ -99,11 +101,50 @@
     return whole.reshape(-1, own.shape[1])
 
 
+def expert_body(units, rows_ref, gate_ref, up_ref, down_ref, out_ref, hidden_ref):
+    step = pl.program_id(0)
+
+    @pl.when(step < units)
+    def _():
+        both = jnp.concatenate([gate_ref[...], up_ref[...]], axis=1)
+        made = jnp.dot(rows_ref[...], both, preferred_element_type=jnp.float32)
+        gate, upward = made[:, : gate_ref.shape[1]], made[:, gate_ref.shape[1] :]
+        hidden = gate / (1.0 + jnp.exp(-gate)) * upward
+        at = pl.multiple_of(step * gate_ref.shape[1], gate_ref.shape[1])
+        hidden_ref[:, pl.ds(at, gate_ref.shape[1])] = hidden.astype(jnp.bfloat16)
+
+    @pl.when(step >= units)
+    def _():
+        out_ref[...] = jnp.dot(
+            hidden_ref[...], down_ref[...], preferred_element_type=jnp.float32
+        ).astype(jnp.bfloat16)
+
+
 def expert_part(rows_in, gate_w, up_w, down_w):
-    gate = jnp.dot(rows_in, gate_w, preferred_element_type=jnp.float32)
-    upward = jnp.dot(rows_in, up_w, preferred_element_type=jnp.float32)
-    hidden = (jax.nn.silu(gate) * upward).astype(jnp.bfloat16)
-    return jnp.dot(hidden, down_w, preferred_element_type=jnp.float32).astype(jnp.bfloat16)
+    count, width = rows_in.shape
+    inner = gate_w.shape[1]
+    unit, wide = 128, 512
+    units, columns = inner // unit, width // wide
+    return pl.pallas_call(
+        lambda *refs: expert_body(units, *refs),
+        grid=(units + columns,),
+        in_specs=[
+            pl.BlockSpec((count, width), lambda i: (0, 0)),
+            pl.BlockSpec((width, unit), lambda i: (0, jnp.minimum(i, units - 1))),
+            pl.BlockSpec((width, unit), lambda i: (0, jnp.minimum(i, units - 1))),
+            pl.BlockSpec((inner, wide), lambda i: (0, jnp.maximum(i - units, 0))),
+        ],
+        out_specs=pl.BlockSpec((count, wide), lambda i: (0, jnp.maximum(i - units, 0))),
+        out_shape=jax.ShapeDtypeStruct((count, width), jnp.bfloat16),
+        scratch_shapes=[pltpu.VMEM((count, inner), jnp.bfloat16)],
+        compiler_params=pltpu.CompilerParams(dimension_semantics=("arbitrary",)),
+        cost_estimate=pl.CostEstimate(
+            flops=6 * count * width * inner,
+            bytes_accessed=6 * width * inner + 4 * count * width,
+            transcendentals=count * inner,
+        ),
+        name="expert_part",
+    )(rows_in, gate_w, up_w, down_w)
 
 
 def shards(
@@ -219,13 +260,16 @@
     across = [shifted(left[:half], "tp", 1), shifted(right[half:], "tp", size - 1)]
     left, right, _ = lax.optimization_barrier((left, right, own))
     from_left = expert_part(left, *weights)
-    parts = [own, shifted(from_left, "tp", size - 1)]
     right, _ = lax.optimization_barrier((right, from_left))
     from_right = expert_part(right, *weights)
-    parts.append(shifted(from_right, "tp", 1))
     across, _ = lax.optimization_barrier((jnp.concatenate(across, axis=0), from_right))
     from_across = expert_part(across, *weights)
-    parts.append(shifted(from_across, "tp", 2))
+    parts = [
+        own,
+        shifted(from_left, "tp", size - 1),
+        shifted(from_right, "tp", 1),
+        shifted(from_across, "tp", 2),
+    ]
     total_out = sum(part.astype(jnp.float32) for part in parts)
     expert_out = total_out.astype(jnp.bfloat16).reshape(slots, experts, width)
     back = traded(jnp.transpose(expert_out, (1, 0, 2)), SP)

time: 350 us -> 340 us (0.971)
  Pallas kernels: 0 us -> 47 us
  matrix products: 46.3 us -> 7.06 us
  waiting for transfers between devices: 130 us -> 121 us
  starting transfers between devices: 85.4 us -> 77.5 us
    pallas_call x0 -> x4, Pallas kernels: none -> 47 us  [expert_part(): pl.pallas_call(lambda *refs: expert_body(units, *refs), grid=(units + col...]
    dot_general x8 -> x0, matrix products: 39 us -> none  [the longest x4 25.2 us: expert_part(): jnp.dot(hidden, down_w, preferred_element_type=jnp.float32)]
    ppermute x14, waiting for transfers between devices: 59.4 us -> 50 us  [shifted(): return lax.ppermute(x, axis, [(i, (i + by) % size) for i in range(size)])]
    ppermute x3, starting transfers between devices: 16.6 us -> 12.3 us  [states_before(): lax.ppermute(whole, 'far', [(i, i + back) for i in range(far - back)])]
  transfers between devices with their start and end apart: 21 -> 21, of which waited for: 11 -> 8; matrix products, arithmetic and copies ran while one was open for 12% -> 4% of each run, Pallas kernels for 0% -> 14%
where the time goes in v1:
time: 340 us; the launch traced here: 338 us
  waiting for transfers between devices  121 us (36%)
  starting transfers between devices  77.5 us (23%)
  blocking collectives  65 us (19%)
  Pallas kernels  47 us (14%)
  local copies, waits for them, and re-layouts  10.6 us (3%)
  other arithmetic  9.99 us (3%)
  matrix products  7.06 us (2%)
    all_to_all x4, waiting for transfers between devices, traded(): return lax.all_to_all(x, axis, split_axis=0, concat_axis=0, tiled=True)  69.2 us
    all_to_all x1, blocking collectives, traded(): return lax.all_to_all(x, axis, split_axis=0, concat_axis=0, tiled=True)  65 us
    ppermute x14, waiting for transfers between devices, shifted(): return lax.ppermute(x, axis, [(i, (i + by) % size) for i in range(size)])  50 us
    pallas_call x4, Pallas kernels, expert_part(): pl.pallas_call(lambda *refs: expert_body(units, *refs), grid=(units + col...  47 us
    ppermute x14, starting transfers between devices, shifted(): return lax.ppermute(x, axis, [(i, (i + by) % size) for i in range(size)])  42 us
    all_to_all x4, starting transfers between devices, traded(): return lax.all_to_all(x, axis, split_axis=0, concat_axis=0, tiled=True)  23.2 us
    ppermute x3, starting transfers between devices, states_before(): lax.ppermute(whole, 'far', [(i, i + back) for i in range(far - back)])  12.3 us
  transfers between devices with their start and end apart: 21, of which 8 were waited for; matrix products, arithmetic and copies ran while one was open for 4% of the time, Pallas kernels for 14%

profile of v1, /device:TPU:40, one launch (start us, length us, event | category | flops | bytes accessed | tf_op | source)
XLA Modules:
  0.0 338.3 jit_solution(206275354596959257)
XLA Ops:
  0.0 0.9 fusion.34
  0.9 0.2 slice_reduce_fusion.4
  1.1 0.9 fusion.76
  2.0 0.8 exponential_bitcast_fusion
  3.1 1.0 copy.79
  4.2 0.5 fusion.17
  4.8 0.8 maximum_maximum_fusion
  5.6 8.5 %all-to-all-start = ((f32[8,40,128]{2,1,0:T(8,128)}), f32[8,40,128]{2,1,0:T(8,128)S(1)}, u32[]{:S(2)}, u32[]{:S(2)}) async-start(f32[8,40,128]{2,1,0:T(8,128)} %maximum_maximum_fusion), calls=%async_computation | async-start | bytes 327680 | tf_op jit(solution)/shard_map/all_to_all | solution.py:28
  14.1 10.6 %collective-permute-start.5 = (bf16[64,512]{1,0:T(8,128)(2,1)}, bf16[64,512]{1,0:T(8,128)(2,1)S(1)}, u32[]{:S(2)}, u32[]{:S(2)}) collective-permute-start(bf16[64,512]{1,0:T(8,128)(2,1)} %bitcast.163), channel_id=1, source_target_pairs={{0,32},{32,64},{64,96},{96,0},{1,33},{33,65},{65,97},{97,1},{2,34}... | collective-permute-start | bytes 196616 | tf_op jit(solution)/shard_map/ppermute | solution.py:24
  24.7 13.2 %collective-permute-start.4 = (bf16[64,512]{1,0:T(8,128)(2,1)}, bf16[64,512]{1,0:T(8,128)(2,1)S(1)}, u32[]{:S(2)}, u32[]{:S(2)}) collective-permute-start(bf16[64,512]{1,0:T(8,128)(2,1)} %bitcast.164), channel_id=1, source_target_pairs={{0,64},{32,96},{64,0},{96,32},{1,65},{33,97},{65,1},{97,33},{2,66}... | collective-permute-start | bytes 196616 | tf_op jit(solution)/shard_map/ppermute | solution.py:24
  38.0 0.7 slice_bitcast_fusion.3
  38.7 0.6 slice_reduce_fusion.2
  39.6 0.7 slice.88
  40.4 0.8 pad.28.clone
  41.2 0.7 pad.27.clone
  42.1 7.8 %collective-permute-start.2 = (f32[40,128]{1,0:T(8,128)S(1)}, f32[40,128]{1,0:T(8,128)S(1)}, u32[]{:S(2)}, u32[]{:S(2)}) collective-permute-start(f32[40,128]{1,0:T(8,128)S(1)} %maximum_bitcast_fusion), channel_id=1, source_target_pairs={{0,32},{32,64},{64,96},{1,33},{33,65},{65,97},{2,34},{34,66},{66,9... | collective-permute-start | bytes 61448 | tf_op jit(solution)/shard_map/ppermute | solution.py:67
  50.1 2.5 collective-permute-start.1
  52.5 2.1 collective-permute-start
  54.7 1.5 collective-permute-done
  57.1 0.8 maximum_maximum_fusion.1
  57.8 5.1 %all-to-all-start.1 = ((f32[8,40,128]{2,1,0:T(8,128)}), f32[8,40,128]{2,1,0:T(8,128)S(1)}, u32[]{:S(2)}, u32[]{:S(2)}) async-start(f32[8,40,128]{2,1,0:T(8,128)} %maximum_maximum_fusion.1), calls=%async_computation.1 | async-start | bytes 327680 | tf_op jit(solution)/shard_map/all_to_all | solution.py:28
  63.0 6.9 %collective-permute-start.8 = (bf16[4,64,512]{2,1,0:T(8,128)(2,1)S(1)}, bf16[4,64,512]{2,1,0:T(8,128)(2,1)S(1)}, u32[]{:S(2)}, u32[]{:S(2)}) collective-permute-start(bf16[4,64,512]{2,1,0:T(8,128)(2,1)S(1)} %get-tuple-element.23), channel_id=1, source_target_pairs={{0,112},{8,120},{16,0},{24,8},{32,16},{40,24},{48,32},{56,40},{64,... | collective-permute-start | bytes 786440 | tf_op jit(solution)/shard_map/ppermute | solution.py:24
  69.9 0.6 collective-permute-start.7
  70.5 1.5 collective-permute-start.6
  71.9 0.4 fusion.15
  72.5 9.8 %collective-permute-done.8 = bf16[4,64,512]{2,1,0:T(8,128)(2,1)S(1)} collective-permute-done((bf16[4,64,512]{2,1,0:T(8,128)(2,1)S(1)}, bf16[4,64,512]{2,1,0:T(8,128)(2,1)S(1)}, u32[]{:S(2)}, u32[]{:S(2)}) %collective-permute-start.8) | collective-permute-done | bytes 262176 | tf_op jit(solution)/shard_map/ppermute | solution.py:24
  82.3 4.9 %collective-permute-done.7 = bf16[4,64,512]{2,1,0:T(8,128)(2,1)S(1)} collective-permute-done((bf16[4,64,512]{2,1,0:T(8,128)(2,1)S(1)}, bf16[4,64,512]{2,1,0:T(8,128)(2,1)S(1)}, u32[]{:S(2)}, u32[]{:S(2)}) %collective-permute-start.7) | collective-permute-done | bytes 262176 | tf_op jit(solution)/shard_map/ppermute | solution.py:24
  87.8 0.4 fusion.8
  88.3 1.4 multiply_reduce_fusion.2
  89.7 0.5 collective-permute-done.9
  90.2 0.2 select_bitcast_fusion.1
  90.4 0.2 pad_maximum_fusion
  90.6 0.2 copy.89
  90.8 0.8 fusion.3
  91.6 0.2 copy-done.7
  91.8 1.8 convolution_convert_fusion
  93.6 4.7 %all-to-all-start.2 = ((bf16[4,56,2048]{2,1,0:T(8,128)(2,1)}), bf16[4,56,2048]{2,1,0:T(8,128)(2,1)S(1)}, u32[]{:S(2)}, u32[]{:S(2)}) async-start(bf16[4,56,2048]{2,1,0:T(8,128)(2,1)} %bitcast.36), calls=%async_computation.2 | async-start | bytes 1835008 | tf_op jit(solution)/shard_map/all_to_all | solution.py:28
  98.8 13.5 %all-to-all-done.2 = bf16[4,56,2048]{2,1,0:T(8,128)(2,1)S(1)} async-done(((bf16[4,56,2048]{2,1,0:T(8,128)(2,1)}), bf16[4,56,2048]{2,1,0:T(8,128)(2,1)S(1)}, u32[]{:S(2)}, u32[]{:S(2)}) %all-to-all-start.2) | async-done | bytes 917536 | tf_op jit(solution)/shard_map/all_to_all | solution.py:28
  112.6 0.5 convolution_convert_fusion.1
  113.2 0.3 reshape.129
  113.5 65.0 %all_to_all.25 = bf16[32,7,2048]{2,1,0:T(8,128)(2,1)S(1)} all-to-all(bf16[32,7,2048]{2,1,0:T(8,128)(2,1)S(1)} %reshape.129), channel_id=1, replica_groups=mesh['grp'=2,'far'=4,'near'=4,'core'=2,'tp'=4] {'far','near','core'}, dimensions={0} | all-to-all | bytes 1835008 | tf_op jit(solution)/shard_map/all_to_all | solution.py:28
  178.5 0.6 copy.90
  179.1 1.3 collective-permute-start.11
  180.4 0.9 collective-permute-start.10
  181.2 11.7 %expert_part.4 = bf16[224,2048]{1,0:T(8,128)(2,1)} custom-call(bf16[224,2048]{1,0:T(8,128)(2,1)} %bitcast.152, bf16[2048,896]{1,0:T(8,128)(2,1)} %bitcast.133, bf16[2048,896]{1,0:T(8,128)(2,1)} %bitcast.137, bf16[896,2048]{1,0:T(8,128)(2,1)} %bitcast.141), custom_call_target="tpu_custom_call" | custom-call | flops 2466250752 | bytes 12845056 | tf_op jit(solution)/shard_map/expert_part/pallas_call | solution.py:128
  192.9 8.5 %collective-permute-done.11.refs_0_ = bf16[224,2048]{1,0:T(8,128)(2,1)S(1)} collective-permute-done((bf16[224,2048]{1,0:T(8,128)(2,1)S(1)}, bf16[224,2048]{1,0:T(8,128)(2,1)S(1)}, u32[]{:S(2)}, u32[]{:S(2)}) %collective-permute-start.11) | collective-permute-done | bytes 917536 | tf_op jit(solution)/shard_map/ppermute | solution.py:24
  201.4 0.9 slice.111
  202.3 2.4 collective-permute-start.15
  204.7 0.9 slice.110
  205.5 0.2 copy-done.4
  205.8 11.7 %expert_part.5 = bf16[224,2048]{1,0:T(8,128)(2,1)} custom-call(bf16[224,2048]{1,0:T(8,128)(2,1)} %copy-done.4, bf16[2048,896]{1,0:T(8,128)(2,1)} %bitcast.134, bf16[2048,896]{1,0:T(8,128)(2,1)} %bitcast.138, bf16[896,2048]{1,0:T(8,128)(2,1)} %bitcast.142), custom_call_target="tpu_custom_call" | custom-call | flops 2466250752 | bytes 12845056 | tf_op jit(solution)/shard_map/expert_part/pallas_call | solution.py:128
  217.5 3.0 collective-permute-start.12
  220.5 11.7 %expert_part.6 = bf16[224,2048]{1,0:T(8,128)(2,1)} custom-call(bf16[224,2048]{1,0:T(8,128)(2,1)} %copy-done.3, bf16[2048,896]{1,0:T(8,128)(2,1)} %bitcast.135, bf16[2048,896]{1,0:T(8,128)(2,1)} %bitcast.139, bf16[896,2048]{1,0:T(8,128)(2,1)} %bitcast.143), custom_call_target="tpu_custom_call" | custom-call | flops 2466250752 | bytes 12845056 | tf_op jit(solution)/shard_map/expert_part/pallas_call | solution.py:128
  232.3 2.2 pad_maximum_fusion.2.refs_0_
  234.5 11.8 %expert_part.7 = bf16[224,2048]{1,0:T(8,128)(2,1)} custom-call(bf16[224,2048]{1,0:T(8,128)(2,1)} %pad_maximum_fusion.2.refs_0_, bf16[2048,896]{1,0:T(8,128)(2,1)} %bitcast.136, bf16[2048,896]{1,0:T(8,128)(2,1)} %bitcast.140, bf16[896,2048]{1,0:T(8,128)(2,1)} %bitcast.144), custom_call_target="tpu_custom_call" | custom-call | flops 2466250752 | bytes 12845056 | tf_op jit(solution)/shard_map/expert_part/pallas_call | solution.py:128
  246.3 1.5 collective-permute-start.16
  247.7 26.2 %collective-permute-done.13 = bf16[224,2048]{1,0:T(8,128)(2,1)S(1)} collective-permute-done((bf16[224,2048]{1,0:T(8,128)(2,1)}, bf16[224,2048]{1,0:T(8,128)(2,1)S(1)}, u32[]{:S(2)}, u32[]{:S(2)}) %collective-permute-start.13) | collective-permute-done | bytes 917536 | tf_op jit(solution)/shard_map/ppermute | solution.py:24
  273.9 0.6 add_convert_fusion
  274.5 1.5 copy.109
  276.0 4.8 %all-to-all-start.4 = ((bf16[32,7,2048]{2,1,0:T(8,128)(2,1)}), bf16[32,7,2048]{2,1,0:T(8,128)(2,1)S(1)}, u32[]{:S(2)}, u32[]{:S(2)}) async-start(bf16[32,7,2048]{2,1,0:T(8,128)(2,1)} %bitcast.148), calls=%async_computation.4 | async-start | bytes 2097152 | tf_op jit(solution)/shard_map/all_to_all | solution.py:28
  280.9 55.7 %all-to-all-done.4 = bf16[32,7,2048]{2,1,0:T(8,128)(2,1)S(1)} async-done(((bf16[32,7,2048]{2,1,0:T(8,128)(2,1)}), bf16[32,7,2048]{2,1,0:T(8,128)(2,1)S(1)}, u32[]{:S(2)}, u32[]{:S(2)}) %all-to-all-start.4) | async-done | bytes 917536 | tf_op jit(solution)/shard_map/all_to_all | solution.py:28
  336.6 0.3 reshape.132
  336.9 0.3 convolution_multiply_fusion
  337.2 1.0 fusion.2
  (97 shorter events, 3.9 us)
Async XLA Ops:
  0.0 4.2 %copy-start = (bf16[224,512]{1,0:T(8,128)(2,1)S(1)}, bf16[224,512]{1,0:T(8,128)(2,1)}, u32[]{:S(2)}) copy-start(bf16[224,512]{1,0:T(8,128)(2,1)} %param.17) | copy-start | bytes 688132
  0.0 63.0 %copy-start.9 = (bf16[512,64]{0,1:T(8,128)(2,1)S(1)}, bf16[512,64]{0,1:T(8,128)(2,1)}, u32[]{:S(2)}) copy-start(bf16[512,64]{0,1:T(8,128)(2,1)} %param.22) | copy-start | bytes 196612
  3.1 68.9 %copy-start.10 = (f32[4,224]{1,0:T(4,128)S(1)}, f32[4,224]{1,0:T(4,128)}, u32[]{:S(2)}) copy-start(f32[4,224]{1,0:T(4,128)} %param.18) | copy-start | bytes 10756
  4.1 68.3 %copy-start.8 = (bf16[224,256]{1,0:T(8,128)(2,1)S(1)}, bf16[224,256]{1,0:T(8,128)(2,1)}, u32[]{:S(2)}) copy-start(bf16[224,256]{1,0:T(8,128)(2,1)} %param.15) | copy-start | bytes 344068
  4.2 68.3 %copy-start.12 = (bf16[512]{0:T(512)(128)(2,1)S(1)}, bf16[512]{0:T(512)(128)(2,1)}, u32[]{:S(2)}) copy-start(bf16[512]{0:T(512)(128)(2,1)} %param.21) | copy-start | bytes 3076
  5.6 33.1 %all-to-all-start = ((f32[8,40,128]{2,1,0:T(8,128)}), f32[8,40,128]{2,1,0:T(8,128)S(1)}, u32[]{:S(2)}, u32[]{:S(2)}) async-start(f32[8,40,128]{2,1,0:T(8,128)} %maximum_maximum_fusion), calls=%async_computation | async-start | bytes 327680 | tf_op jit(solution)/shard_map/all_to_all | solution.py:28
  14.1 48.9 %collective-permute-start.5 = (bf16[64,512]{1,0:T(8,128)(2,1)}, bf16[64,512]{1,0:T(8,128)(2,1)S(1)}, u32[]{:S(2)}, u32[]{:S(2)}) collective-permute-start(bf16[64,512]{1,0:T(8,128)(2,1)} %bitcast.163), channel_id=1, source_target_pairs={{0,32},{32,64},{64,96},{96,0},{1,33},{33,65},{65,97},{97,1},{2,34}... | collective-permute-start | bytes 196616 | tf_op jit(solution)/shard_map/ppermute | solution.py:24
  24.7 38.2 %collective-permute-start.4 = (bf16[64,512]{1,0:T(8,128)(2,1)}, bf16[64,512]{1,0:T(8,128)(2,1)S(1)}, u32[]{:S(2)}, u32[]{:S(2)}) collective-permute-start(bf16[64,512]{1,0:T(8,128)(2,1)} %bitcast.164), channel_id=1, source_target_pairs={{0,64},{32,96},{64,0},{96,32},{1,65},{33,97},{65,1},{97,33},{2,66}... | collective-permute-start | bytes 196616 | tf_op jit(solution)/shard_map/ppermute | solution.py:24
  37.9 25.1 %collective-permute-start.3 = (bf16[64,512]{1,0:T(8,128)(2,1)}, bf16[64,512]{1,0:T(8,128)(2,1)S(1)}, u32[]{:S(2)}, u32[]{:S(2)}) collective-permute-start(bf16[64,512]{1,0:T(8,128)(2,1)} %bitcast.165), channel_id=1, source_target_pairs={{0,96},{32,0},{64,32},{96,64},{1,97},{33,1},{65,33},{97,65},{2,98}... | collective-permute-start | bytes 196616 | tf_op jit(solution)/shard_map/ppermute | solution.py:24
  42.1 10.4 %collective-permute-start.2 = (f32[40,128]{1,0:T(8,128)S(1)}, f32[40,128]{1,0:T(8,128)S(1)}, u32[]{:S(2)}, u32[]{:S(2)}) collective-permute-start(f32[40,128]{1,0:T(8,128)S(1)} %maximum_bitcast_fusion), channel_id=1, source_target_pairs={{0,32},{32,64},{64,96},{1,33},{33,65},{65,97},{2,34},{34,66},{66,9... | collective-permute-start | bytes 61448 | tf_op jit(solution)/shard_map/ppermute | solution.py:67
  50.1 4.6 %collective-permute-start.1 = (f32[40,128]{1,0:T(8,128)S(1)}, f32[40,128]{1,0:T(8,128)S(1)}, u32[]{:S(2)}, u32[]{:S(2)}) collective-permute-start(f32[40,128]{1,0:T(8,128)S(1)} %maximum_bitcast_fusion), channel_id=1, source_target_pairs={{0,64},{32,96},{1,65},{33,97},{2,66},{34,98},{3,67},{35,99},{4,68}... | collective-permute-start | bytes 61448 | tf_op jit(solution)/shard_map/ppermute | solution.py:67
  52.5 3.6 %collective-permute-start = (f32[40,128]{1,0:T(8,128)S(1)}, f32[40,128]{1,0:T(8,128)S(1)}, u32[]{:S(2)}, u32[]{:S(2)}) collective-permute-start(f32[40,128]{1,0:T(8,128)S(1)} %maximum_bitcast_fusion), channel_id=1, source_target_pairs={{0,96},{1,97},{2,98},{3,99},{4,100},{5,101},{6,102},{7,103},{8,104... | collective-permute-start | bytes 61448 | tf_op jit(solution)/shard_map/ppermute | solution.py:67
  57.8 29.7 %all-to-all-start.1 = ((f32[8,40,128]{2,1,0:T(8,128)}), f32[8,40,128]{2,1,0:T(8,128)S(1)}, u32[]{:S(2)}, u32[]{:S(2)}) async-start(f32[8,40,128]{2,1,0:T(8,128)} %maximum_maximum_fusion.1), calls=%async_computation.1 | async-start | bytes 327680 | tf_op jit(solution)/shard_map/all_to_all | solution.py:28
  63.0 19.3 %collective-permute-start.8 = (bf16[4,64,512]{2,1,0:T(8,128)(2,1)S(1)}, bf16[4,64,512]{2,1,0:T(8,128)(2,1)S(1)}, u32[]{:S(2)}, u32[]{:S(2)}) collective-permute-start(bf16[4,64,512]{2,1,0:T(8,128)(2,1)S(1)} %get-tuple-element.23), channel_id=1, source_target_pairs={{0,112},{8,120},{16,0},{24,8},{32,16},{40,24},{48,32},{56,40},{64,... | collective-permute-start | bytes 786440 | tf_op jit(solution)/shard_map/ppermute | solution.py:24
  69.9 17.3 %collective-permute-start.7 = (bf16[4,64,512]{2,1,0:T(8,128)(2,1)S(1)}, bf16[4,64,512]{2,1,0:T(8,128)(2,1)S(1)}, u32[]{:S(2)}, u32[]{:S(2)}) collective-permute-start(bf16[4,64,512]{2,1,0:T(8,128)(2,1)S(1)} %get-tuple-element.23), channel_id=1, source_target_pairs={{0,120},{8,0},{16,8},{24,16},{32,24},{40,32},{48,40},{56,48},{64,5... | collective-permute-start | bytes 786440 | tf_op jit(solution)/shard_map/ppermute | solution.py:24
  70.5 16.8 %collective-permute-start.6 = (bf16[4,64,512]{2,1,0:T(8,128)(2,1)S(1)}, bf16[4,64,512]{2,1,0:T(8,128)(2,1)S(1)}, u32[]{:S(2)}, u32[]{:S(2)}) collective-permute-start(bf16[4,64,512]{2,1,0:T(8,128)(2,1)S(1)} %get-tuple-element.23), channel_id=1, source_target_pairs={{0,8},{8,16},{16,24},{24,32},{32,40},{40,48},{48,56},{56,64},{64,7... | collective-permute-start | bytes 786440 | tf_op jit(solution)/shard_map/ppermute | solution.py:24
  87.4 2.8 collective-permute-start.9
  90.8 1.0 copy-start.7
  91.8 6.6 %copy-start.11 = (bf16[2048]{0:T(1024)(128)(2,1)S(1)}, bf16[2048]{0:T(1024)(128)(2,1)}, u32[]{:S(2)}) copy-start(bf16[2048]{0:T(1024)(128)(2,1)} %param.24) | copy-start | bytes 12292
  91.8 6.7 %copy-start.13 = (s32[56,2]{0,1:T(2,128)S(1)}, s32[56,2]{0,1:T(2,128)}, u32[]{:S(2)}) copy-start(s32[56,2]{0,1:T(2,128)} %param.25) | copy-start | bytes 1348
  93.6 18.9 %copy-start.5 = (bf16[56,2048]{1,0:T(8,128)(2,1)S(1)}, bf16[56,2048]{1,0:T(8,128)(2,1)}, u32[]{:S(2)}) copy-start(bf16[56,2048]{1,0:T(8,128)(2,1)} %param.23) | copy-start | bytes 688132
  93.6 18.7 %all-to-all-start.2 = ((bf16[4,56,2048]{2,1,0:T(8,128)(2,1)}), bf16[4,56,2048]{2,1,0:T(8,128)(2,1)S(1)}, u32[]{:S(2)}, u32[]{:S(2)}) async-start(bf16[4,56,2048]{2,1,0:T(8,128)(2,1)} %bitcast.36), calls=%async_computation.2 | async-start | bytes 1835008 | tf_op jit(solution)/shard_map/all_to_all | solution.py:28
  179.1 2.2 copy-start.1
  179.1 22.4 %collective-permute-start.11 = (bf16[224,2048]{1,0:T(8,128)(2,1)S(1)}, bf16[224,2048]{1,0:T(8,128)(2,1)S(1)}, u32[]{:S(2)}, u32[]{:S(2)}) collective-permute-start(bf16[224,2048]{1,0:T(8,128)(2,1)S(1)} %bitcast.150), channel_id=1, source_target_pairs={{0,3},{1,0},{2,1},{3,2},{4,7},{5,4},{6,5},{7,6},{8,11},{9,8},{10,9... | collective-permute-start | bytes 2752520 | tf_op jit(solution)/shard_map/ppermute | solution.py:24
  180.4 24.3 %collective-permute-start.10 = (bf16[224,2048]{1,0:T(8,128)(2,1)S(1)}, bf16[224,2048]{1,0:T(8,128)(2,1)S(1)}, u32[]{:S(2)}, u32[]{:S(2)}) collective-permute-start(bf16[224,2048]{1,0:T(8,128)(2,1)S(1)} %bitcast.151), channel_id=1, source_target_pairs={{0,1},{1,2},{2,3},{3,0},{4,5},{5,6},{6,7},{7,4},{8,9},{9,10},{10,1... | collective-permute-start | bytes 2752520 | tf_op jit(solution)/shard_map/ppermute | solution.py:24
  201.4 16.1 %copy-start.3 = (bf16[224,2048]{1,0:T(8,128)(2,1)}, bf16[224,2048]{1,0:T(8,128)(2,1)S(1)}, u32[]{:S(2)}) copy-start(bf16[224,2048]{1,0:T(8,128)(2,1)S(1)} %collective-permute-done.11.refs_0_) | copy-start | bytes 2752516
  202.3 30.0 %collective-permute-start.15 = (bf16[112,2048]{1,0:T(8,128)(2,1)}, bf16[112,2048]{1,0:T(8,128)(2,1)}, u32[]{:S(2)}, u32[]{:S(2)}) collective-permute-start(bf16[112,2048]{1,0:T(8,128)(2,1)} %slice.111), channel_id=1, source_target_pairs={{0,3},{1,0},{2,1},{3,2},{4,7},{5,4},{6,5},{7,6},{8,11},{9,8},{10,9... | collective-permute-start | bytes 1376264 | tf_op jit(solution)/shard_map/ppermute | solution.py:24
  204.7 1.1 copy-start.4
  205.5 26.7 %collective-permute-start.14 = (bf16[112,2048]{1,0:T(8,128)(2,1)}, bf16[112,2048]{1,0:T(8,128)(2,1)}, u32[]{:S(2)}, u32[]{:S(2)}) collective-permute-start(bf16[112,2048]{1,0:T(8,128)(2,1)} %slice.110), channel_id=1, source_target_pairs={{0,1},{1,2},{2,3},{3,0},{4,5},{5,6},{6,7},{7,4},{8,9},{9,10},{10,1... | collective-permute-start | bytes 1376264 | tf_op jit(solution)/shard_map/ppermute | solution.py:24
  217.5 56.4 %collective-permute-start.12 = (bf16[224,2048]{1,0:T(8,128)(2,1)}, bf16[224,2048]{1,0:T(8,128)(2,1)S(1)}, u32[]{:S(2)}, u32[]{:S(2)}) collective-permute-start(bf16[224,2048]{1,0:T(8,128)(2,1)} %expert_part.5), channel_id=1, source_target_pairs={{0,3},{1,0},{2,1},{3,2},{4,7},{5,4},{6,5},{7,6},{8,11},{9,8},{10,9... | collective-permute-start | bytes 2752520 | tf_op jit(solution)/shard_map/ppermute | solution.py:24
  232.3 41.6 %collective-permute-start.13 = (bf16[224,2048]{1,0:T(8,128)(2,1)}, bf16[224,2048]{1,0:T(8,128)(2,1)S(1)}, u32[]{:S(2)}, u32[]{:S(2)}) collective-permute-start(bf16[224,2048]{1,0:T(8,128)(2,1)} %expert_part.6), channel_id=1, source_target_pairs={{0,1},{1,2},{2,3},{3,0},{4,5},{5,6},{6,7},{7,4},{8,9},{9,10},{10,1... | collective-permute-start | bytes 2752520 | tf_op jit(solution)/shard_map/ppermute | solution.py:24
  234.5 39.4 %copy-start.2 = (bf16[224,2048]{1,0:T(8,128)(2,1)S(1)}, bf16[224,2048]{1,0:T(8,128)(2,1)}, u32[]{:S(2)}) copy-start(bf16[224,2048]{1,0:T(8,128)(2,1)} %expert_part.4) | copy-start | bytes 2752516
  246.3 27.7 %collective-permute-start.16 = (bf16[224,2048]{1,0:T(8,128)(2,1)}, bf16[224,2048]{1,0:T(8,128)(2,1)S(1)}, u32[]{:S(2)}, u32[]{:S(2)}) collective-permute-start(bf16[224,2048]{1,0:T(8,128)(2,1)} %expert_part.7), channel_id=1, source_target_pairs={{0,2},{1,3},{2,0},{3,1},{4,6},{5,7},{6,4},{7,5},{8,10},{9,11},{10,... | collective-permute-start | bytes 2752520 | tf_op jit(solution)/shard_map/ppermute | solution.py:24
  274.5 6.4 %copy-start.14 = (f32[56,2]{0,1:T(2,128)S(1)}, f32[56,2]{0,1:T(2,128)}, u32[]{:S(2)}) copy-start(f32[56,2]{0,1:T(2,128)} %param.26) | copy-start | bytes 1348
  276.0 60.6 %all-to-all-start.4 = ((bf16[32,7,2048]{2,1,0:T(8,128)(2,1)}), bf16[32,7,2048]{2,1,0:T(8,128)(2,1)S(1)}, u32[]{:S(2)}, u32[]{:S(2)}) async-start(bf16[32,7,2048]{2,1,0:T(8,128)(2,1)} %bitcast.148), calls=%async_computation.4 | async-start | bytes 2097152 | tf_op jit(solution)/shard_map/all_to_all | solution.py:28
  280.9 56.3 %copy-start.6 = (bf16[56,2048]{1,0:T(8,128)(2,1)S(1)}, bf16[56,2048]{1,0:T(8,128)(2,1)}, u32[]{:S(2)}) copy-start(bf16[56,2048]{1,0:T(8,128)(2,1)} %param.23) | copy-start | bytes 688132

commit v2 on v0

--- a/solution.py
+++ b/solution.py
@@ -1,6 +1,8 @@
 import jax
 import jax.numpy as jnp
 from jax import lax
+from jax.experimental import pallas as pl
+from jax.experimental.pallas import tpu as pltpu
 from jax.sharding import Mesh
 from jax.sharding import PartitionSpec as P
 
@@ -99,11 +101,94 @@
     return whole.reshape(-1, own.shape[1])
 
 
+def expert_body(rows_ref, gate_ref, up_ref, down_ref, out_ref, hidden_ref):
+    inner, width = down_ref.shape
+    unit, wide = 128, 256
+
+    def hide(k, _):
+        at = pl.ds(pl.multiple_of(k * unit, unit), unit)
+        both = jnp.concatenate([gate_ref[:, at], up_ref[:, at]], axis=1)
+        made = jnp.dot(rows_ref[...], both, preferred_element_type=jnp.float32)
+        gate, upward = made[:, :unit], made[:, unit:]
+        hidden = gate / (1.0 + jnp.exp(-gate)) * upward
+        hidden_ref[:, at] = hidden.astype(jnp.bfloat16)
+
+    def show(k, _):
+        at = pl.ds(pl.multiple_of(k * wide, wide), wide)
+        out_ref[:, at] = jnp.dot(
+            hidden_ref[...], down_ref[:, at], preferred_element_type=jnp.float32
+        ).astype(jnp.bfloat16)
+
+    lax.fori_loop(0, inner // unit, hide, None)
+    lax.fori_loop(0, width // wide, show, None)
+
+
 def expert_part(rows_in, gate_w, up_w, down_w):
-    gate = jnp.dot(rows_in, gate_w, preferred_element_type=jnp.float32)
-    upward = jnp.dot(rows_in, up_w, preferred_element_type=jnp.float32)
-    hidden = (jax.nn.silu(gate) * upward).astype(jnp.bfloat16)
-    return jnp.dot(hidden, down_w, preferred_element_type=jnp.float32).astype(jnp.bfloat16)
+    count, width = rows_in.shape
+    inner = gate_w.shape[1]
+    whole = pl.BlockSpec(memory_space=pltpu.VMEM)
+    return pl.pallas_call(
+        expert_body,
+        in_specs=[whole] * 4,
+        out_specs=whole,
+        out_shape=jax.ShapeDtypeStruct((count, width), jnp.bfloat16),
+        scratch_shapes=[pltpu.VMEM((count, inner), jnp.bfloat16)],
+        compiler_params=pltpu.CompilerParams(vmem_limit_bytes=24 << 20),
+        cost_estimate=pl.CostEstimate(
+            flops=6 * count * width * inner,
+            bytes_accessed=6 * width * inner + 4 * count * width,
+            transcendentals=count * inner,
+        ),
+        name="expert_part",
+    )(rows_in, gate_w, up_w, down_w)
+
+
+def packed(by_slot, lines):
+    slots, _, width = by_slot.shape
+    if slots < lines:
+        part = width * slots // lines
+        rest = [by_slot[s, :, part:] for s in range(slots)]
+        rest = jnp.concatenate(rest, axis=1)
+        rest = rest.reshape(rest.shape[0], lines - slots, part).swapaxes(0, 1)
+        by_slot = jnp.concatenate([by_slot[:, :, :part], rest], axis=0)
+    return jnp.transpose(by_slot, (1, 0, 2))
+
+
+def unpacked(messages, slots, width):
+    lines, part = messages.shape[1:]
+    by_line = jnp.transpose(messages, (1, 0, 2))
+    if slots == lines:
+        return by_line
+    rest = by_line[slots:].swapaxes(0, 1).reshape(by_line.shape[1], -1)
+    tail = width - part
+    return jnp.stack(
+        [
+            jnp.concatenate([by_line[s], rest[:, s * tail : (s + 1) * tail]], axis=1)
+            for s in range(slots)
+        ]
+    )
+
+
+def through_experts(by_slot, weights):
+    slots, peers, width = by_slot.shape
+    rows = by_slot.reshape(slots * peers, width)
+    size = lax.axis_size("tp")
+    half = rows.shape[0] // 2
+    left = shifted(rows, "tp", 1)
+    right = shifted(rows, "tp", size - 1)
+    own = expert_part(rows, *weights)
+    across = [shifted(left[:half], "tp", 1), shifted(right[half:], "tp", size - 1)]
+    left, right, _ = lax.optimization_barrier((left, right, own))
+    from_left = expert_part(left, *weights)
+    right, _ = lax.optimization_barrier((right, from_left))
+    from_right = expert_part(right, *weights)
+    across, _ = lax.optimization_barrier((jnp.concatenate(across, axis=0), from_right))
+    from_across = expert_part(across, *weights)
+    parts = [own]
+    for piece, by in ((from_left, size - 1), (from_right, 1), (from_across, 2)):
+        parts.append(shifted(piece, "tp", by))
+    made = sum(part.astype(jnp.float32) for part in parts).astype(jnp.bfloat16)
+    return made.reshape(by_slot.shape), from_across
 
 
 def shards(
@@ -198,7 +283,7 @@
     picks = []
     for k in range(2):
         place = jnp.sum(named[k].astype(jnp.float32) * ahead[k], axis=1, keepdims=True)
-        slot = chosen_expert_index[:, k : k + 1] * slots + place.astype(jnp.int32)
+        slot = place.astype(jnp.int32) * experts + chosen_expert_index[:, k : k + 1]
         target = lax.broadcasted_iota(jnp.int32, (rows, experts * slots), 1)
         picks.append((slot == target).astype(jnp.bfloat16))
     outgoing = lax.dot_general(
@@ -208,32 +293,26 @@
         preferred_element_type=jnp.float32,
     ).astype(jnp.bfloat16)
 
-    arrived = traded(outgoing.reshape(experts, slots, width), SP)
-    arrived = jnp.transpose(arrived, (1, 0, 2)).reshape(slots * experts, width)
     weights = (expert_gate_matrix[0], expert_up_matrix[0], expert_down_matrix[0])
-    size = lax.axis_size("tp")
-    half = arrived.shape[0] // 2
-    left = shifted(arrived, "tp", 1)
-    right = shifted(arrived, "tp", size - 1)
-    own = expert_part(arrived, *weights)
-    across = [shifted(left[:half], "tp", 1), shifted(right[half:], "tp", size - 1)]
-    left, right, _ = lax.optimization_barrier((left, right, own))
-    from_left = expert_part(left, *weights)
-    parts = [own, shifted(from_left, "tp", size - 1)]
-    right, _ = lax.optimization_barrier((right, from_left))
-    from_right = expert_part(right, *weights)
-    parts.append(shifted(from_right, "tp", 1))
-    across, _ = lax.optimization_barrier((jnp.concatenate(across, axis=0), from_right))
-    from_across = expert_part(across, *weights)
-    parts.append(shifted(from_across, "tp", 2))
-    total_out = sum(part.astype(jnp.float32) for part in parts)
-    expert_out = total_out.astype(jnp.bfloat16).reshape(slots, experts, width)
-    back = traded(jnp.transpose(expert_out, (1, 0, 2)), SP)
-    flat_out = back.reshape(experts * slots, width)
+    early = (slots + 1) // 2
+    by_slot = outgoing.reshape(slots, experts, width)
+    got_a = traded(packed(by_slot[:early], early), SP)
+    got_b = traded(packed(by_slot[early:], early), SP)
+    made_a, last = through_experts(unpacked(got_a, early, width), weights)
+    got_b, _ = lax.optimization_barrier((got_b, last))
+    back_a = traded(packed(made_a, early), SP)
+    made_b, _ = through_experts(unpacked(got_b, slots - early, width), weights)
+    back_b = traded(packed(made_b, early), SP)
 
     out = residual
+    cut = early * experts
+    out_a = unpacked(back_a, early, width).reshape(cut, width)
+    out_b = unpacked(back_b, slots - early, width).reshape(-1, width)
     for k in range(2):
-        picked = jnp.dot(picks[k], flat_out, preferred_element_type=jnp.float32)
+        picked = jnp.dot(picks[k][:, :cut], out_a, preferred_element_type=jnp.float32)
+        out = out + chosen_expert_weight[:, k : k + 1] * picked
+    for k in range(2):
+        picked = jnp.dot(picks[k][:, cut:], out_b, preferred_element_type=jnp.float32)
         out = out + chosen_expert_weight[:, k : k + 1] * picked
     return out.astype(jnp.bfloat16)
 

time: 350 us -> 331 us (0.946)
  blocking collectives: 64.4 us -> 0 us
  starting transfers between devices: 85.4 us -> 125 us
  matrix products: 46.3 us -> 7.54 us
  Pallas kernels: 0 us -> 34.1 us
  local copies, waits for them, and re-layouts: 10.4 us -> 22.6 us
    all_to_all x1 -> x0, blocking collectives: 64.4 us -> none  [traded(): return lax.all_to_all(x, axis, split_axis=0, concat_axis=0, tiled=True)]
    dot_general x10 -> x4, matrix products: 40.4 us -> 1.54 us  [the longest x2 1.11 us: shards(): jnp.dot(picks[k][:, cut:], out_b, preferred_element_type=jnp.float32)]
    all_to_all x4 -> x7, starting transfers between devices: 23.5 us -> 59.1 us  [traded(): return lax.all_to_all(x, axis, split_axis=0, concat_axis=0, tiled=True)]
    pallas_call x0 -> x8, Pallas kernels: none -> 34.1 us  [expert_part(): pl.pallas_call(expert_body, in_specs=[whole] * 4, out_specs=whole, out_sh...]
    unnamed x24 -> x40, local copies, waits for them, and re-layouts: 1.15 us -> 13.4 us
    ppermute x14 -> x21, waiting for transfers between devices: 59.4 us -> 49.9 us  [shifted(): return lax.ppermute(x, axis, [(i, (i + by) % size) for i in range(size)])]
    all_to_all x4 -> x7, waiting for transfers between devices: 68.9 us -> 78.3 us  [traded(): return lax.all_to_all(x, axis, split_axis=0, concat_axis=0, tiled=True)]
    ppermute x14 -> x21, starting transfers between devices: 45.3 us -> 53.1 us  [shifted(): return lax.ppermute(x, axis, [(i, (i + by) % size) for i in range(size)])]
  transfers between devices with their start and end apart: 21 -> 31, of which waited for: 11 -> 10; matrix products, arithmetic and copies ran while one was open for 12% -> 4% of each run, Pallas kernels for 0% -> 10%
where the time goes in v2:
time: 331 us; the launch traced here: 329 us
  waiting for transfers between devices  130 us (39%)
  starting transfers between devices  125 us (38%)
  Pallas kernels  34.1 us (10%)
  local copies, waits for them, and re-layouts  22.6 us (7%)
  other arithmetic  8.86 us (3%)
  matrix products  7.54 us (2%)
    all_to_all x7, waiting for transfers between devices, traded(): return lax.all_to_all(x, axis, split_axis=0, concat_axis=0, tiled=True)  78.3 us
    all_to_all x7, starting transfers between devices, traded(): return lax.all_to_all(x, axis, split_axis=0, concat_axis=0, tiled=True)  59.1 us
    ppermute x21, starting transfers between devices, shifted(): return lax.ppermute(x, axis, [(i, (i + by) % size) for i in range(size)])  53.1 us
    ppermute x21, waiting for transfers between devices, shifted(): return lax.ppermute(x, axis, [(i, (i + by) % size) for i in range(size)])  49.9 us
    pallas_call x8, Pallas kernels, expert_part(): pl.pallas_call(expert_body, in_specs=[whole] * 4, out_specs=whole, out_sh...  34.1 us
    unnamed x40, local copies, waits for them, and re-layouts  13.4 us
    ppermute x3, starting transfers between devices, states_before(): lax.ppermute(whole, 'far', [(i, i + back) for i in range(far - back)])  13 us
  transfers between devices with their start and end apart: 31, of which 10 were waited for; matrix products, arithmetic and copies ran while one was open for 4% of the time, Pallas kernels for 10%

profile of v2, /device:TPU:40, one launch (start us, length us, event | category | flops | bytes accessed | tf_op | source)
XLA Modules:
  0.0 328.9 jit_solution(11746682034399785659)
XLA Ops:
  0.0 0.9 fusion.36
  1.1 0.9 fusion.76
  2.0 0.8 exponential_bitcast_fusion
  3.1 1.0 copy.89
  4.9 0.8 maximum_maximum_fusion
  5.6 8.5 %all-to-all-start = ((f32[8,40,128]{2,1,0:T(8,128)}), f32[8,40,128]{2,1,0:T(8,128)S(1)}, u32[]{:S(2)}, u32[]{:S(2)}) async-start(f32[8,40,128]{2,1,0:T(8,128)} %maximum_maximum_fusion), calls=%async_computation | async-start | bytes 327680 | tf_op jit(solution)/shard_map/all_to_all | solution.py:28
  14.1 10.6 %collective-permute-start.5 = (bf16[64,512]{1,0:T(8,128)(2,1)}, bf16[64,512]{1,0:T(8,128)(2,1)S(1)}, u32[]{:S(2)}, u32[]{:S(2)}) collective-permute-start(bf16[64,512]{1,0:T(8,128)(2,1)} %bitcast.255), channel_id=1, source_target_pairs={{0,32},{32,64},{64,96},{96,0},{1,33},{33,65},{65,97},{97,1},{2,34}... | collective-permute-start | bytes 196616 | tf_op jit(solution)/shard_map/ppermute | solution.py:24
  24.7 13.2 %collective-permute-start.4 = (bf16[64,512]{1,0:T(8,128)(2,1)}, bf16[64,512]{1,0:T(8,128)(2,1)S(1)}, u32[]{:S(2)}, u32[]{:S(2)}) collective-permute-start(bf16[64,512]{1,0:T(8,128)(2,1)} %bitcast.256), channel_id=1, source_target_pairs={{0,64},{32,96},{64,0},{96,32},{1,65},{33,97},{65,1},{97,33},{2,66}... | collective-permute-start | bytes 196616 | tf_op jit(solution)/shard_map/ppermute | solution.py:24
  38.1 0.6 slice_reduce_fusion.2
  39.0 0.6 slice.186
  39.7 0.6 pad.58.clone
  40.4 0.7 pad.57.clone
  41.2 7.8 %collective-permute-start.2 = (f32[40,128]{1,0:T(8,128)S(1)}, f32[40,128]{1,0:T(8,128)S(1)}, u32[]{:S(2)}, u32[]{:S(2)}) collective-permute-start(f32[40,128]{1,0:T(8,128)S(1)} %maximum_bitcast_fusion.10), channel_id=1, source_target_pairs={{0,32},{32,64},{64,96},{1,33},{33,65},{65,97},{2,34},{34,66},{66,9... | collective-permute-start | bytes 61448 | tf_op jit(solution)/shard_map/ppermute | solution.py:67
  49.2 3.1 collective-permute-start.1
  52.4 2.1 collective-permute-start
  54.5 1.4 collective-permute-done
  56.8 0.8 maximum_maximum_fusion.1
  57.6 4.9 %all-to-all-start.1 = ((f32[8,40,128]{2,1,0:T(8,128)}), f32[8,40,128]{2,1,0:T(8,128)S(1)}, u32[]{:S(2)}, u32[]{:S(2)}) async-start(f32[8,40,128]{2,1,0:T(8,128)} %maximum_maximum_fusion.1), calls=%async_computation.1 | async-start | bytes 327680 | tf_op jit(solution)/shard_map/all_to_all | solution.py:28
  62.6 6.9 %collective-permute-start.8 = (bf16[4,64,512]{2,1,0:T(8,128)(2,1)S(1)}, bf16[4,64,512]{2,1,0:T(8,128)(2,1)S(1)}, u32[]{:S(2)}, u32[]{:S(2)}) collective-permute-start(bf16[4,64,512]{2,1,0:T(8,128)(2,1)S(1)} %get-tuple-element.47), channel_id=1, source_target_pairs={{0,112},{8,120},{16,0},{24,8},{32,16},{40,24},{48,32},{56,40},{64,... | collective-permute-start | bytes 786440 | tf_op jit(solution)/shard_map/ppermute | solution.py:24
  70.0 1.5 collective-permute-start.6
  72.1 0.6 bitcast_convert_fusion
  72.7 9.2 %collective-permute-done.8 = bf16[4,64,512]{2,1,0:T(8,128)(2,1)S(1)} collective-permute-done((bf16[4,64,512]{2,1,0:T(8,128)(2,1)S(1)}, bf16[4,64,512]{2,1,0:T(8,128)(2,1)S(1)}, u32[]{:S(2)}, u32[]{:S(2)}) %collective-permute-start.8) | collective-permute-done | bytes 262176 | tf_op jit(solution)/shard_map/ppermute | solution.py:24
  81.9 5.2 %collective-permute-done.7 = bf16[4,64,512]{2,1,0:T(8,128)(2,1)S(1)} collective-permute-done((bf16[4,64,512]{2,1,0:T(8,128)(2,1)S(1)}, bf16[4,64,512]{2,1,0:T(8,128)(2,1)S(1)}, u32[]{:S(2)}, u32[]{:S(2)}) %collective-permute-start.7) | collective-permute-done | bytes 262176 | tf_op jit(solution)/shard_map/ppermute | solution.py:24
  88.1 1.6 multiply_reduce_fusion.2
  90.7 0.8 fusion.5
  91.5 1.8 convolution_convert_fusion
  93.3 4.7 %all-to-all-start.2 = ((bf16[4,56,2048]{2,1,0:T(8,128)(2,1)}), bf16[4,56,2048]{2,1,0:T(8,128)(2,1)S(1)}, u32[]{:S(2)}, u32[]{:S(2)}) async-start(bf16[4,56,2048]{2,1,0:T(8,128)(2,1)} %bitcast.36), calls=%async_computation.2 | async-start | bytes 1835008 | tf_op jit(solution)/shard_map/all_to_all | solution.py:28
  98.4 13.6 %all-to-all-done.2 = bf16[4,56,2048]{2,1,0:T(8,128)(2,1)S(1)} async-done(((bf16[4,56,2048]{2,1,0:T(8,128)(2,1)}), bf16[4,56,2048]{2,1,0:T(8,128)(2,1)S(1)}, u32[]{:S(2)}, u32[]{:S(2)}) %all-to-all-start.2) | async-done | bytes 917536 | tf_op jit(solution)/shard_map/all_to_all | solution.py:28
  113.0 1.2 copy.129
  114.2 9.9 %all-to-all-start.3 = ((bf16[32,4,2048]{2,1,0:T(4,128)(2,1)}), bf16[32,4,2048]{2,1,0:T(4,128)(2,1)S(1)}, u32[]{:S(2)}, u32[]{:S(2)}) async-start(bf16[32,4,2048]{2,1,0:T(4,128)(2,1)} %bitcast.197), calls=%async_computation.3 | async-start | bytes 1048576 | tf_op jit(solution)/shard_map/all_to_all | solution.py:28
  124.2 1.1 copy.104
  125.3 31.9 %all-to-all-done.3 = bf16[32,4,2048]{2,1,0:T(4,128)(2,1)S(1)} async-done(((bf16[32,4,2048]{2,1,0:T(4,128)(2,1)}), bf16[32,4,2048]{2,1,0:T(4,128)(2,1)S(1)}, u32[]{:S(2)}, u32[]{:S(2)}) %all-to-all-start.3) | async-done | bytes 524320 | tf_op jit(solution)/shard_map/all_to_all | solution.py:28
  157.2 4.8 %all-to-all-start.5 = ((bf16[32,4,1536]{2,1,0:T(4,128)(2,1)}), bf16[32,4,1536]{2,1,0:T(4,128)(2,1)S(1)}, u32[]{:S(2)}, u32[]{:S(2)}) async-start(bf16[32,4,1536]{2,1,0:T(4,128)(2,1)} %copy.104), calls=%async_computation.5 | async-start | bytes 786432 | tf_op jit(solution)/shard_map/all_to_all | solution.py:28
  162.3 1.3 collective-permute-start.11
  163.6 0.9 collective-permute-start.10
  164.4 2.0 copy-done.1
  166.5 2.0 copy-done.4
  168.5 2.0 copy-done.6
  170.5 4.3 %expert_part.8 = bf16[128,2048]{1,0:T(8,128)(2,1)S(1)} custom-call(bf16[128,2048]{1,0:T(8,128)(2,1)S(1)} %bitcast.226, bf16[2048,896]{1,0:T(8,128)(2,1)S(1)} %bitcast.200, bf16[2048,896]{1,0:T(8,128)(2,1)S(1)} %bitcast.208, bf16[896,2048]{1,0:T(8,128)(2,1)S(1)} %bitcast.216), custom_call_target="tpu_custom_call" | custom-call | flops 1409286144 | bytes 12058624 | tf_op jit(solution)/shard_map/expert_part/pallas_call | solution.py:130
  174.9 0.8 collective-permute-done.11.rows_ref
  175.7 2.5 collective-permute-start.15
  178.4 4.3 %expert_part.9 = bf16[128,2048]{1,0:T(8,128)(2,1)S(1)} custom-call(bf16[128,2048]{1,0:T(8,128)(2,1)S(1)} %collective-permute-done.10.rows_ref, bf16[2048,896]{1,0:T(8,128)(2,1)S(1)} %bitcast.201, bf16[2048,896]{1,0:T(8,128)(2,1)S(1)} %bitcast.209, bf16[896,2048]{1,0:T(8,128)(2,1)S(1)} %bitcast.217), custom_call_target="tpu_custom_call" | custom-call | flops 1409286144 | bytes 12058624 | tf_op jit(solution)/shard_map/expert_part/pallas_call | solution.py:130
  182.7 4.3 %expert_part.10 = bf16[128,2048]{1,0:T(8,128)(2,1)S(1)} custom-call(bf16[128,2048]{1,0:T(8,128)(2,1)S(1)} %collective-permute-done.11.rows_ref, bf16[2048,896]{1,0:T(8,128)(2,1)S(1)} %bitcast.202, bf16[2048,896]{1,0:T(8,128)(2,1)S(1)} %bitcast.210, bf16[896,2048]{1,0:T(8,128)(2,1)S(1)} %bitcast.218), custom_call_target="tpu_custom_call" | custom-call | flops 1409286144 | bytes 12058624 | tf_op jit(solution)/shard_map/expert_part/pallas_call | solution.py:130
  187.1 4.3 %expert_part.11 = bf16[128,2048]{1,0:T(8,128)(2,1)S(1)} custom-call(bf16[128,2048]{1,0:T(8,128)(2,1)S(1)} %pad_maximum_fusion.2.rows_ref, bf16[2048,896]{1,0:T(8,128)(2,1)S(1)} %bitcast.203, bf16[2048,896]{1,0:T(8,128)(2,1)S(1)} %bitcast.211, bf16[896,2048]{1,0:T(8,128)(2,1)S(1)} %bitcast.219), custom_call_target="tpu_custom_call" | custom-call | flops 1409286144 | bytes 12058624 | tf_op jit(solution)/shard_map/expert_part/pallas_call | solution.py:130
  191.7 3.3 %collective-permute-start.18 = (bf16[96,2048]{1,0:T(8,128)(2,1)S(1)}, bf16[96,2048]{1,0:T(8,128)(2,1)S(1)}, u32[]{:S(2)}, u32[]{:S(2)}) collective-permute-start(bf16[96,2048]{1,0:T(8,128)(2,1)S(1)} %bitcast.227), channel_id=1, source_target_pairs={{0,3},{1,0},{2,1},{3,2},{4,7},{5,4},{6,5},{7,6},{8,11},{9,8},{10,9... | collective-permute-start | bytes 1179656 | tf_op jit(solution)/shard_map/ppermute | solution.py:24
  195.0 2.0 copy-done.3
  197.1 2.0 copy-done.5
  199.1 2.0 copy-done.7
  201.1 4.2 %expert_part.12 = bf16[96,2048]{1,0:T(8,128)(2,1)S(1)} custom-call(bf16[96,2048]{1,0:T(8,128)(2,1)S(1)} %bitcast.229, bf16[2048,896]{1,0:T(8,128)(2,1)S(1)} %bitcast.204, bf16[2048,896]{1,0:T(8,128)(2,1)S(1)} %bitcast.212, bf16[896,2048]{1,0:T(8,128)(2,1)S(1)} %bitcast.220), custom_call_target="tpu_custom_call" | custom-call | flops 1056964608 | bytes 11796480 | tf_op jit(solution)/shard_map/expert_part/pallas_call | solution.py:130
  205.4 3.3 %collective-permute-start.22 = (bf16[48,2048]{1,0:T(8,128)(2,1)S(1)}, bf16[48,2048]{1,0:T(8,128)(2,1)S(1)}, u32[]{:S(2)}, u32[]{:S(2)}) collective-permute-start(bf16[48,2048]{1,0:T(8,128)(2,1)S(1)} %slice.259), channel_id=1, source_target_pairs={{0,3},{1,0},{2,1},{3,2},{4,7},{5,4},{6,5},{7,6},{8,11},{9,8},{10,9... | collective-permute-start | bytes 589832 | tf_op jit(solution)/shard_map/ppermute | solution.py:24
  209.1 4.2 %expert_part.13 = bf16[96,2048]{1,0:T(8,128)(2,1)S(1)} custom-call(bf16[96,2048]{1,0:T(8,128)(2,1)S(1)} %collective-permute-done.17.rows_ref, bf16[2048,896]{1,0:T(8,128)(2,1)S(1)} %bitcast.205, bf16[2048,896]{1,0:T(8,128)(2,1)S(1)} %bitcast.213, bf16[896,2048]{1,0:T(8,128)(2,1)S(1)} %bitcast.221), custom_call_target="tpu_custom_call" | custom-call | flops 1056964608 | bytes 11796480 | tf_op jit(solution)/shard_map/expert_part/pallas_call | solution.py:130
  213.3 3.3 %collective-permute-start.19 = (bf16[96,2048]{1,0:T(8,128)(2,1)S(1)}, bf16[96,2048]{1,0:T(8,128)(2,1)S(1)}, u32[]{:S(2)}, u32[]{:S(2)}) collective-permute-start(bf16[96,2048]{1,0:T(8,128)(2,1)S(1)} %expert_part.13), channel_id=1, source_target_pairs={{0,3},{1,0},{2,1},{3,2},{4,7},{5,4},{6,5},{7,6},{8,11},{9,8},{10,9... | collective-permute-start | bytes 1179656 | tf_op jit(solution)/shard_map/ppermute | solution.py:24
  216.7 4.2 %expert_part.14 = bf16[96,2048]{1,0:T(8,128)(2,1)S(1)} custom-call(bf16[96,2048]{1,0:T(8,128)(2,1)S(1)} %collective-permute-done.18.rows_ref, bf16[2048,896]{1,0:T(8,128)(2,1)S(1)} %bitcast.206, bf16[2048,896]{1,0:T(8,128)(2,1)S(1)} %bitcast.214, bf16[896,2048]{1,0:T(8,128)(2,1)S(1)} %bitcast.222), custom_call_target="tpu_custom_call" | custom-call | flops 1056964608 | bytes 11796480 | tf_op jit(solution)/shard_map/expert_part/pallas_call | solution.py:130
  221.1 4.2 %expert_part.15 = bf16[96,2048]{1,0:T(8,128)(2,1)S(1)} custom-call(bf16[96,2048]{1,0:T(8,128)(2,1)S(1)} %pad_maximum_fusion.4.rows_ref, bf16[2048,896]{1,0:T(8,128)(2,1)S(1)} %bitcast.207, bf16[2048,896]{1,0:T(8,128)(2,1)S(1)} %bitcast.215, bf16[896,2048]{1,0:T(8,128)(2,1)S(1)} %bitcast.223), custom_call_target="tpu_custom_call" | custom-call | flops 1056964608 | bytes 11796480 | tf_op jit(solution)/shard_map/expert_part/pallas_call | solution.py:130
  225.3 1.6 collective-permute-start.23
  226.9 11.5 %collective-permute-done.20 = bf16[96,2048]{1,0:T(8,128)(2,1)S(1)} collective-permute-done((bf16[96,2048]{1,0:T(8,128)(2,1)S(1)}, bf16[96,2048]{1,0:T(8,128)(2,1)S(1)}, u32[]{:S(2)}, u32[]{:S(2)}) %collective-permute-start.20) | collective-permute-done | bytes 393248 | tf_op jit(solution)/shard_map/ppermute | solution.py:24
  238.8 1.1 copy.106
  239.8 13.6 %all-to-all-start.6 = ((bf16[32,4,1536]{2,1,0:T(4,128)(2,1)}), bf16[32,4,1536]{2,1,0:T(4,128)(2,1)S(1)}, u32[]{:S(2)}, u32[]{:S(2)}) async-start(bf16[32,4,1536]{2,1,0:T(4,128)(2,1)} %copy.106), calls=%async_computation.6 | async-start | bytes 786432 | tf_op jit(solution)/shard_map/all_to_all | solution.py:28
  253.6 3.2 collective-permute-start.12
  256.9 22.7 %collective-permute-done.13 = bf16[128,2048]{1,0:T(8,128)(2,1)S(1)} collective-permute-done((bf16[128,2048]{1,0:T(8,128)(2,1)S(1)}, bf16[128,2048]{1,0:T(8,128)(2,1)S(1)}, u32[]{:S(2)}, u32[]{:S(2)}) %collective-permute-start.13) | collective-permute-done | bytes 524320 | tf_op jit(solution)/shard_map/ppermute | solution.py:24
  280.0 1.2 copy.128
  281.2 12.7 %all-to-all-start.4 = ((bf16[32,4,2048]{2,1,0:T(4,128)(2,1)}), bf16[32,4,2048]{2,1,0:T(4,128)(2,1)S(1)}, u32[]{:S(2)}, u32[]{:S(2)}) async-start(bf16[32,4,2048]{2,1,0:T(4,128)(2,1)} %bitcast.196), calls=%async_computation.4 | async-start | bytes 1048576 | tf_op jit(solution)/shard_map/all_to_all | solution.py:28
  294.3 32.8 %all-to-all-done.4 = bf16[32,4,2048]{2,1,0:T(4,128)(2,1)S(1)} async-done(((bf16[32,4,2048]{2,1,0:T(4,128)(2,1)}), bf16[32,4,2048]{2,1,0:T(4,128)(2,1)S(1)}, u32[]{:S(2)}, u32[]{:S(2)}) %all-to-all-start.4) | async-done | bytes 524320 | tf_op jit(solution)/shard_map/all_to_all | solution.py:28
  328.0 0.9 fusion.4
  (161 shorter events, 10.8 us)
Async XLA Ops:
  0.0 4.2 %copy-start = (bf16[224,512]{1,0:T(8,128)(2,1)S(1)}, bf16[224,512]{1,0:T(8,128)(2,1)}, u32[]{:S(2)}) copy-start(bf16[224,512]{1,0:T(8,128)(2,1)} %param.17) | copy-start | bytes 688132
  0.0 62.5 %copy-start.12 = (bf16[512,64]{0,1:T(8,128)(2,1)S(1)}, bf16[512,64]{0,1:T(8,128)(2,1)}, u32[]{:S(2)}) copy-start(bf16[512,64]{0,1:T(8,128)(2,1)} %param.22) | copy-start | bytes 196612
  3.1 68.4 %copy-start.13 = (f32[4,224]{1,0:T(4,128)S(1)}, f32[4,224]{1,0:T(4,128)}, u32[]{:S(2)}) copy-start(f32[4,224]{1,0:T(4,128)} %param.18) | copy-start | bytes 10756
  4.1 1.5 copy-start.10
  4.1 67.8 %copy-start.15 = (bf16[2048]{0:T(1024)(128)(2,1)S(1)}, bf16[2048]{0:T(1024)(128)(2,1)}, u32[]{:S(2)}) copy-start(bf16[2048]{0:T(1024)(128)(2,1)} %param.24) | copy-start | bytes 12292
  4.1 67.8 %copy-start.11 = (bf16[224,256]{1,0:T(8,128)(2,1)S(1)}, bf16[224,256]{1,0:T(8,128)(2,1)}, u32[]{:S(2)}) copy-start(bf16[224,256]{1,0:T(8,128)(2,1)} %param.15) | copy-start | bytes 344068
  4.2 67.8 %copy-start.17 = (bf16[512]{0:T(512)(128)(2,1)S(1)}, bf16[512]{0:T(512)(128)(2,1)}, u32[]{:S(2)}) copy-start(bf16[512]{0:T(512)(128)(2,1)} %param.21) | copy-start | bytes 3076
  5.6 32.5 %all-to-all-start = ((f32[8,40,128]{2,1,0:T(8,128)}), f32[8,40,128]{2,1,0:T(8,128)S(1)}, u32[]{:S(2)}, u32[]{:S(2)}) async-start(f32[8,40,128]{2,1,0:T(8,128)} %maximum_maximum_fusion), calls=%async_computation | async-start | bytes 327680 | tf_op jit(solution)/shard_map/all_to_all | solution.py:28
  14.1 48.4 %collective-permute-start.5 = (bf16[64,512]{1,0:T(8,128)(2,1)}, bf16[64,512]{1,0:T(8,128)(2,1)S(1)}, u32[]{:S(2)}, u32[]{:S(2)}) collective-permute-start(bf16[64,512]{1,0:T(8,128)(2,1)} %bitcast.255), channel_id=1, source_target_pairs={{0,32},{32,64},{64,96},{96,0},{1,33},{33,65},{65,97},{97,1},{2,34}... | collective-permute-start | bytes 196616 | tf_op jit(solution)/shard_map/ppermute | solution.py:24
  24.7 37.8 %collective-permute-start.4 = (bf16[64,512]{1,0:T(8,128)(2,1)}, bf16[64,512]{1,0:T(8,128)(2,1)S(1)}, u32[]{:S(2)}, u32[]{:S(2)}) collective-permute-start(bf16[64,512]{1,0:T(8,128)(2,1)} %bitcast.256), channel_id=1, source_target_pairs={{0,64},{32,96},{64,0},{96,32},{1,65},{33,97},{65,1},{97,33},{2,66}... | collective-permute-start | bytes 196616 | tf_op jit(solution)/shard_map/ppermute | solution.py:24
  37.9 24.6 %collective-permute-start.3 = (bf16[64,512]{1,0:T(8,128)(2,1)}, bf16[64,512]{1,0:T(8,128)(2,1)S(1)}, u32[]{:S(2)}, u32[]{:S(2)}) collective-permute-start(bf16[64,512]{1,0:T(8,128)(2,1)} %bitcast.257), channel_id=1, source_target_pairs={{0,96},{32,0},{64,32},{96,64},{1,97},{33,1},{65,33},{97,65},{2,98}... | collective-permute-start | bytes 196616 | tf_op jit(solution)/shard_map/ppermute | solution.py:24
  38.1 33.9 %copy-start.9 = (pred[224,224]{1,0:T(8,128)(4,1)}, pred[224,224]{1,0:T(8,128)(4,1)S(1)}, u32[]{:S(2)}) copy-start(pred[224,224]{1,0:T(8,128)(4,1)S(1)} %iota_compare_fusion.1) | copy-start | bytes 150532
  41.2 11.1 %collective-permute-start.2 = (f32[40,128]{1,0:T(8,128)S(1)}, f32[40,128]{1,0:T(8,128)S(1)}, u32[]{:S(2)}, u32[]{:S(2)}) collective-permute-start(f32[40,128]{1,0:T(8,128)S(1)} %maximum_bitcast_fusion.10), channel_id=1, source_target_pairs={{0,32},{32,64},{64,96},{1,33},{33,65},{65,97},{2,34},{34,66},{66,9... | collective-permute-start | bytes 61448 | tf_op jit(solution)/shard_map/ppermute | solution.py:67
  49.2 5.3 %collective-permute-start.1 = (f32[40,128]{1,0:T(8,128)S(1)}, f32[40,128]{1,0:T(8,128)S(1)}, u32[]{:S(2)}, u32[]{:S(2)}) collective-permute-start(f32[40,128]{1,0:T(8,128)S(1)} %maximum_bitcast_fusion.10), channel_id=1, source_target_pairs={{0,64},{32,96},{1,65},{33,97},{2,66},{34,98},{3,67},{35,99},{4,68}... | collective-permute-start | bytes 61448 | tf_op jit(solution)/shard_map/ppermute | solution.py:67
  52.4 3.6 %collective-permute-start = (f32[40,128]{1,0:T(8,128)S(1)}, f32[40,128]{1,0:T(8,128)S(1)}, u32[]{:S(2)}, u32[]{:S(2)}) collective-permute-start(f32[40,128]{1,0:T(8,128)S(1)} %maximum_bitcast_fusion.10), channel_id=1, source_target_pairs={{0,96},{1,97},{2,98},{3,99},{4,100},{5,101},{6,102},{7,103},{8,104... | collective-permute-start | bytes 61448 | tf_op jit(solution)/shard_map/ppermute | solution.py:67
  57.6 29.8 %all-to-all-start.1 = ((f32[8,40,128]{2,1,0:T(8,128)}), f32[8,40,128]{2,1,0:T(8,128)S(1)}, u32[]{:S(2)}, u32[]{:S(2)}) async-start(f32[8,40,128]{2,1,0:T(8,128)} %maximum_maximum_fusion.1), calls=%async_computation.1 | async-start | bytes 327680 | tf_op jit(solution)/shard_map/all_to_all | solution.py:28
  62.6 19.3 %collective-permute-start.8 = (bf16[4,64,512]{2,1,0:T(8,128)(2,1)S(1)}, bf16[4,64,512]{2,1,0:T(8,128)(2,1)S(1)}, u32[]{:S(2)}, u32[]{:S(2)}) collective-permute-start(bf16[4,64,512]{2,1,0:T(8,128)(2,1)S(1)} %get-tuple-element.47), channel_id=1, source_target_pairs={{0,112},{8,120},{16,0},{24,8},{32,16},{40,24},{48,32},{56,40},{64,... | collective-permute-start | bytes 786440 | tf_op jit(solution)/shard_map/ppermute | solution.py:24
  69.5 17.6 %collective-permute-start.7 = (bf16[4,64,512]{2,1,0:T(8,128)(2,1)S(1)}, bf16[4,64,512]{2,1,0:T(8,128)(2,1)S(1)}, u32[]{:S(2)}, u32[]{:S(2)}) collective-permute-start(bf16[4,64,512]{2,1,0:T(8,128)(2,1)S(1)} %get-tuple-element.47), channel_id=1, source_target_pairs={{0,120},{8,0},{16,8},{24,16},{32,24},{40,32},{48,40},{56,48},{64,5... | collective-permute-start | bytes 786440 | tf_op jit(solution)/shard_map/ppermute | solution.py:24
  70.0 17.1 %collective-permute-start.6 = (bf16[4,64,512]{2,1,0:T(8,128)(2,1)S(1)}, bf16[4,64,512]{2,1,0:T(8,128)(2,1)S(1)}, u32[]{:S(2)}, u32[]{:S(2)}) collective-permute-start(bf16[4,64,512]{2,1,0:T(8,128)(2,1)S(1)} %get-tuple-element.47), channel_id=1, source_target_pairs={{0,8},{8,16},{16,24},{24,32},{32,40},{40,48},{48,56},{56,64},{64,7... | collective-permute-start | bytes 786440 | tf_op jit(solution)/shard_map/ppermute | solution.py:24
  87.3 2.8 collective-permute-start.9
  90.7 0.8 copy-start.14
  91.5 6.5 %copy-start.16 = (s32[56,2]{0,1:T(2,128)S(1)}, s32[56,2]{0,1:T(2,128)}, u32[]{:S(2)}) copy-start(s32[56,2]{0,1:T(2,128)} %param.25) | copy-start | bytes 1348
  93.3 18.9 %copy-start.8 = (bf16[56,2048]{1,0:T(8,128)(2,1)S(1)}, bf16[56,2048]{1,0:T(8,128)(2,1)}, u32[]{:S(2)}) copy-start(bf16[56,2048]{1,0:T(8,128)(2,1)} %param.23) | copy-start | bytes 688132
  93.3 18.8 %all-to-all-start.2 = ((bf16[4,56,2048]{2,1,0:T(8,128)(2,1)}), bf16[4,56,2048]{2,1,0:T(8,128)(2,1)S(1)}, u32[]{:S(2)}, u32[]{:S(2)}) async-start(bf16[4,56,2048]{2,1,0:T(8,128)(2,1)} %bitcast.36), calls=%async_computation.2 | async-start | bytes 1835008 | tf_op jit(solution)/shard_map/all_to_all | solution.py:28
  114.2 43.0 %all-to-all-start.3 = ((bf16[32,4,2048]{2,1,0:T(4,128)(2,1)}), bf16[32,4,2048]{2,1,0:T(4,128)(2,1)S(1)}, u32[]{:S(2)}, u32[]{:S(2)}) async-start(bf16[32,4,2048]{2,1,0:T(4,128)(2,1)} %bitcast.197), calls=%async_computation.3 | async-start | bytes 1048576 | tf_op jit(solution)/shard_map/all_to_all | solution.py:28
  157.2 34.3 %all-to-all-start.5 = ((bf16[32,4,1536]{2,1,0:T(4,128)(2,1)}), bf16[32,4,1536]{2,1,0:T(4,128)(2,1)S(1)}, u32[]{:S(2)}, u32[]{:S(2)}) async-start(bf16[32,4,1536]{2,1,0:T(4,128)(2,1)} %copy.104), calls=%async_computation.5 | async-start | bytes 786432 | tf_op jit(solution)/shard_map/all_to_all | solution.py:28
  162.3 13.4 %collective-permute-start.11 = (bf16[128,2048]{1,0:T(8,128)(2,1)S(1)}, bf16[128,2048]{1,0:T(8,128)(2,1)S(1)}, u32[]{:S(2)}, u32[]{:S(2)}) collective-permute-start(bf16[128,2048]{1,0:T(8,128)(2,1)S(1)} %bitcast.224), channel_id=1, source_target_pairs={{0,3},{1,0},{2,1},{3,2},{4,7},{5,4},{6,5},{7,6},{8,11},{9,8},{10,9... | collective-permute-start | bytes 1572872 | tf_op jit(solution)/shard_map/ppermute | solution.py:24
  163.6 14.7 %collective-permute-start.10 = (bf16[128,2048]{1,0:T(8,128)(2,1)S(1)}, bf16[128,2048]{1,0:T(8,128)(2,1)S(1)}, u32[]{:S(2)}, u32[]{:S(2)}) collective-permute-start(bf16[128,2048]{1,0:T(8,128)(2,1)S(1)} %bitcast.225), channel_id=1, source_target_pairs={{0,1},{1,2},{2,3},{3,0},{4,5},{5,6},{6,7},{7,4},{8,9},{9,10},{10,1... | collective-permute-start | bytes 1572872 | tf_op jit(solution)/shard_map/ppermute | solution.py:24
  164.4 2.0 copy-start.1
  166.4 2.0 copy-start.4
  168.5 2.0 copy-start.6
  175.7 11.3 %collective-permute-start.15 = (bf16[64,2048]{1,0:T(8,128)(2,1)S(1)}, bf16[64,2048]{1,0:T(8,128)(2,1)S(1)}, u32[]{:S(2)}, u32[]{:S(2)}) collective-permute-start(bf16[64,2048]{1,0:T(8,128)(2,1)S(1)} %slice.243), channel_id=1, source_target_pairs={{0,3},{1,0},{2,1},{3,2},{4,7},{5,4},{6,5},{7,6},{8,11},{9,8},{10,9... | collective-permute-start | bytes 786440 | tf_op jit(solution)/shard_map/ppermute | solution.py:24
  178.2 8.8 %collective-permute-start.14 = (bf16[64,2048]{1,0:T(8,128)(2,1)S(1)}, bf16[64,2048]{1,0:T(8,128)(2,1)S(1)}, u32[]{:S(2)}, u32[]{:S(2)}) collective-permute-start(bf16[64,2048]{1,0:T(8,128)(2,1)S(1)} %slice.242), channel_id=1, source_target_pairs={{0,1},{1,2},{2,3},{3,0},{4,5},{5,6},{6,7},{7,4},{8,9},{9,10},{10,1... | collective-permute-start | bytes 786440 | tf_op jit(solution)/shard_map/ppermute | solution.py:24
  182.7 4.4 %copy-start.2 = (bf16[1,2048,896]{2,1,0:T(8,128)(2,1)S(1)}, bf16[1,2048,896]{2,1,0:T(8,128)(2,1)}, u32[]{:S(2)}) copy-start(bf16[1,2048,896]{2,1,0:T(8,128)(2,1)} %param.27) | copy-start | bytes 11010052
  191.7 13.7 %collective-permute-start.18 = (bf16[96,2048]{1,0:T(8,128)(2,1)S(1)}, bf16[96,2048]{1,0:T(8,128)(2,1)S(1)}, u32[]{:S(2)}, u32[]{:S(2)}) collective-permute-start(bf16[96,2048]{1,0:T(8,128)(2,1)S(1)} %bitcast.227), channel_id=1, source_target_pairs={{0,3},{1,0},{2,1},{3,2},{4,7},{5,4},{6,5},{7,6},{8,11},{9,8},{10,9... | collective-permute-start | bytes 1179656 | tf_op jit(solution)/shard_map/ppermute | solution.py:24
  195.0 13.7 %collective-permute-start.17 = (bf16[96,2048]{1,0:T(8,128)(2,1)S(1)}, bf16[96,2048]{1,0:T(8,128)(2,1)S(1)}, u32[]{:S(2)}, u32[]{:S(2)}) collective-permute-start(bf16[96,2048]{1,0:T(8,128)(2,1)S(1)} %bitcast.228), channel_id=1, source_target_pairs={{0,1},{1,2},{2,3},{3,0},{4,5},{5,6},{6,7},{7,4},{8,9},{9,10},{10,1... | collective-permute-start | bytes 1179656 | tf_op jit(solution)/shard_map/ppermute | solution.py:24
  195.0 2.0 copy-start.3
  197.1 2.0 copy-start.5
  199.1 2.0 copy-start.7
  205.4 15.6 %collective-permute-start.22 = (bf16[48,2048]{1,0:T(8,128)(2,1)S(1)}, bf16[48,2048]{1,0:T(8,128)(2,1)S(1)}, u32[]{:S(2)}, u32[]{:S(2)}) collective-permute-start(bf16[48,2048]{1,0:T(8,128)(2,1)S(1)} %slice.259), channel_id=1, source_target_pairs={{0,3},{1,0},{2,1},{3,2},{4,7},{5,4},{6,5},{7,6},{8,11},{9,8},{10,9... | collective-permute-start | bytes 589832 | tf_op jit(solution)/shard_map/ppermute | solution.py:24
  208.8 12.3 %collective-permute-start.21 = (bf16[48,2048]{1,0:T(8,128)(2,1)S(1)}, bf16[48,2048]{1,0:T(8,128)(2,1)S(1)}, u32[]{:S(2)}, u32[]{:S(2)}) collective-permute-start(bf16[48,2048]{1,0:T(8,128)(2,1)S(1)} %slice.258), channel_id=1, source_target_pairs={{0,1},{1,2},{2,3},{3,0},{4,5},{5,6},{6,7},{7,4},{8,9},{9,10},{10,1... | collective-permute-start | bytes 589832 | tf_op jit(solution)/shard_map/ppermute | solution.py:24
  213.3 25.1 %collective-permute-start.19 = (bf16[96,2048]{1,0:T(8,128)(2,1)S(1)}, bf16[96,2048]{1,0:T(8,128)(2,1)S(1)}, u32[]{:S(2)}, u32[]{:S(2)}) collective-permute-start(bf16[96,2048]{1,0:T(8,128)(2,1)S(1)} %expert_part.13), channel_id=1, source_target_pairs={{0,3},{1,0},{2,1},{3,2},{4,7},{5,4},{6,5},{7,6},{8,11},{9,8},{10,9... | collective-permute-start | bytes 1179656 | tf_op jit(solution)/shard_map/ppermute | solution.py:24
  220.9 17.5 %collective-permute-start.20 = (bf16[96,2048]{1,0:T(8,128)(2,1)S(1)}, bf16[96,2048]{1,0:T(8,128)(2,1)S(1)}, u32[]{:S(2)}, u32[]{:S(2)}) collective-permute-start(bf16[96,2048]{1,0:T(8,128)(2,1)S(1)} %expert_part.14), channel_id=1, source_target_pairs={{0,1},{1,2},{2,3},{3,0},{4,5},{5,6},{6,7},{7,4},{8,9},{9,10},{10,1... | collective-permute-start | bytes 1179656 | tf_op jit(solution)/shard_map/ppermute | solution.py:24
  225.3 13.1 %collective-permute-start.23 = (bf16[96,2048]{1,0:T(8,128)(2,1)S(1)}, bf16[96,2048]{1,0:T(8,128)(2,1)S(1)}, u32[]{:S(2)}, u32[]{:S(2)}) collective-permute-start(bf16[96,2048]{1,0:T(8,128)(2,1)S(1)} %expert_part.15), channel_id=1, source_target_pairs={{0,2},{1,3},{2,0},{3,1},{4,6},{5,7},{6,4},{7,5},{8,10},{9,11},{10,... | collective-permute-start | bytes 1179656 | tf_op jit(solution)/shard_map/ppermute | solution.py:24
  239.8 41.4 %all-to-all-start.6 = ((bf16[32,4,1536]{2,1,0:T(4,128)(2,1)}), bf16[32,4,1536]{2,1,0:T(4,128)(2,1)S(1)}, u32[]{:S(2)}, u32[]{:S(2)}) async-start(bf16[32,4,1536]{2,1,0:T(4,128)(2,1)} %copy.106), calls=%async_computation.6 | async-start | bytes 786432 | tf_op jit(solution)/shard_map/all_to_all | solution.py:28
  253.4 26.2 %collective-permute-start.13 = (bf16[128,2048]{1,0:T(8,128)(2,1)S(1)}, bf16[128,2048]{1,0:T(8,128)(2,1)S(1)}, u32[]{:S(2)}, u32[]{:S(2)}) collective-permute-start(bf16[128,2048]{1,0:T(8,128)(2,1)S(1)} %expert_part.10), channel_id=1, source_target_pairs={{0,1},{1,2},{2,3},{3,0},{4,5},{5,6},{6,7},{7,4},{8,9},{9,10},{10,1... | collective-permute-start | bytes 1572872 | tf_op jit(solution)/shard_map/ppermute | solution.py:24
  253.6 26.1 %collective-permute-start.12 = (bf16[128,2048]{1,0:T(8,128)(2,1)S(1)}, bf16[128,2048]{1,0:T(8,128)(2,1)S(1)}, u32[]{:S(2)}, u32[]{:S(2)}) collective-permute-start(bf16[128,2048]{1,0:T(8,128)(2,1)S(1)} %expert_part.9), channel_id=1, source_target_pairs={{0,3},{1,0},{2,1},{3,2},{4,7},{5,4},{6,5},{7,6},{8,11},{9,8},{10,9... | collective-permute-start | bytes 1572872 | tf_op jit(solution)/shard_map/ppermute | solution.py:24
  256.8 22.9 %collective-permute-start.16 = (bf16[128,2048]{1,0:T(8,128)(2,1)S(1)}, bf16[128,2048]{1,0:T(8,128)(2,1)S(1)}, u32[]{:S(2)}, u32[]{:S(2)}) collective-permute-start(bf16[128,2048]{1,0:T(8,128)(2,1)S(1)} %expert_part.11), channel_id=1, source_target_pairs={{0,2},{1,3},{2,0},{3,1},{4,6},{5,7},{6,4},{7,5},{8,10},{9,11},{10,... | collective-permute-start | bytes 1572872 | tf_op jit(solution)/shard_map/ppermute | solution.py:24
  256.9 37.1 %copy-start.18 = (f32[56,2]{0,1:T(2,128)S(1)}, f32[56,2]{0,1:T(2,128)}, u32[]{:S(2)}) copy-start(f32[56,2]{0,1:T(2,128)} %param.26) | copy-start | bytes 1348
  281.2 45.8 %all-to-all-start.4 = ((bf16[32,4,2048]{2,1,0:T(4,128)(2,1)}), bf16[32,4,2048]{2,1,0:T(4,128)(2,1)S(1)}, u32[]{:S(2)}, u32[]{:S(2)}) async-start(bf16[32,4,2048]{2,1,0:T(4,128)(2,1)} %bitcast.196), calls=%async_computation.4 | async-start | bytes 1048576 | tf_op jit(solution)/shard_map/all_to_all | solution.py:28

commit v3 on v2

--- a/solution.py
+++ b/solution.py
@@ -101,46 +101,84 @@
     return whole.reshape(-1, own.shape[1])
 
 
-def expert_body(rows_ref, gate_ref, up_ref, down_ref, out_ref, hidden_ref):
-    inner, width = down_ref.shape
-    unit, wide = 128, 256
+UNIT = 128
+WIDE = 256
+
+
+def expert_body(
+    one_ref, two_ref, gate_hbm, up_hbm, down_hbm, one_out, two_out,
+    gate_ref, up_ref, down_ref, hidden_ref, gate_sem, up_sem, down_sem,
+):
+    units, columns, count = gate_ref.shape[0], down_ref.shape[0], one_ref.shape[0]
+
+    def block(k, size):
+        return pl.ds(pl.multiple_of(k * size, size), size)
+
+    def gate_copy(k):
+        return pltpu.make_async_copy(gate_hbm.at[:, block(k, UNIT)], gate_ref.at[k], gate_sem.at[k])
+
+    def up_copy(k):
+        return pltpu.make_async_copy(up_hbm.at[:, block(k, UNIT)], up_ref.at[k], up_sem.at[k])
+
+    def down_copy(k):
+        return pltpu.make_async_copy(down_hbm.at[:, block(k, WIDE)], down_ref.at[k], down_sem.at[k])
+
+    def ask(k, _):
+        gate_copy(k).start()
+        up_copy(k).start()
 
     def hide(k, _):
-        at = pl.ds(pl.multiple_of(k * unit, unit), unit)
-        both = jnp.concatenate([gate_ref[:, at], up_ref[:, at]], axis=1)
-        made = jnp.dot(rows_ref[...], both, preferred_element_type=jnp.float32)
-        gate, upward = made[:, :unit], made[:, unit:]
+        gate_copy(k).wait()
+        up_copy(k).wait()
+        both = jnp.concatenate([gate_ref[k], up_ref[k]], axis=1)
+        rows = jnp.concatenate([one_ref[...], two_ref[...]], axis=0)
+        made = jnp.dot(rows, both, preferred_element_type=jnp.float32)
+        gate, upward = made[:, :UNIT], made[:, UNIT:]
         hidden = gate / (1.0 + jnp.exp(-gate)) * upward
-        hidden_ref[:, at] = hidden.astype(jnp.bfloat16)
+        hidden_ref[:, block(k, UNIT)] = hidden.astype(jnp.bfloat16)
 
     def show(k, _):
-        at = pl.ds(pl.multiple_of(k * wide, wide), wide)
-        out_ref[:, at] = jnp.dot(
-            hidden_ref[...], down_ref[:, at], preferred_element_type=jnp.float32
-        ).astype(jnp.bfloat16)
-
-    lax.fori_loop(0, inner // unit, hide, None)
-    lax.fori_loop(0, width // wide, show, None)
-
-
-def expert_part(rows_in, gate_w, up_w, down_w):
-    count, width = rows_in.shape
+        down_copy(k).wait()
+        made = jnp.dot(hidden_ref[...], down_ref[k], preferred_element_type=jnp.float32)
+        made = made.astype(jnp.bfloat16)
+        one_out[:, block(k, WIDE)] = made[:count]
+        two_out[:, block(k, WIDE)] = made[count:]
+
+    lax.fori_loop(0, units, ask, None)
+    lax.fori_loop(0, columns, lambda k, _: down_copy(k).start(), None)
+    lax.fori_loop(0, units, hide, None)
+    lax.fori_loop(0, columns, show, None)
+
+
+def expert_parts(one, two, gate_w, up_w, down_w):
+    count, width = one.shape
     inner = gate_w.shape[1]
+    units, columns = inner // UNIT, width // WIDE
     whole = pl.BlockSpec(memory_space=pltpu.VMEM)
+    stored = pl.BlockSpec(memory_space=pltpu.HBM)
+    rows = jax.ShapeDtypeStruct((count, width), jnp.bfloat16)
     return pl.pallas_call(
         expert_body,
-        in_specs=[whole] * 4,
-        out_specs=whole,
-        out_shape=jax.ShapeDtypeStruct((count, width), jnp.bfloat16),
-        scratch_shapes=[pltpu.VMEM((count, inner), jnp.bfloat16)],
-        compiler_params=pltpu.CompilerParams(vmem_limit_bytes=24 << 20),
+        in_specs=[whole, whole, stored, stored, stored],
+        out_specs=[whole, whole],
+        out_shape=[rows, rows],
+        scratch_shapes=[
+            pltpu.VMEM((units, width, UNIT), jnp.bfloat16),
+            pltpu.VMEM((units, width, UNIT), jnp.bfloat16),
+            pltpu.VMEM((columns, inner, WIDE), jnp.bfloat16),
+            pltpu.VMEM((2 * count, inner), jnp.bfloat16),
+            pltpu.SemaphoreType.DMA((units,)),
+            pltpu.SemaphoreType.DMA((units,)),
+            pltpu.SemaphoreType.DMA((columns,)),
+        ],
+        compiler_params=pltpu.CompilerParams(vmem_limit_bytes=32 << 20),
         cost_estimate=pl.CostEstimate(
-            flops=6 * count * width * inner,
-            bytes_accessed=6 * width * inner + 4 * count * width,
-            transcendentals=count * inner,
+            flops=12 * count * width * inner,
+            bytes_accessed=6 * width * inner + 8 * count * width,
+            transcendentals=2 * count * inner,
         ),
-        name="expert_part",
-    )(rows_in, gate_w, up_w, down_w)
+        name="expert_parts",
+    )(one, two, gate_w, up_w, down_w)
 
 
 def packed(by_slot, lines):
@@ -176,17 +214,13 @@
     half = rows.shape[0] // 2
     left = shifted(rows, "tp", 1)
     right = shifted(rows, "tp", size - 1)
-    own = expert_part(rows, *weights)
     across = [shifted(left[:half], "tp", 1), shifted(right[half:], "tp", size - 1)]
-    left, right, _ = lax.optimization_barrier((left, right, own))
-    from_left = expert_part(left, *weights)
-    right, _ = lax.optimization_barrier((right, from_left))
-    from_right = expert_part(right, *weights)
-    across, _ = lax.optimization_barrier((jnp.concatenate(across, axis=0), from_right))
-    from_across = expert_part(across, *weights)
-    parts = [own]
-    for piece, by in ((from_left, size - 1), (from_right, 1), (from_across, 2)):
-        parts.append(shifted(piece, "tp", by))
+    left, right = lax.optimization_barrier((left, right))
+    from_left, from_right = expert_parts(left, right, *weights)
+    parts = [shifted(from_left, "tp", size - 1), shifted(from_right, "tp", 1)]
+    across, rows, _ = lax.optimization_barrier((jnp.concatenate(across, axis=0), rows, from_right))
+    from_across, own = expert_parts(across, rows, *weights)
+    parts = [own, *parts, shifted(from_across, "tp", 2)]
     made = sum(part.astype(jnp.float32) for part in parts).astype(jnp.bfloat16)
     return made.reshape(by_slot.shape), from_across
 
@@ -293,7 +327,7 @@
         preferred_element_type=jnp.float32,
     ).astype(jnp.bfloat16)
 
-    weights = (expert_gate_matrix[0], expert_up_matrix[0], expert_down_matrix[0])
+    weights = tuple(pltpu.with_memory_space_constraint(w[0], pltpu.HBM) for w in (expert_gate_matrix, expert_up_matrix, expert_down_matrix))
     early = (slots + 1) // 2
     by_slot = outgoing.reshape(slots, experts, width)
     got_a = traded(packed(by_slot[:early], early), SP)

time: 331 us -> 325 us (0.982)
  waiting for transfers between devices: 130 us -> 144 us
  local copies, waits for them, and re-layouts: 22.6 us -> 10.2 us
  Pallas kernels: 34.1 us -> 26.9 us
    ppermute x21, waiting for transfers between devices: 49.9 us -> 64 us  [shifted(): return lax.ppermute(x, axis, [(i, (i + by) % size) for i in range(size)])]
    unnamed x40 -> x26, local copies, waits for them, and re-layouts: 13.4 us -> 1.17 us
    pallas_call x8 -> x4, Pallas kernels: 34.1 us -> 26.9 us  [expert_parts(): pl.pallas_call(expert_body, in_specs=[whole, whole, stored, stored, store...]
  transfers between devices with their start and end apart: 31 -> 31, of which waited for: 10 -> 15; matrix products, arithmetic and copies ran while one was open for 4% -> 4% of each run, Pallas kernels for 10% -> 8%
where the time goes in v3:
time: 325 us; the launch traced here: 324 us
  waiting for transfers between devices  144 us (44%)
  starting transfers between devices  125 us (38%)
  Pallas kernels  26.9 us (8%)
  local copies, waits for them, and re-layouts  10.2 us (3%)
  other arithmetic  8.85 us (3%)
  matrix products  7.53 us (2%)
    all_to_all x7, waiting for transfers between devices, traded(): return lax.all_to_all(x, axis, split_axis=0, concat_axis=0, tiled=True)  78.3 us
    ppermute x21, waiting for transfers between devices, shifted(): return lax.ppermute(x, axis, [(i, (i + by) % size) for i in range(size)])  64 us
    all_to_all x7, starting transfers between devices, traded(): return lax.all_to_all(x, axis, split_axis=0, concat_axis=0, tiled=True)  59.5 us
    ppermute x21, starting transfers between devices, shifted(): return lax.ppermute(x, axis, [(i, (i + by) % size) for i in range(size)])  52.9 us
    pallas_call x4, Pallas kernels, expert_parts(): pl.pallas_call(expert_body, in_specs=[whole, whole, stored, stored, store...  26.9 us
    ppermute x3, starting transfers between devices, states_before(): lax.ppermute(whole, 'far', [(i, i + back) for i in range(far - back)])  13 us
  transfers between devices with their start and end apart: 31, of which 15 were waited for; matrix products, arithmetic and copies ran while one was open for 4% of the time, Pallas kernels for 8%

profile of v3, /device:TPU:40, one launch (start us, length us, event | category | flops | bytes accessed | tf_op | source)
XLA Modules:
  0.0 323.5 jit_solution(14160755229415921156)
XLA Ops:
  0.0 0.9 fusion.36
  1.1 0.9 fusion.76
  2.0 0.8 exponential_bitcast_fusion
  3.1 1.0 copy.89
  4.2 0.5 fusion.19
  4.9 0.8 maximum_maximum_fusion
  5.6 8.5 %all-to-all-start = ((f32[8,40,128]{2,1,0:T(8,128)}), f32[8,40,128]{2,1,0:T(8,128)S(1)}, u32[]{:S(2)}, u32[]{:S(2)}) async-start(f32[8,40,128]{2,1,0:T(8,128)} %maximum_maximum_fusion), calls=%async_computation | async-start | bytes 327680 | tf_op jit(solution)/shard_map/all_to_all | solution.py:28
  14.1 10.6 %collective-permute-start.5 = (bf16[64,512]{1,0:T(8,128)(2,1)}, bf16[64,512]{1,0:T(8,128)(2,1)S(1)}, u32[]{:S(2)}, u32[]{:S(2)}) collective-permute-start(bf16[64,512]{1,0:T(8,128)(2,1)} %bitcast.243), channel_id=1, source_target_pairs={{0,32},{32,64},{64,96},{96,0},{1,33},{33,65},{65,97},{97,1},{2,34}... | collective-permute-start | bytes 196616 | tf_op jit(solution)/shard_map/ppermute | solution.py:24
  24.7 13.2 %collective-permute-start.4 = (bf16[64,512]{1,0:T(8,128)(2,1)}, bf16[64,512]{1,0:T(8,128)(2,1)S(1)}, u32[]{:S(2)}, u32[]{:S(2)}) collective-permute-start(bf16[64,512]{1,0:T(8,128)(2,1)} %bitcast.244), channel_id=1, source_target_pairs={{0,64},{32,96},{64,0},{96,32},{1,65},{33,97},{65,1},{97,33},{2,66}... | collective-permute-start | bytes 196616 | tf_op jit(solution)/shard_map/ppermute | solution.py:24
  38.1 0.6 slice_reduce_fusion.2
  39.0 0.6 slice.186
  39.7 0.6 pad.58.clone
  40.3 0.7 pad.57.clone
  41.2 7.8 %collective-permute-start.2 = (f32[40,128]{1,0:T(8,128)S(1)}, f32[40,128]{1,0:T(8,128)S(1)}, u32[]{:S(2)}, u32[]{:S(2)}) collective-permute-start(f32[40,128]{1,0:T(8,128)S(1)} %maximum_bitcast_fusion.10), channel_id=1, source_target_pairs={{0,32},{32,64},{64,96},{1,33},{33,65},{65,97},{2,34},{34,66},{66,9... | collective-permute-start | bytes 61448 | tf_op jit(solution)/shard_map/ppermute | solution.py:67
  49.2 3.1 collective-permute-start.1
  52.3 2.1 collective-permute-start
  54.4 1.4 collective-permute-done
  56.8 0.8 maximum_maximum_fusion.1
  57.5 5.0 %all-to-all-start.1 = ((f32[8,40,128]{2,1,0:T(8,128)}), f32[8,40,128]{2,1,0:T(8,128)S(1)}, u32[]{:S(2)}, u32[]{:S(2)}) async-start(f32[8,40,128]{2,1,0:T(8,128)} %maximum_maximum_fusion.1), calls=%async_computation.1 | async-start | bytes 327680 | tf_op jit(solution)/shard_map/all_to_all | solution.py:28
  62.6 6.9 %collective-permute-start.8 = (bf16[4,64,512]{2,1,0:T(8,128)(2,1)S(1)}, bf16[4,64,512]{2,1,0:T(8,128)(2,1)S(1)}, u32[]{:S(2)}, u32[]{:S(2)}) collective-permute-start(bf16[4,64,512]{2,1,0:T(8,128)(2,1)S(1)} %get-tuple-element.63), channel_id=1, source_target_pairs={{0,112},{8,120},{16,0},{24,8},{32,16},{40,24},{48,32},{56,40},{64,... | collective-permute-start | bytes 786440 | tf_op jit(solution)/shard_map/ppermute | solution.py:24
  69.5 0.6 collective-permute-start.7
  70.0 1.5 collective-permute-start.6
  72.1 0.6 bitcast_convert_fusion
  72.7 9.2 %collective-permute-done.8 = bf16[4,64,512]{2,1,0:T(8,128)(2,1)S(1)} collective-permute-done((bf16[4,64,512]{2,1,0:T(8,128)(2,1)S(1)}, bf16[4,64,512]{2,1,0:T(8,128)(2,1)S(1)}, u32[]{:S(2)}, u32[]{:S(2)}) %collective-permute-start.8) | collective-permute-done | bytes 262176 | tf_op jit(solution)/shard_map/ppermute | solution.py:24
  81.9 5.2 %collective-permute-done.7 = bf16[4,64,512]{2,1,0:T(8,128)(2,1)S(1)} collective-permute-done((bf16[4,64,512]{2,1,0:T(8,128)(2,1)S(1)}, bf16[4,64,512]{2,1,0:T(8,128)(2,1)S(1)}, u32[]{:S(2)}, u32[]{:S(2)}) %collective-permute-start.7) | collective-permute-done | bytes 262176 | tf_op jit(solution)/shard_map/ppermute | solution.py:24
  87.7 0.4 fusion.10
  88.1 1.6 multiply_reduce_fusion.2
  90.7 0.8 fusion.5
  91.5 1.8 convolution_convert_fusion
  93.3 4.7 %all-to-all-start.2 = ((bf16[4,56,2048]{2,1,0:T(8,128)(2,1)}), bf16[4,56,2048]{2,1,0:T(8,128)(2,1)S(1)}, u32[]{:S(2)}, u32[]{:S(2)}) async-start(bf16[4,56,2048]{2,1,0:T(8,128)(2,1)} %bitcast.36), calls=%async_computation.2 | async-start | bytes 1835008 | tf_op jit(solution)/shard_map/all_to_all | solution.py:28
  98.4 13.6 %all-to-all-done.2 = bf16[4,56,2048]{2,1,0:T(8,128)(2,1)S(1)} async-done(((bf16[4,56,2048]{2,1,0:T(8,128)(2,1)}), bf16[4,56,2048]{2,1,0:T(8,128)(2,1)S(1)}, u32[]{:S(2)}, u32[]{:S(2)}) %all-to-all-start.2) | async-done | bytes 917536 | tf_op jit(solution)/shard_map/all_to_all | solution.py:28
  112.4 0.5 convolution_convert_fusion.1
  112.9 1.2 copy.129
  114.1 9.9 %all-to-all-start.3 = ((bf16[32,4,2048]{2,1,0:T(4,128)(2,1)}), bf16[32,4,2048]{2,1,0:T(4,128)(2,1)S(1)}, u32[]{:S(2)}, u32[]{:S(2)}) async-start(bf16[32,4,2048]{2,1,0:T(4,128)(2,1)} %bitcast.197), calls=%async_computation.3 | async-start | bytes 1048576 | tf_op jit(solution)/shard_map/all_to_all | solution.py:28
  124.2 1.1 copy.104
  125.2 31.9 %all-to-all-done.3 = bf16[32,4,2048]{2,1,0:T(4,128)(2,1)S(1)} async-done(((bf16[32,4,2048]{2,1,0:T(4,128)(2,1)}), bf16[32,4,2048]{2,1,0:T(4,128)(2,1)S(1)}, u32[]{:S(2)}, u32[]{:S(2)}) %all-to-all-start.3) | async-done | bytes 524320 | tf_op jit(solution)/shard_map/all_to_all | solution.py:28
  157.1 4.8 %all-to-all-start.5 = ((bf16[32,4,1536]{2,1,0:T(4,128)(2,1)}), bf16[32,4,1536]{2,1,0:T(4,128)(2,1)S(1)}, u32[]{:S(2)}, u32[]{:S(2)}) async-start(bf16[32,4,1536]{2,1,0:T(4,128)(2,1)} %copy.104), calls=%async_computation.5 | async-start | bytes 786432 | tf_op jit(solution)/shard_map/all_to_all | solution.py:28
  162.2 1.3 collective-permute-start.12
  163.5 0.9 collective-permute-start.10
  164.4 11.3 %collective-permute-done.12.two_ref = bf16[128,2048]{1,0:T(8,128)(2,1)S(1)} collective-permute-done((bf16[128,2048]{1,0:T(8,128)(2,1)S(1)}, bf16[128,2048]{1,0:T(8,128)(2,1)S(1)}, u32[]{:S(2)}, u32[]{:S(2)}) %collective-permute-start.12) | collective-permute-done | bytes 524320 | tf_op jit(solution)/shard_map/ppermute | solution.py:24
  175.7 2.5 collective-permute-start.13
  178.3 7.1 %expert_parts.4 = (bf16[128,2048]{1,0:T(8,128)(2,1)S(1)}, bf16[128,2048]{1,0:T(8,128)(2,1)S(1)}) custom-call(bf16[128,2048]{1,0:T(8,128)(2,1)S(1)} %collective-permute-done.10.one_ref, bf16[128,2048]{1,0:T(8,128)(2,1)S(1)} %collective-permute-done.12.two_ref, bf16[2048,896]{1,0:T(8,128)(2,1)} %bitcast.206, bf16[2048,896]{1,0:T(8,128)(2,1)} %bitcast.210, ...), custom_call_target="tpu_custom_call" | custom-call | flops 2818572288 | bytes 13107200 | tf_op jit(solution)/shard_map/expert_parts/pallas_call | solution.py:160
  185.4 0.6 collective-permute-done.11
  186.1 7.1 %expert_parts.5 = (bf16[128,2048]{1,0:T(8,128)(2,1)S(1)}, bf16[128,2048]{1,0:T(8,128)(2,1)S(1)}) custom-call(bf16[128,2048]{1,0:T(8,128)(2,1)S(1)} %pad_maximum_fusion.2.one_ref, bf16[128,2048]{1,0:T(8,128)(2,1)S(1)} %bitcast.202, bf16[2048,896]{1,0:T(8,128)(2,1)} %bitcast.207, bf16[2048,896]{1,0:T(8,128)(2,1)} %bitcast.211, bf16[896,2048]{1,0:T(8,128)(2,1)} %bitcast.215), custom_call_target="tpu_custom_call" | custom-call | flops 2818572288 | bytes 13107200 | tf_op jit(solution)/shard_map/expert_parts/pallas_call | solution.py:160
  193.5 2.7 collective-permute-start.19
  196.2 6.6 %collective-permute-done.19.two_ref = bf16[96,2048]{1,0:T(8,128)(2,1)S(1)} collective-permute-done((bf16[96,2048]{1,0:T(8,128)(2,1)S(1)}, bf16[96,2048]{1,0:T(8,128)(2,1)S(1)}, u32[]{:S(2)}, u32[]{:S(2)}) %collective-permute-start.19) | collective-permute-done | bytes 393248 | tf_op jit(solution)/shard_map/ppermute | solution.py:24
  202.8 3.8 %collective-permute-start.20 = (bf16[48,2048]{1,0:T(8,128)(2,1)S(1)}, bf16[48,2048]{1,0:T(8,128)(2,1)S(1)}, u32[]{:S(2)}, u32[]{:S(2)}) collective-permute-start(bf16[48,2048]{1,0:T(8,128)(2,1)S(1)} %slice.259), channel_id=1, source_target_pairs={{0,3},{1,0},{2,1},{3,2},{4,7},{5,4},{6,5},{7,6},{8,11},{9,8},{10,9... | collective-permute-start | bytes 589832 | tf_op jit(solution)/shard_map/ppermute | solution.py:24
  206.7 6.4 %expert_parts.6 = (bf16[96,2048]{1,0:T(8,128)(2,1)S(1)}, bf16[96,2048]{1,0:T(8,128)(2,1)S(1)}) custom-call(bf16[96,2048]{1,0:T(8,128)(2,1)S(1)} %collective-permute-done.17.one_ref, bf16[96,2048]{1,0:T(8,128)(2,1)S(1)} %collective-permute-done.19.two_ref, bf16[2048,896]{1,0:T(8,128)(2,1)} %bitcast.208, bf16[2048,896]{1,0:T(8,128)(2,1)} %bitcast.212, ...), custom_call_target="tpu_custom_call" | custom-call | flops 2113929216 | bytes 12582912 | tf_op jit(solution)/shard_map/expert_parts/pallas_call | solution.py:160
  213.5 3.3 %collective-permute-start.21 = (bf16[96,2048]{1,0:T(8,128)(2,1)S(1)}, bf16[96,2048]{1,0:T(8,128)(2,1)S(1)}, u32[]{:S(2)}, u32[]{:S(2)}) collective-permute-start(bf16[96,2048]{1,0:T(8,128)(2,1)S(1)} %get-tuple-element.37), channel_id=1, source_target_pairs={{0,3},{1,0},{2,1},{3,2},{4,7},{5,4},{6,5},{7,6},{8,11},{9,8},{10,9... | collective-permute-start | bytes 1179656 | tf_op jit(solution)/shard_map/ppermute | solution.py:24
  216.8 6.4 %expert_parts.7 = (bf16[96,2048]{1,0:T(8,128)(2,1)S(1)}, bf16[96,2048]{1,0:T(8,128)(2,1)S(1)}) custom-call(bf16[96,2048]{1,0:T(8,128)(2,1)S(1)} %pad_maximum_fusion.4.one_ref, bf16[96,2048]{1,0:T(8,128)(2,1)S(1)} %bitcast.205, bf16[2048,896]{1,0:T(8,128)(2,1)} %bitcast.209, bf16[2048,896]{1,0:T(8,128)(2,1)} %bitcast.213, bf16[896,2048]{1,0:T(8,128)(2,1)} %bitcast.217), custom_call_target="tpu_custom_call" | custom-call | flops 2113929216 | bytes 12582912 | tf_op jit(solution)/shard_map/expert_parts/pallas_call | solution.py:160
  223.2 1.5 collective-permute-start.23
  224.7 1.7 collective-permute-done.21
  226.3 6.3 %collective-permute-done.23 = bf16[96,2048]{1,0:T(8,128)(2,1)S(1)} collective-permute-done((bf16[96,2048]{1,0:T(8,128)(2,1)S(1)}, bf16[96,2048]{1,0:T(8,128)(2,1)S(1)}, u32[]{:S(2)}, u32[]{:S(2)}) %collective-permute-start.23) | collective-permute-done | bytes 393248 | tf_op jit(solution)/shard_map/ppermute | solution.py:24
  233.0 1.1 copy.106
  234.0 13.9 %all-to-all-start.6 = ((bf16[32,4,1536]{2,1,0:T(4,128)(2,1)}), bf16[32,4,1536]{2,1,0:T(4,128)(2,1)S(1)}, u32[]{:S(2)}, u32[]{:S(2)}) async-start(bf16[32,4,1536]{2,1,0:T(4,128)(2,1)} %copy.106), calls=%async_computation.6 | async-start | bytes 786432 | tf_op jit(solution)/shard_map/all_to_all | solution.py:28
  248.0 1.2 collective-permute-start.15
  249.2 2.1 collective-permute-start.14
  251.5 12.5 %collective-permute-done.15 = bf16[128,2048]{1,0:T(8,128)(2,1)S(1)} collective-permute-done((bf16[128,2048]{1,0:T(8,128)(2,1)S(1)}, bf16[128,2048]{1,0:T(8,128)(2,1)S(1)}, u32[]{:S(2)}, u32[]{:S(2)}) %collective-permute-start.15) | collective-permute-done | bytes 524320 | tf_op jit(solution)/shard_map/ppermute | solution.py:24
  264.0 9.5 %collective-permute-done.14 = bf16[128,2048]{1,0:T(8,128)(2,1)S(1)} collective-permute-done((bf16[128,2048]{1,0:T(8,128)(2,1)S(1)}, bf16[128,2048]{1,0:T(8,128)(2,1)S(1)}, u32[]{:S(2)}, u32[]{:S(2)}) %collective-permute-start.14) | collective-permute-done | bytes 524320 | tf_op jit(solution)/shard_map/ppermute | solution.py:24
  273.5 0.8 collective-permute-done.16
  274.6 1.2 copy.128
  275.8 12.7 %all-to-all-start.4 = ((bf16[32,4,2048]{2,1,0:T(4,128)(2,1)}), bf16[32,4,2048]{2,1,0:T(4,128)(2,1)S(1)}, u32[]{:S(2)}, u32[]{:S(2)}) async-start(bf16[32,4,2048]{2,1,0:T(4,128)(2,1)} %bitcast.196), calls=%async_computation.4 | async-start | bytes 1048576 | tf_op jit(solution)/shard_map/all_to_all | solution.py:28
  288.9 32.8 %all-to-all-done.4 = bf16[32,4,2048]{2,1,0:T(4,128)(2,1)S(1)} async-done(((bf16[32,4,2048]{2,1,0:T(4,128)(2,1)}), bf16[32,4,2048]{2,1,0:T(4,128)(2,1)S(1)}, u32[]{:S(2)}, u32[]{:S(2)}) %all-to-all-start.4) | async-done | bytes 524320 | tf_op jit(solution)/shard_map/all_to_all | solution.py:28
  322.6 0.9 fusion.4
  (143 shorter events, 8.8 us)
Async XLA Ops:
  0.0 4.2 %copy-start = (bf16[224,512]{1,0:T(8,128)(2,1)S(1)}, bf16[224,512]{1,0:T(8,128)(2,1)}, u32[]{:S(2)}) copy-start(bf16[224,512]{1,0:T(8,128)(2,1)} %param.17) | copy-start | bytes 688132
  0.0 62.5 %copy-start.5 = (bf16[512,64]{0,1:T(8,128)(2,1)S(1)}, bf16[512,64]{0,1:T(8,128)(2,1)}, u32[]{:S(2)}) copy-start(bf16[512,64]{0,1:T(8,128)(2,1)} %param.22) | copy-start | bytes 196612
  3.1 68.4 %copy-start.6 = (f32[4,224]{1,0:T(4,128)S(1)}, f32[4,224]{1,0:T(4,128)}, u32[]{:S(2)}) copy-start(f32[4,224]{1,0:T(4,128)} %param.18) | copy-start | bytes 10756
  4.1 1.5 copy-start.3
  4.1 67.8 %copy-start.8 = (bf16[2048]{0:T(1024)(128)(2,1)S(1)}, bf16[2048]{0:T(1024)(128)(2,1)}, u32[]{:S(2)}) copy-start(bf16[2048]{0:T(1024)(128)(2,1)} %param.24) | copy-start | bytes 12292
  4.1 67.8 %copy-start.4 = (bf16[224,256]{1,0:T(8,128)(2,1)S(1)}, bf16[224,256]{1,0:T(8,128)(2,1)}, u32[]{:S(2)}) copy-start(bf16[224,256]{1,0:T(8,128)(2,1)} %param.15) | copy-start | bytes 344068
  4.2 67.8 %copy-start.10 = (bf16[512]{0:T(512)(128)(2,1)S(1)}, bf16[512]{0:T(512)(128)(2,1)}, u32[]{:S(2)}) copy-start(bf16[512]{0:T(512)(128)(2,1)} %param.21) | copy-start | bytes 3076
  5.6 32.5 %all-to-all-start = ((f32[8,40,128]{2,1,0:T(8,128)}), f32[8,40,128]{2,1,0:T(8,128)S(1)}, u32[]{:S(2)}, u32[]{:S(2)}) async-start(f32[8,40,128]{2,1,0:T(8,128)} %maximum_maximum_fusion), calls=%async_computation | async-start | bytes 327680 | tf_op jit(solution)/shard_map/all_to_all | solution.py:28
  14.1 48.4 %collective-permute-start.5 = (bf16[64,512]{1,0:T(8,128)(2,1)}, bf16[64,512]{1,0:T(8,128)(2,1)S(1)}, u32[]{:S(2)}, u32[]{:S(2)}) collective-permute-start(bf16[64,512]{1,0:T(8,128)(2,1)} %bitcast.243), channel_id=1, source_target_pairs={{0,32},{32,64},{64,96},{96,0},{1,33},{33,65},{65,97},{97,1},{2,34}... | collective-permute-start | bytes 196616 | tf_op jit(solution)/shard_map/ppermute | solution.py:24
  24.7 37.8 %collective-permute-start.4 = (bf16[64,512]{1,0:T(8,128)(2,1)}, bf16[64,512]{1,0:T(8,128)(2,1)S(1)}, u32[]{:S(2)}, u32[]{:S(2)}) collective-permute-start(bf16[64,512]{1,0:T(8,128)(2,1)} %bitcast.244), channel_id=1, source_target_pairs={{0,64},{32,96},{64,0},{96,32},{1,65},{33,97},{65,1},{97,33},{2,66}... | collective-permute-start | bytes 196616 | tf_op jit(solution)/shard_map/ppermute | solution.py:24
  37.9 24.6 %collective-permute-start.3 = (bf16[64,512]{1,0:T(8,128)(2,1)}, bf16[64,512]{1,0:T(8,128)(2,1)S(1)}, u32[]{:S(2)}, u32[]{:S(2)}) collective-permute-start(bf16[64,512]{1,0:T(8,128)(2,1)} %bitcast.245), channel_id=1, source_target_pairs={{0,96},{32,0},{64,32},{96,64},{1,97},{33,1},{65,33},{97,65},{2,98}... | collective-permute-start | bytes 196616 | tf_op jit(solution)/shard_map/ppermute | solution.py:24
  38.1 33.9 %copy-start.2 = (pred[224,224]{1,0:T(8,128)(4,1)}, pred[224,224]{1,0:T(8,128)(4,1)S(1)}, u32[]{:S(2)}) copy-start(pred[224,224]{1,0:T(8,128)(4,1)S(1)} %iota_compare_fusion.1) | copy-start | bytes 150532
  41.2 11.1 %collective-permute-start.2 = (f32[40,128]{1,0:T(8,128)S(1)}, f32[40,128]{1,0:T(8,128)S(1)}, u32[]{:S(2)}, u32[]{:S(2)}) collective-permute-start(f32[40,128]{1,0:T(8,128)S(1)} %maximum_bitcast_fusion.10), channel_id=1, source_target_pairs={{0,32},{32,64},{64,96},{1,33},{33,65},{65,97},{2,34},{34,66},{66,9... | collective-permute-start | bytes 61448 | tf_op jit(solution)/shard_map/ppermute | solution.py:67
  49.2 5.3 %collective-permute-start.1 = (f32[40,128]{1,0:T(8,128)S(1)}, f32[40,128]{1,0:T(8,128)S(1)}, u32[]{:S(2)}, u32[]{:S(2)}) collective-permute-start(f32[40,128]{1,0:T(8,128)S(1)} %maximum_bitcast_fusion.10), channel_id=1, source_target_pairs={{0,64},{32,96},{1,65},{33,97},{2,66},{34,98},{3,67},{35,99},{4,68}... | collective-permute-start | bytes 61448 | tf_op jit(solution)/shard_map/ppermute | solution.py:67
  52.3 3.6 %collective-permute-start = (f32[40,128]{1,0:T(8,128)S(1)}, f32[40,128]{1,0:T(8,128)S(1)}, u32[]{:S(2)}, u32[]{:S(2)}) collective-permute-start(f32[40,128]{1,0:T(8,128)S(1)} %maximum_bitcast_fusion.10), channel_id=1, source_target_pairs={{0,96},{1,97},{2,98},{3,99},{4,100},{5,101},{6,102},{7,103},{8,104... | collective-permute-start | bytes 61448 | tf_op jit(solution)/shard_map/ppermute | solution.py:67
  57.5 29.9 %all-to-all-start.1 = ((f32[8,40,128]{2,1,0:T(8,128)}), f32[8,40,128]{2,1,0:T(8,128)S(1)}, u32[]{:S(2)}, u32[]{:S(2)}) async-start(f32[8,40,128]{2,1,0:T(8,128)} %maximum_maximum_fusion.1), calls=%async_computation.1 | async-start | bytes 327680 | tf_op jit(solution)/shard_map/all_to_all | solution.py:28
  62.6 19.3 %collective-permute-start.8 = (bf16[4,64,512]{2,1,0:T(8,128)(2,1)S(1)}, bf16[4,64,512]{2,1,0:T(8,128)(2,1)S(1)}, u32[]{:S(2)}, u32[]{:S(2)}) collective-permute-start(bf16[4,64,512]{2,1,0:T(8,128)(2,1)S(1)} %get-tuple-element.63), channel_id=1, source_target_pairs={{0,112},{8,120},{16,0},{24,8},{32,16},{40,24},{48,32},{56,40},{64,... | collective-permute-start | bytes 786440 | tf_op jit(solution)/shard_map/ppermute | solution.py:24
  69.5 17.6 %collective-permute-start.7 = (bf16[4,64,512]{2,1,0:T(8,128)(2,1)S(1)}, bf16[4,64,512]{2,1,0:T(8,128)(2,1)S(1)}, u32[]{:S(2)}, u32[]{:S(2)}) collective-permute-start(bf16[4,64,512]{2,1,0:T(8,128)(2,1)S(1)} %get-tuple-element.63), channel_id=1, source_target_pairs={{0,120},{8,0},{16,8},{24,16},{32,24},{40,32},{48,40},{56,48},{64,5... | collective-permute-start | bytes 786440 | tf_op jit(solution)/shard_map/ppermute | solution.py:24
  70.0 17.1 %collective-permute-start.6 = (bf16[4,64,512]{2,1,0:T(8,128)(2,1)S(1)}, bf16[4,64,512]{2,1,0:T(8,128)(2,1)S(1)}, u32[]{:S(2)}, u32[]{:S(2)}) collective-permute-start(bf16[4,64,512]{2,1,0:T(8,128)(2,1)S(1)} %get-tuple-element.63), channel_id=1, source_target_pairs={{0,8},{8,16},{16,24},{24,32},{32,40},{40,48},{48,56},{56,64},{64,7... | collective-permute-start | bytes 786440 | tf_op jit(solution)/shard_map/ppermute | solution.py:24
  87.3 2.8 collective-permute-start.9
  90.7 0.8 copy-start.7
  91.5 6.5 %copy-start.9 = (s32[56,2]{0,1:T(2,128)S(1)}, s32[56,2]{0,1:T(2,128)}, u32[]{:S(2)}) copy-start(s32[56,2]{0,1:T(2,128)} %param.25) | copy-start | bytes 1348
  93.3 18.9 %copy-start.1 = (bf16[56,2048]{1,0:T(8,128)(2,1)S(1)}, bf16[56,2048]{1,0:T(8,128)(2,1)}, u32[]{:S(2)}) copy-start(bf16[56,2048]{1,0:T(8,128)(2,1)} %param.23) | copy-start | bytes 688132
  93.3 18.8 %all-to-all-start.2 = ((bf16[4,56,2048]{2,1,0:T(8,128)(2,1)}), bf16[4,56,2048]{2,1,0:T(8,128)(2,1)S(1)}, u32[]{:S(2)}, u32[]{:S(2)}) async-start(bf16[4,56,2048]{2,1,0:T(8,128)(2,1)} %bitcast.36), calls=%async_computation.2 | async-start | bytes 1835008 | tf_op jit(solution)/shard_map/all_to_all | solution.py:28
  114.1 43.0 %all-to-all-start.3 = ((bf16[32,4,2048]{2,1,0:T(4,128)(2,1)}), bf16[32,4,2048]{2,1,0:T(4,128)(2,1)S(1)}, u32[]{:S(2)}, u32[]{:S(2)}) async-start(bf16[32,4,2048]{2,1,0:T(4,128)(2,1)} %bitcast.197), calls=%async_computation.3 | async-start | bytes 1048576 | tf_op jit(solution)/shard_map/all_to_all | solution.py:28
  157.1 36.1 %all-to-all-start.5 = ((bf16[32,4,1536]{2,1,0:T(4,128)(2,1)}), bf16[32,4,1536]{2,1,0:T(4,128)(2,1)S(1)}, u32[]{:S(2)}, u32[]{:S(2)}) async-start(bf16[32,4,1536]{2,1,0:T(4,128)(2,1)} %copy.104), calls=%async_computation.5 | async-start | bytes 786432 | tf_op jit(solution)/shard_map/all_to_all | solution.py:28
  162.2 13.4 %collective-permute-start.12 = (bf16[128,2048]{1,0:T(8,128)(2,1)S(1)}, bf16[128,2048]{1,0:T(8,128)(2,1)S(1)}, u32[]{:S(2)}, u32[]{:S(2)}) collective-permute-start(bf16[128,2048]{1,0:T(8,128)(2,1)S(1)} %bitcast.200), channel_id=1, source_target_pairs={{0,3},{1,0},{2,1},{3,2},{4,7},{5,4},{6,5},{7,6},{8,11},{9,8},{10,9... | collective-permute-start | bytes 1572872 | tf_op jit(solution)/shard_map/ppermute | solution.py:24
  163.5 14.7 %collective-permute-start.10 = (bf16[128,2048]{1,0:T(8,128)(2,1)S(1)}, bf16[128,2048]{1,0:T(8,128)(2,1)S(1)}, u32[]{:S(2)}, u32[]{:S(2)}) collective-permute-start(bf16[128,2048]{1,0:T(8,128)(2,1)S(1)} %bitcast.201), channel_id=1, source_target_pairs={{0,1},{1,2},{2,3},{3,0},{4,5},{5,6},{6,7},{7,4},{8,9},{9,10},{10,1... | collective-permute-start | bytes 1572872 | tf_op jit(solution)/shard_map/ppermute | solution.py:24
  175.7 9.8 %collective-permute-start.13 = (bf16[64,2048]{1,0:T(8,128)(2,1)S(1)}, bf16[64,2048]{1,0:T(8,128)(2,1)S(1)}, u32[]{:S(2)}, u32[]{:S(2)}) collective-permute-start(bf16[64,2048]{1,0:T(8,128)(2,1)S(1)} %slice.243), channel_id=1, source_target_pairs={{0,3},{1,0},{2,1},{3,2},{4,7},{5,4},{6,5},{7,6},{8,11},{9,8},{10,9... | collective-permute-start | bytes 786440 | tf_op jit(solution)/shard_map/ppermute | solution.py:24
  178.2 7.9 %collective-permute-start.11 = (bf16[64,2048]{1,0:T(8,128)(2,1)S(1)}, bf16[64,2048]{1,0:T(8,128)(2,1)S(1)}, u32[]{:S(2)}, u32[]{:S(2)}) collective-permute-start(bf16[64,2048]{1,0:T(8,128)(2,1)S(1)} %slice.242), channel_id=1, source_target_pairs={{0,1},{1,2},{2,3},{3,0},{4,5},{5,6},{6,7},{7,4},{8,9},{9,10},{10,1... | collective-permute-start | bytes 786440 | tf_op jit(solution)/shard_map/ppermute | solution.py:24
  193.5 9.3 %collective-permute-start.19 = (bf16[96,2048]{1,0:T(8,128)(2,1)S(1)}, bf16[96,2048]{1,0:T(8,128)(2,1)S(1)}, u32[]{:S(2)}, u32[]{:S(2)}) collective-permute-start(bf16[96,2048]{1,0:T(8,128)(2,1)S(1)} %bitcast.203), channel_id=1, source_target_pairs={{0,3},{1,0},{2,1},{3,2},{4,7},{5,4},{6,5},{7,6},{8,11},{9,8},{10,9... | collective-permute-start | bytes 1179656 | tf_op jit(solution)/shard_map/ppermute | solution.py:24
  196.1 10.4 %collective-permute-start.17 = (bf16[96,2048]{1,0:T(8,128)(2,1)S(1)}, bf16[96,2048]{1,0:T(8,128)(2,1)S(1)}, u32[]{:S(2)}, u32[]{:S(2)}) collective-permute-start(bf16[96,2048]{1,0:T(8,128)(2,1)S(1)} %bitcast.204), channel_id=1, source_target_pairs={{0,1},{1,2},{2,3},{3,0},{4,5},{5,6},{6,7},{7,4},{8,9},{9,10},{10,1... | collective-permute-start | bytes 1179656 | tf_op jit(solution)/shard_map/ppermute | solution.py:24
  202.8 14.0 %collective-permute-start.20 = (bf16[48,2048]{1,0:T(8,128)(2,1)S(1)}, bf16[48,2048]{1,0:T(8,128)(2,1)S(1)}, u32[]{:S(2)}, u32[]{:S(2)}) collective-permute-start(bf16[48,2048]{1,0:T(8,128)(2,1)S(1)} %slice.259), channel_id=1, source_target_pairs={{0,3},{1,0},{2,1},{3,2},{4,7},{5,4},{6,5},{7,6},{8,11},{9,8},{10,9... | collective-permute-start | bytes 589832 | tf_op jit(solution)/shard_map/ppermute | solution.py:24
  206.6 10.2 %collective-permute-start.18 = (bf16[48,2048]{1,0:T(8,128)(2,1)S(1)}, bf16[48,2048]{1,0:T(8,128)(2,1)S(1)}, u32[]{:S(2)}, u32[]{:S(2)}) collective-permute-start(bf16[48,2048]{1,0:T(8,128)(2,1)S(1)} %slice.258), channel_id=1, source_target_pairs={{0,1},{1,2},{2,3},{3,0},{4,5},{5,6},{6,7},{7,4},{8,9},{9,10},{10,1... | collective-permute-start | bytes 589832 | tf_op jit(solution)/shard_map/ppermute | solution.py:24
  213.1 11.6 %collective-permute-start.22 = (bf16[96,2048]{1,0:T(8,128)(2,1)S(1)}, bf16[96,2048]{1,0:T(8,128)(2,1)S(1)}, u32[]{:S(2)}, u32[]{:S(2)}) collective-permute-start(bf16[96,2048]{1,0:T(8,128)(2,1)S(1)} %get-tuple-element.33), channel_id=1, source_target_pairs={{0,1},{1,2},{2,3},{3,0},{4,5},{5,6},{6,7},{7,4},{8,9},{9,10},{10,1... | collective-permute-start | bytes 1179656 | tf_op jit(solution)/shard_map/ppermute | solution.py:24
  213.5 12.9 %collective-permute-start.21 = (bf16[96,2048]{1,0:T(8,128)(2,1)S(1)}, bf16[96,2048]{1,0:T(8,128)(2,1)S(1)}, u32[]{:S(2)}, u32[]{:S(2)}) collective-permute-start(bf16[96,2048]{1,0:T(8,128)(2,1)S(1)} %get-tuple-element.37), channel_id=1, source_target_pairs={{0,3},{1,0},{2,1},{3,2},{4,7},{5,4},{6,5},{7,6},{8,11},{9,8},{10,9... | collective-permute-start | bytes 1179656 | tf_op jit(solution)/shard_map/ppermute | solution.py:24
  223.2 9.4 %collective-permute-start.23 = (bf16[96,2048]{1,0:T(8,128)(2,1)S(1)}, bf16[96,2048]{1,0:T(8,128)(2,1)S(1)}, u32[]{:S(2)}, u32[]{:S(2)}) collective-permute-start(bf16[96,2048]{1,0:T(8,128)(2,1)S(1)} %get-tuple-element.38), channel_id=1, source_target_pairs={{0,2},{1,3},{2,0},{3,1},{4,6},{5,7},{6,4},{7,5},{8,10},{9,11},{10,... | collective-permute-start | bytes 1179656 | tf_op jit(solution)/shard_map/ppermute | solution.py:24
  234.0 41.8 %all-to-all-start.6 = ((bf16[32,4,1536]{2,1,0:T(4,128)(2,1)}), bf16[32,4,1536]{2,1,0:T(4,128)(2,1)S(1)}, u32[]{:S(2)}, u32[]{:S(2)}) async-start(bf16[32,4,1536]{2,1,0:T(4,128)(2,1)} %copy.106), calls=%async_computation.6 | async-start | bytes 786432 | tf_op jit(solution)/shard_map/all_to_all | solution.py:28
  248.0 16.0 %collective-permute-start.15 = (bf16[128,2048]{1,0:T(8,128)(2,1)S(1)}, bf16[128,2048]{1,0:T(8,128)(2,1)S(1)}, u32[]{:S(2)}, u32[]{:S(2)}) collective-permute-start(bf16[128,2048]{1,0:T(8,128)(2,1)S(1)} %get-tuple-element.24), channel_id=1, source_target_pairs={{0,1},{1,2},{2,3},{3,0},{4,5},{5,6},{6,7},{7,4},{8,9},{9,10},{10,1... | collective-permute-start | bytes 1572872 | tf_op jit(solution)/shard_map/ppermute | solution.py:24
  249.2 24.3 %collective-permute-start.14 = (bf16[128,2048]{1,0:T(8,128)(2,1)S(1)}, bf16[128,2048]{1,0:T(8,128)(2,1)S(1)}, u32[]{:S(2)}, u32[]{:S(2)}) collective-permute-start(bf16[128,2048]{1,0:T(8,128)(2,1)S(1)} %get-tuple-element.28), channel_id=1, source_target_pairs={{0,3},{1,0},{2,1},{3,2},{4,7},{5,4},{6,5},{7,6},{8,11},{9,8},{10,9... | collective-permute-start | bytes 1572872 | tf_op jit(solution)/shard_map/ppermute | solution.py:24
  251.3 22.9 %collective-permute-start.16 = (bf16[128,2048]{1,0:T(8,128)(2,1)S(1)}, bf16[128,2048]{1,0:T(8,128)(2,1)S(1)}, u32[]{:S(2)}, u32[]{:S(2)}) collective-permute-start(bf16[128,2048]{1,0:T(8,128)(2,1)S(1)} %get-tuple-element.29), channel_id=1, source_target_pairs={{0,2},{1,3},{2,0},{3,1},{4,6},{5,7},{6,4},{7,5},{8,10},{9,11},{10,... | collective-permute-start | bytes 1572872 | tf_op jit(solution)/shard_map/ppermute | solution.py:24
  274.3 14.3 %copy-start.11 = (f32[56,2]{0,1:T(2,128)S(1)}, f32[56,2]{0,1:T(2,128)}, u32[]{:S(2)}) copy-start(f32[56,2]{0,1:T(2,128)} %param.26) | copy-start | bytes 1348
  275.8 45.8 %all-to-all-start.4 = ((bf16[32,4,2048]{2,1,0:T(4,128)(2,1)}), bf16[32,4,2048]{2,1,0:T(4,128)(2,1)S(1)}, u32[]{:S(2)}, u32[]{:S(2)}) async-start(bf16[32,4,2048]{2,1,0:T(4,128)(2,1)} %bitcast.196), calls=%async_computation.4 | async-start | bytes 1048576 | tf_op jit(solution)/shard_map/all_to_all | solution.py:28

commit v4 on v3

--- a/solution.py
+++ b/solution.py
@@ -28,15 +28,42 @@
     return lax.all_to_all(x, axis, split_axis=0, concat_axis=0, tiled=True)
 
 
-def strength_of(totals, peaks):
-    size = totals.shape[0]
-    shape = (size + 1, size, size)
-    t, s, u = (lax.broadcasted_iota(jnp.int32, shape, d) for d in range(3))
-    decay = jnp.sum(jnp.where((s < u) & (u < t), totals[None, None, :], 0.0), axis=2)
-    earlier = s[:, :, 0] < t[:, :, 0]
-    logs = jnp.where(earlier, decay + peaks[None, :], far_below)
-    tops = jnp.max(logs, axis=1)
-    return jnp.where(earlier, jnp.exp(logs - tops[:, None]), 0.0), tops
+def combined(state, total, part, peak):
+    memory, top = state
+    kept = top + total
+    higher = jnp.maximum(kept, peak)
+    return jnp.exp(kept - higher) * memory + jnp.exp(peak - higher) * part, higher
+
+
+def group_body(parts_ref, out_ref):
+    size, lines, lanes = parts_ref.shape
+    rows = lines - 8
+    state = parts_ref[0, :rows], parts_ref[0, rows + 1 : rows + 2]
+    total = parts_ref[0, rows : rows + 1]
+    for p in range(1, size):
+        more = parts_ref[p, rows : rows + 1]
+        state = combined(state, more, parts_ref[p, :rows], parts_ref[p, rows + 1 : rows + 2])
+        total = total + more
+    out_ref[:rows] = state[0]
+    line = lax.broadcasted_iota(jnp.int32, (8, lanes), 0)
+    out_ref[rows:] = jnp.where(line == 0, total, state[1])
+
+
+def before_body(group_ref, parts_ref, *refs):
+    *others, out_ref = refs
+    size, lines, lanes = parts_ref.shape
+    rows = lines - 8
+    state = jnp.zeros((rows, lanes), jnp.float32), jnp.full((1, lanes), far_below, jnp.float32)
+    for back, other in zip(range(len(others), 0, -1), others):
+        known = group_ref[0] >= back
+        total = jnp.where(known, other[rows : rows + 1], 0.0)
+        peak = jnp.where(known, other[rows + 1 : rows + 2], far_below)
+        state = combined(state, total, jnp.where(known, other[:rows], 0.0), peak)
+    for p in range(size):
+        out_ref[p, :rows] = state[0]
+        out_ref[p, rows:] = jnp.broadcast_to(state[1], (8, lanes))
+        total, peak = parts_ref[p, rows : rows + 1], parts_ref[p, rows + 1 : rows + 2]
+        state = combined(state, total, parts_ref[p, :rows], peak)
 
 
 def with_header(body, *scalars):
@@ -56,25 +83,25 @@
         memory.reshape(near, rows, dv), jnp.repeat(totals, per_head), jnp.repeat(peaks, per_head)
     )
     got = traded(sent, NEAR)
-    parts, total, peak = got[:, :rows], got[:, rows, 0], got[:, rows + 1, 0]
-    size = total.shape[0]
-    weight, tops = strength_of(total, peak)
-    whole = jnp.sum(weight[size][:, None, None] * parts, axis=0)
-    whole = with_header(whole[None], jnp.sum(total).reshape(1), tops[size].reshape(1))[0]
-    group = lax.axis_index("far")
+    whole = pl.pallas_call(
+        group_body,
+        out_shape=jax.ShapeDtypeStruct(got.shape[1:], jnp.float32),
+        compiler_params=pltpu.CompilerParams(vmem_limit_bytes=4 << 20),
+        name="group_state",
+    )(got)
     before = []
     for back in range(far - 1, 0, -1):
-        other = lax.ppermute(whole, "far", [(i, i + back) for i in range(far - back)])
-        before.append(jnp.where(group >= back, other, jnp.zeros_like(other)))
-    stack = jnp.stack(before)
-    known = group >= jnp.arange(far - 1, 0, -1)
-    all_total = jnp.concatenate([stack[:, rows, 0], total])
-    all_peak = jnp.concatenate([jnp.where(known, stack[:, rows + 1, 0], far_below), peak])
-    weight, tops = strength_of(all_total, all_peak)
-    weight, tops = weight[far - 1 : -1], tops[far - 1 : -1]
-    states = jnp.concatenate([stack[:, :rows], parts], axis=0)
-    states = jnp.sum(weight[:, :, None, None] * states[None], axis=1)
-    mine = traded(with_header(states, tops), NEAR)
+        before.append(lax.ppermute(whole, "far", [(i, i + back) for i in range(far - back)]))
+    whole_spec = pl.BlockSpec(memory_space=pltpu.VMEM)
+    states = pl.pallas_call(
+        before_body,
+        in_specs=[pl.BlockSpec(memory_space=pltpu.SMEM)] + [whole_spec] * far,
+        out_specs=whole_spec,
+        out_shape=jax.ShapeDtypeStruct(got.shape, jnp.float32),
+        compiler_params=pltpu.CompilerParams(vmem_limit_bytes=4 << 20),
+        name="states_before",
+    )(lax.axis_index("far").reshape(1), got, *before)
+    mine = traded(states, NEAR)
     return mine[:, :rows].reshape(heads, dk, dv), mine[::per_head, rows, 0]
 
 
@@ -328,15 +355,15 @@
     ).astype(jnp.bfloat16)
 
     weights = tuple(pltpu.with_memory_space_constraint(w[0], pltpu.HBM) for w in (expert_gate_matrix, expert_up_matrix, expert_down_matrix))
-    early = (slots + 1) // 2
+    early, lines = slots // 2, (slots + 1) // 2
     by_slot = outgoing.reshape(slots, experts, width)
-    got_a = traded(packed(by_slot[:early], early), SP)
-    got_b = traded(packed(by_slot[early:], early), SP)
+    got_a = traded(packed(by_slot[:early], lines), SP)
+    got_b = traded(packed(by_slot[early:], lines), SP)
     made_a, last = through_experts(unpacked(got_a, early, width), weights)
     got_b, _ = lax.optimization_barrier((got_b, last))
-    back_a = traded(packed(made_a, early), SP)
+    back_a = traded(packed(made_a, lines), SP)
     made_b, _ = through_experts(unpacked(got_b, slots - early, width), weights)
-    back_b = traded(packed(made_b, early), SP)
+    back_b = traded(packed(made_b, lines), SP)
 
     out = residual
     cut = early * experts

time: 325 us -> 308 us (0.948)
  waiting for transfers between devices: 144 us -> 124 us
  blocking collectives: 0 us -> 15.5 us
  starting transfers between devices: 125 us -> 117 us
    ppermute x3, starting transfers between devices: 13 us -> 35.1 us  [states_before(): lax.ppermute(whole, 'far', [(i, i + back) for i in range(far - back)])]
    ppermute x21, starting transfers between devices: 52.9 us -> 32.4 us  [shifted(): return lax.ppermute(x, axis, [(i, (i + by) % size) for i in range(size)])]
    all_to_all x0 -> x1, blocking collectives: none -> 15.5 us  [traded(): return lax.all_to_all(x, axis, split_axis=0, concat_axis=0, tiled=True)]
    ppermute x21, waiting for transfers between devices: 64 us -> 48.5 us  [shifted(): return lax.ppermute(x, axis, [(i, (i + by) % size) for i in range(size)])]
    all_to_all x7 -> x6, starting transfers between devices: 59.5 us -> 50 us  [traded(): return lax.all_to_all(x, axis, split_axis=0, concat_axis=0, tiled=True)]
    all_to_all x7 -> x6, waiting for transfers between devices: 78.3 us -> 74.2 us  [traded(): return lax.all_to_all(x, axis, split_axis=0, concat_axis=0, tiled=True)]
  transfers between devices with their start and end apart: 31 -> 30, of which waited for: 15 -> 13; matrix products, arithmetic and copies ran while one was open for 4% -> 3% of each run, Pallas kernels for 8% -> 9%
where the time goes in v4:
time: 308 us; the launch traced here: 306 us
  waiting for transfers between devices  124 us (40%)
  starting transfers between devices  117 us (38%)
  Pallas kernels  27.7 us (9%)
  blocking collectives  15.5 us (5%)
  local copies, waits for them, and re-layouts  7.75 us (3%)
  matrix products  6.76 us (2%)
  other arithmetic  6.36 us (2%)
    all_to_all x6, waiting for transfers between devices, traded(): return lax.all_to_all(x, axis, split_axis=0, concat_axis=0, tiled=True)  74.2 us
    all_to_all x6, starting transfers between devices, traded(): return lax.all_to_all(x, axis, split_axis=0, concat_axis=0, tiled=True)  50 us
    ppermute x21, waiting for transfers between devices, shifted(): return lax.ppermute(x, axis, [(i, (i + by) % size) for i in range(size)])  48.5 us
    ppermute x3, starting transfers between devices, states_before(): lax.ppermute(whole, 'far', [(i, i + back) for i in range(far - back)])  35.1 us
    ppermute x21, starting transfers between devices, shifted(): return lax.ppermute(x, axis, [(i, (i + by) % size) for i in range(size)])  32.4 us
    pallas_call x4, Pallas kernels, expert_parts(): pl.pallas_call(expert_body, in_specs=[whole, whole, stored, stored, store...  26.9 us
    all_to_all x1, blocking collectives, traded(): return lax.all_to_all(x, axis, split_axis=0, concat_axis=0, tiled=True)  15.5 us
  transfers between devices with their start and end apart: 30, of which 13 were waited for; matrix products, arithmetic and copies ran while one was open for 3% of the time, Pallas kernels for 9%

profile of v4, /device:TPU:40, one launch (start us, length us, event | category | flops | bytes accessed | tf_op | source)
XLA Modules:
  0.0 306.3 jit_solution(5738463394868519765)
XLA Ops:
  0.0 1.0 copy.50
  1.1 0.8 fusion.36
  2.2 0.9 fusion.68
  3.0 0.8 exponential_bitcast_fusion
  4.2 0.5 fusion.19
  4.9 15.5 %all_to_all.35.parts_ref = f32[8,40,128]{2,1,0:T(8,128)S(1)} all-to-all(f32[8,40,128]{2,1,0:T(8,128)S(1)} %maximum_maximum_fusion), channel_id=1, replica_groups=mesh['grp'=2,'far'=4,'near'=4,'core'=2,'tp'=4] {'near','core'}, dimensions={0} | all-to-all | bytes 327680 | tf_op jit(solution)/shard_map/all_to_all | solution.py:28
  20.5 20.4 %collective-permute-start = (f32[40,128]{1,0:T(8,128)S(1)}, f32[40,128]{1,0:T(8,128)S(1)}, u32[]{:S(2)}, u32[]{:S(2)}) collective-permute-start(f32[40,128]{1,0:T(8,128)S(1)} %group_state.1), channel_id=1, source_target_pairs={{0,96},{1,97},{2,98},{3,99},{4,100},{5,101},{6,102},{7,103},{8,104... | collective-permute-start | bytes 61448 | tf_op jit(solution)/shard_map/ppermute | solution.py:94
  41.0 4.7 %collective-permute-start.4 = (bf16[64,512]{1,0:T(8,128)(2,1)}, bf16[64,512]{1,0:T(8,128)(2,1)S(1)}, u32[]{:S(2)}, u32[]{:S(2)}) collective-permute-start(bf16[64,512]{1,0:T(8,128)(2,1)} %bitcast.220), channel_id=1, source_target_pairs={{0,64},{32,96},{64,0},{96,32},{1,65},{33,97},{65,1},{97,33},{2,66}... | collective-permute-start | bytes 196616 | tf_op jit(solution)/shard_map/ppermute | solution.py:24
  45.7 1.2 collective-permute-start.3
  46.9 12.7 %collective-permute-start.1 = (f32[40,128]{1,0:T(8,128)S(1)}, f32[40,128]{1,0:T(8,128)S(1)}, u32[]{:S(2)}, u32[]{:S(2)}) collective-permute-start(f32[40,128]{1,0:T(8,128)S(1)} %group_state.1), channel_id=1, source_target_pairs={{0,64},{32,96},{1,65},{33,97},{2,66},{34,98},{3,67},{35,99},{4,68}... | collective-permute-start | bytes 61448 | tf_op jit(solution)/shard_map/ppermute | solution.py:94
  59.6 2.1 collective-permute-start.2
  61.7 1.4 collective-permute-done.2.refs_2_
  63.1 0.7 states_before.1
  63.8 3.6 %all-to-all-start.1 = ((f32[8,40,128]{2,1,0:T(8,128)}), f32[8,40,128]{2,1,0:T(8,128)S(1)}, u32[]{:S(2)}, u32[]{:S(2)}) async-start(f32[8,40,128]{2,1,0:T(8,128)} %states_before.1), calls=%async_computation.1 | async-start | bytes 327680 | tf_op jit(solution)/shard_map/all_to_all | solution.py:28
  67.5 5.3 %collective-permute-start.8 = (bf16[4,64,512]{2,1,0:T(8,128)(2,1)S(1)}, bf16[4,64,512]{2,1,0:T(8,128)(2,1)S(1)}, u32[]{:S(2)}, u32[]{:S(2)}) collective-permute-start(bf16[4,64,512]{2,1,0:T(8,128)(2,1)S(1)} %get-tuple-element.56), channel_id=1, source_target_pairs={{0,112},{8,120},{16,0},{24,8},{32,16},{40,24},{48,32},{56,40},{64,... | collective-permute-start | bytes 786440 | tf_op jit(solution)/shard_map/ppermute | solution.py:24
  72.9 0.6 collective-permute-start.7
  73.4 1.5 collective-permute-start.6
  74.9 0.4 fusion.17
  75.5 11.2 %collective-permute-done.8 = bf16[4,64,512]{2,1,0:T(8,128)(2,1)S(1)} collective-permute-done((bf16[4,64,512]{2,1,0:T(8,128)(2,1)S(1)}, bf16[4,64,512]{2,1,0:T(8,128)(2,1)S(1)}, u32[]{:S(2)}, u32[]{:S(2)}) %collective-permute-start.8) | collective-permute-done | bytes 262176 | tf_op jit(solution)/shard_map/ppermute | solution.py:24
  86.6 5.2 %collective-permute-done.7 = bf16[4,64,512]{2,1,0:T(8,128)(2,1)S(1)} collective-permute-done((bf16[4,64,512]{2,1,0:T(8,128)(2,1)S(1)}, bf16[4,64,512]{2,1,0:T(8,128)(2,1)S(1)}, u32[]{:S(2)}, u32[]{:S(2)}) %collective-permute-start.7) | collective-permute-done | bytes 262176 | tf_op jit(solution)/shard_map/ppermute | solution.py:24
  92.4 0.6 fusion.9
  93.0 0.6 multiply_reduce_fusion.1
  93.6 1.1 collective-permute-done.9
  95.4 0.8 fusion.5
  96.1 1.8 convolution_convert_fusion
  97.9 4.7 %all-to-all-start.2 = ((bf16[4,56,2048]{2,1,0:T(8,128)(2,1)}), bf16[4,56,2048]{2,1,0:T(8,128)(2,1)S(1)}, u32[]{:S(2)}, u32[]{:S(2)}) async-start(bf16[4,56,2048]{2,1,0:T(8,128)(2,1)} %bitcast.29), calls=%async_computation.2 | async-start | bytes 1835008 | tf_op jit(solution)/shard_map/all_to_all | solution.py:28
  103.1 13.5 %all-to-all-done.2 = bf16[4,56,2048]{2,1,0:T(8,128)(2,1)S(1)} async-done(((bf16[4,56,2048]{2,1,0:T(8,128)(2,1)}), bf16[4,56,2048]{2,1,0:T(8,128)(2,1)S(1)}, u32[]{:S(2)}, u32[]{:S(2)}) %all-to-all-start.2) | async-done | bytes 917536 | tf_op jit(solution)/shard_map/all_to_all | solution.py:28
  117.0 0.5 convolution_convert_fusion.1
  117.6 1.0 copy.58
  118.7 10.7 %all-to-all-start.3 = ((bf16[32,4,1536]{2,1,0:T(4,128)(2,1)}), bf16[32,4,1536]{2,1,0:T(4,128)(2,1)S(1)}, u32[]{:S(2)}, u32[]{:S(2)}) async-start(bf16[32,4,1536]{2,1,0:T(4,128)(2,1)} %copy.58), calls=%async_computation.3 | async-start | bytes 786432 | tf_op jit(solution)/shard_map/all_to_all | solution.py:28
  129.4 1.2 copy.85
  130.6 26.3 %all-to-all-done.3 = bf16[32,4,1536]{2,1,0:T(4,128)(2,1)S(1)} async-done(((bf16[32,4,1536]{2,1,0:T(4,128)(2,1)}), bf16[32,4,1536]{2,1,0:T(4,128)(2,1)S(1)}, u32[]{:S(2)}, u32[]{:S(2)}) %all-to-all-start.3) | async-done | bytes 393248 | tf_op jit(solution)/shard_map/all_to_all | solution.py:28
  156.9 4.8 %all-to-all-start.5 = ((bf16[32,4,2048]{2,1,0:T(4,128)(2,1)}), bf16[32,4,2048]{2,1,0:T(4,128)(2,1)S(1)}, u32[]{:S(2)}, u32[]{:S(2)}) async-start(bf16[32,4,2048]{2,1,0:T(4,128)(2,1)} %bitcast.173), calls=%async_computation.5 | async-start | bytes 1048576 | tf_op jit(solution)/shard_map/all_to_all | solution.py:28
  162.0 1.3 collective-permute-start.12
  163.2 0.9 collective-permute-start.10
  164.1 8.5 %collective-permute-done.12.two_ref = bf16[96,2048]{1,0:T(8,128)(2,1)S(1)} collective-permute-done((bf16[96,2048]{1,0:T(8,128)(2,1)S(1)}, bf16[96,2048]{1,0:T(8,128)(2,1)S(1)}, u32[]{:S(2)}, u32[]{:S(2)}) %collective-permute-start.12) | collective-permute-done | bytes 393248 | tf_op jit(solution)/shard_map/ppermute | solution.py:24
  172.6 2.5 collective-permute-start.13
  175.3 6.4 %expert_parts.4 = (bf16[96,2048]{1,0:T(8,128)(2,1)S(1)}, bf16[96,2048]{1,0:T(8,128)(2,1)S(1)}) custom-call(bf16[96,2048]{1,0:T(8,128)(2,1)S(1)} %collective-permute-done.10.one_ref, bf16[96,2048]{1,0:T(8,128)(2,1)S(1)} %collective-permute-done.12.two_ref, bf16[2048,896]{1,0:T(8,128)(2,1)} %bitcast.182, bf16[2048,896]{1,0:T(8,128)(2,1)} %bitcast.186, ...), custom_call_target="tpu_custom_call" | custom-call | flops 2113929216 | bytes 12582912 | tf_op jit(solution)/shard_map/expert_parts/pallas_call | solution.py:187
  181.9 3.2 %collective-permute-start.14 = (bf16[96,2048]{1,0:T(8,128)(2,1)S(1)}, bf16[96,2048]{1,0:T(8,128)(2,1)}, u32[]{:S(2)}, u32[]{:S(2)}) collective-permute-start(bf16[96,2048]{1,0:T(8,128)(2,1)S(1)} %get-tuple-element.28), channel_id=1, source_target_pairs={{0,3},{1,0},{2,1},{3,2},{4,7},{5,4},{6,5},{7,6},{8,11},{9,8},{10,9... | collective-permute-start | bytes 1179656 | tf_op jit(solution)/shard_map/ppermute | solution.py:24
  185.1 6.4 %expert_parts.5 = (bf16[96,2048]{1,0:T(8,128)(2,1)S(1)}, bf16[96,2048]{1,0:T(8,128)(2,1)S(1)}) custom-call(bf16[96,2048]{1,0:T(8,128)(2,1)S(1)} %pad_maximum_fusion.4.one_ref, bf16[96,2048]{1,0:T(8,128)(2,1)S(1)} %bitcast.181, bf16[2048,896]{1,0:T(8,128)(2,1)} %bitcast.183, bf16[2048,896]{1,0:T(8,128)(2,1)} %bitcast.187, bf16[896,2048]{1,0:T(8,128)(2,1)} %bitcast.191), custom_call_target="tpu_custom_call" | custom-call | flops 2113929216 | bytes 12582912 | tf_op jit(solution)/shard_map/expert_parts/pallas_call | solution.py:187
  191.5 1.5 collective-permute-start.16
  193.0 1.9 all-to-all-done.5
  194.9 0.3 copy.63
  195.2 1.3 collective-permute-start.19
  196.5 0.9 collective-permute-start.17
  197.3 7.9 %collective-permute-done.16 = bf16[96,2048]{1,0:T(8,128)(2,1)} collective-permute-done((bf16[96,2048]{1,0:T(8,128)(2,1)S(1)}, bf16[96,2048]{1,0:T(8,128)(2,1)}, u32[]{:S(2)}, u32[]{:S(2)}) %collective-permute-start.16) | collective-permute-done | bytes 393248 | tf_op jit(solution)/shard_map/ppermute | solution.py:24
  205.3 1.5 add_convert_fusion.1
  206.8 1.0 copy.60
  207.9 13.3 %all-to-all-start.4 = ((bf16[32,4,1536]{2,1,0:T(4,128)(2,1)}), bf16[32,4,1536]{2,1,0:T(4,128)(2,1)S(1)}, u32[]{:S(2)}, u32[]{:S(2)}) async-start(bf16[32,4,1536]{2,1,0:T(4,128)(2,1)} %copy.60), calls=%async_computation.4 | async-start | bytes 786432 | tf_op jit(solution)/shard_map/all_to_all | solution.py:28
  221.2 2.0 collective-permute-start.20
  223.2 0.3 collective-permute-start.18
  223.5 7.1 %expert_parts.6 = (bf16[128,2048]{1,0:T(8,128)(2,1)S(1)}, bf16[128,2048]{1,0:T(8,128)(2,1)S(1)}) custom-call(bf16[128,2048]{1,0:T(8,128)(2,1)S(1)} %collective-permute-done.17.one_ref, bf16[128,2048]{1,0:T(8,128)(2,1)S(1)} %collective-permute-done.19.two_ref, bf16[2048,896]{1,0:T(8,128)(2,1)} %bitcast.184, bf16[2048,896]{1,0:T(8,128)(2,1)} %bitcast.188, ...), custom_call_target="tpu_custom_call" | custom-call | flops 2818572288 | bytes 13107200 | tf_op jit(solution)/shard_map/expert_parts/pallas_call | solution.py:187
  230.6 0.5 collective-permute-start.22
  231.1 2.8 collective-permute-start.21
  234.0 7.1 %expert_parts.7 = (bf16[128,2048]{1,0:T(8,128)(2,1)S(1)}, bf16[128,2048]{1,0:T(8,128)(2,1)S(1)}) custom-call(bf16[128,2048]{1,0:T(8,128)(2,1)S(1)} %pad_maximum_fusion.2.one_ref, bf16[128,2048]{1,0:T(8,128)(2,1)S(1)} %bitcast.178, bf16[2048,896]{1,0:T(8,128)(2,1)} %bitcast.185, bf16[2048,896]{1,0:T(8,128)(2,1)} %bitcast.189, bf16[896,2048]{1,0:T(8,128)(2,1)} %bitcast.193), custom_call_target="tpu_custom_call" | custom-call | flops 2818572288 | bytes 13107200 | tf_op jit(solution)/shard_map/expert_parts/pallas_call | solution.py:187
  241.1 1.4 collective-permute-start.23
  242.7 3.0 collective-permute-done.22
  245.7 9.8 %collective-permute-done.21 = bf16[128,2048]{1,0:T(8,128)(2,1)S(1)} collective-permute-done((bf16[128,2048]{1,0:T(8,128)(2,1)S(1)}, bf16[128,2048]{1,0:T(8,128)(2,1)S(1)}, u32[]{:S(2)}, u32[]{:S(2)}) %collective-permute-start.21) | collective-permute-done | bytes 524320 | tf_op jit(solution)/shard_map/ppermute | solution.py:24
  255.5 1.8 collective-permute-done.23
  257.3 0.3 add_convert_fusion
  257.6 1.2 copy.84
  258.8 12.9 %all-to-all-start.6 = ((bf16[32,4,2048]{2,1,0:T(4,128)(2,1)}), bf16[32,4,2048]{2,1,0:T(4,128)(2,1)S(1)}, u32[]{:S(2)}, u32[]{:S(2)}) async-start(bf16[32,4,2048]{2,1,0:T(4,128)(2,1)} %bitcast.172), calls=%async_computation.6 | async-start | bytes 1048576 | tf_op jit(solution)/shard_map/all_to_all | solution.py:28
  272.4 32.4 %all-to-all-done.6 = bf16[32,4,2048]{2,1,0:T(4,128)(2,1)S(1)} async-done(((bf16[32,4,2048]{2,1,0:T(4,128)(2,1)}), bf16[32,4,2048]{2,1,0:T(4,128)(2,1)S(1)}, u32[]{:S(2)}, u32[]{:S(2)}) %all-to-all-start.6) | async-done | bytes 524320 | tf_op jit(solution)/shard_map/all_to_all | solution.py:28
  305.4 1.0 fusion.4
  (114 shorter events, 5.5 us)
Async XLA Ops:
  0.0 4.2 %copy-start = (bf16[224,512]{1,0:T(8,128)(2,1)S(1)}, bf16[224,512]{1,0:T(8,128)(2,1)}, u32[]{:S(2)}) copy-start(bf16[224,512]{1,0:T(8,128)(2,1)} %param.17) | copy-start | bytes 688132
  0.0 74.9 %copy-start.7 = (f32[4,224]{1,0:T(4,128)S(1)}, f32[4,224]{1,0:T(4,128)}, u32[]{:S(2)}) copy-start(f32[4,224]{1,0:T(4,128)} %param.18) | copy-start | bytes 10756
  0.0 67.5 %copy-start.6 = (bf16[512,64]{0,1:T(8,128)(2,1)S(1)}, bf16[512,64]{0,1:T(8,128)(2,1)}, u32[]{:S(2)}) copy-start(bf16[512,64]{0,1:T(8,128)(2,1)} %param.22) | copy-start | bytes 196612
  0.0 75.3 %copy-start.8 = (bf16[2048]{0:T(1024)(128)(2,1)S(1)}, bf16[2048]{0:T(1024)(128)(2,1)}, u32[]{:S(2)}) copy-start(bf16[2048]{0:T(1024)(128)(2,1)} %param.24) | copy-start | bytes 12292
  0.0 75.3 %copy-start.5 = (bf16[224,256]{1,0:T(8,128)(2,1)S(1)}, bf16[224,256]{1,0:T(8,128)(2,1)}, u32[]{:S(2)}) copy-start(bf16[224,256]{1,0:T(8,128)(2,1)} %param.15) | copy-start | bytes 344068
  0.0 75.4 %copy-start.10 = (bf16[512]{0:T(512)(128)(2,1)S(1)}, bf16[512]{0:T(512)(128)(2,1)}, u32[]{:S(2)}) copy-start(bf16[512]{0:T(512)(128)(2,1)} %param.21) | copy-start | bytes 3076
  20.5 39.1 %collective-permute-start = (f32[40,128]{1,0:T(8,128)S(1)}, f32[40,128]{1,0:T(8,128)S(1)}, u32[]{:S(2)}, u32[]{:S(2)}) collective-permute-start(f32[40,128]{1,0:T(8,128)S(1)} %group_state.1), channel_id=1, source_target_pairs={{0,96},{1,97},{2,98},{3,99},{4,100},{5,101},{6,102},{7,103},{8,104... | collective-permute-start | bytes 61448 | tf_op jit(solution)/shard_map/ppermute | solution.py:94
  40.8 26.6 %collective-permute-start.5 = (bf16[64,512]{1,0:T(8,128)(2,1)}, bf16[64,512]{1,0:T(8,128)(2,1)S(1)}, u32[]{:S(2)}, u32[]{:S(2)}) collective-permute-start(bf16[64,512]{1,0:T(8,128)(2,1)} %bitcast.219), channel_id=1, source_target_pairs={{0,32},{32,64},{64,96},{96,0},{1,33},{33,65},{65,97},{97,1},{2,34}... | collective-permute-start | bytes 196616 | tf_op jit(solution)/shard_map/ppermute | solution.py:24
  41.0 26.5 %collective-permute-start.4 = (bf16[64,512]{1,0:T(8,128)(2,1)}, bf16[64,512]{1,0:T(8,128)(2,1)S(1)}, u32[]{:S(2)}, u32[]{:S(2)}) collective-permute-start(bf16[64,512]{1,0:T(8,128)(2,1)} %bitcast.220), channel_id=1, source_target_pairs={{0,64},{32,96},{64,0},{96,32},{1,65},{33,97},{65,1},{97,33},{2,66}... | collective-permute-start | bytes 196616 | tf_op jit(solution)/shard_map/ppermute | solution.py:24
  45.7 21.8 %collective-permute-start.3 = (bf16[64,512]{1,0:T(8,128)(2,1)}, bf16[64,512]{1,0:T(8,128)(2,1)S(1)}, u32[]{:S(2)}, u32[]{:S(2)}) collective-permute-start(bf16[64,512]{1,0:T(8,128)(2,1)} %bitcast.221), channel_id=1, source_target_pairs={{0,96},{32,0},{64,32},{96,64},{1,97},{33,1},{65,33},{97,65},{2,98}... | collective-permute-start | bytes 196616 | tf_op jit(solution)/shard_map/ppermute | solution.py:24
  46.9 14.8 %collective-permute-start.1 = (f32[40,128]{1,0:T(8,128)S(1)}, f32[40,128]{1,0:T(8,128)S(1)}, u32[]{:S(2)}, u32[]{:S(2)}) collective-permute-start(f32[40,128]{1,0:T(8,128)S(1)} %group_state.1), channel_id=1, source_target_pairs={{0,64},{32,96},{1,65},{33,97},{2,66},{34,98},{3,67},{35,99},{4,68}... | collective-permute-start | bytes 61448 | tf_op jit(solution)/shard_map/ppermute | solution.py:94
  59.6 3.6 %collective-permute-start.2 = (f32[40,128]{1,0:T(8,128)S(1)}, f32[40,128]{1,0:T(8,128)S(1)}, u32[]{:S(2)}, u32[]{:S(2)}) collective-permute-start(f32[40,128]{1,0:T(8,128)S(1)} %group_state.1), channel_id=1, source_target_pairs={{0,32},{32,64},{64,96},{1,33},{33,65},{65,97},{2,34},{34,66},{66,9... | collective-permute-start | bytes 61448 | tf_op jit(solution)/shard_map/ppermute | solution.py:94
  63.8 28.2 %all-to-all-start.1 = ((f32[8,40,128]{2,1,0:T(8,128)}), f32[8,40,128]{2,1,0:T(8,128)S(1)}, u32[]{:S(2)}, u32[]{:S(2)}) async-start(f32[8,40,128]{2,1,0:T(8,128)} %states_before.1), calls=%async_computation.1 | async-start | bytes 327680 | tf_op jit(solution)/shard_map/all_to_all | solution.py:28
  67.5 19.1 %collective-permute-start.8 = (bf16[4,64,512]{2,1,0:T(8,128)(2,1)S(1)}, bf16[4,64,512]{2,1,0:T(8,128)(2,1)S(1)}, u32[]{:S(2)}, u32[]{:S(2)}) collective-permute-start(bf16[4,64,512]{2,1,0:T(8,128)(2,1)S(1)} %get-tuple-element.56), channel_id=1, source_target_pairs={{0,112},{8,120},{16,0},{24,8},{32,16},{40,24},{48,32},{56,40},{64,... | collective-permute-start | bytes 786440 | tf_op jit(solution)/shard_map/ppermute | solution.py:24
  72.9 18.9 %collective-permute-start.7 = (bf16[4,64,512]{2,1,0:T(8,128)(2,1)S(1)}, bf16[4,64,512]{2,1,0:T(8,128)(2,1)S(1)}, u32[]{:S(2)}, u32[]{:S(2)}) collective-permute-start(bf16[4,64,512]{2,1,0:T(8,128)(2,1)S(1)} %get-tuple-element.56), channel_id=1, source_target_pairs={{0,120},{8,0},{16,8},{24,16},{32,24},{40,32},{48,40},{56,48},{64,5... | collective-permute-start | bytes 786440 | tf_op jit(solution)/shard_map/ppermute | solution.py:24
  73.4 18.4 %collective-permute-start.6 = (bf16[4,64,512]{2,1,0:T(8,128)(2,1)S(1)}, bf16[4,64,512]{2,1,0:T(8,128)(2,1)S(1)}, u32[]{:S(2)}, u32[]{:S(2)}) collective-permute-start(bf16[4,64,512]{2,1,0:T(8,128)(2,1)S(1)} %get-tuple-element.56), channel_id=1, source_target_pairs={{0,8},{8,16},{16,24},{24,32},{32,40},{40,48},{48,56},{56,64},{64,7... | collective-permute-start | bytes 786440 | tf_op jit(solution)/shard_map/ppermute | solution.py:24
  91.9 2.8 collective-permute-start.9
  96.1 6.5 %copy-start.9 = (s32[56,2]{0,1:T(2,128)S(1)}, s32[56,2]{0,1:T(2,128)}, u32[]{:S(2)}) copy-start(s32[56,2]{0,1:T(2,128)} %param.25) | copy-start | bytes 1348
  97.9 18.9 %copy-start.3 = (bf16[56,2048]{1,0:T(8,128)(2,1)S(1)}, bf16[56,2048]{1,0:T(8,128)(2,1)}, u32[]{:S(2)}) copy-start(bf16[56,2048]{1,0:T(8,128)(2,1)} %param.23) | copy-start | bytes 688132
  97.9 18.7 %all-to-all-start.2 = ((bf16[4,56,2048]{2,1,0:T(8,128)(2,1)}), bf16[4,56,2048]{2,1,0:T(8,128)(2,1)S(1)}, u32[]{:S(2)}, u32[]{:S(2)}) async-start(bf16[4,56,2048]{2,1,0:T(8,128)(2,1)} %bitcast.29), calls=%async_computation.2 | async-start | bytes 1835008 | tf_op jit(solution)/shard_map/all_to_all | solution.py:28
  116.8 0.8 copy-start.1
  118.7 38.3 %all-to-all-start.3 = ((bf16[32,4,1536]{2,1,0:T(4,128)(2,1)}), bf16[32,4,1536]{2,1,0:T(4,128)(2,1)S(1)}, u32[]{:S(2)}, u32[]{:S(2)}) async-start(bf16[32,4,1536]{2,1,0:T(4,128)(2,1)} %copy.58), calls=%async_computation.3 | async-start | bytes 786432 | tf_op jit(solution)/shard_map/all_to_all | solution.py:28
  156.9 38.0 %all-to-all-start.5 = ((bf16[32,4,2048]{2,1,0:T(4,128)(2,1)}), bf16[32,4,2048]{2,1,0:T(4,128)(2,1)S(1)}, u32[]{:S(2)}, u32[]{:S(2)}) async-start(bf16[32,4,2048]{2,1,0:T(4,128)(2,1)} %bitcast.173), calls=%async_computation.5 | async-start | bytes 1048576 | tf_op jit(solution)/shard_map/all_to_all | solution.py:28
  162.0 10.6 %collective-permute-start.12 = (bf16[96,2048]{1,0:T(8,128)(2,1)S(1)}, bf16[96,2048]{1,0:T(8,128)(2,1)S(1)}, u32[]{:S(2)}, u32[]{:S(2)}) collective-permute-start(bf16[96,2048]{1,0:T(8,128)(2,1)S(1)} %bitcast.179), channel_id=1, source_target_pairs={{0,3},{1,0},{2,1},{3,2},{4,7},{5,4},{6,5},{7,6},{8,11},{9,8},{10,9... | collective-permute-start | bytes 1179656 | tf_op jit(solution)/shard_map/ppermute | solution.py:24
  163.2 11.8 %collective-permute-start.10 = (bf16[96,2048]{1,0:T(8,128)(2,1)S(1)}, bf16[96,2048]{1,0:T(8,128)(2,1)S(1)}, u32[]{:S(2)}, u32[]{:S(2)}) collective-permute-start(bf16[96,2048]{1,0:T(8,128)(2,1)S(1)} %bitcast.180), channel_id=1, source_target_pairs={{0,1},{1,2},{2,3},{3,0},{4,5},{5,6},{6,7},{7,4},{8,9},{9,10},{10,1... | collective-permute-start | bytes 1179656 | tf_op jit(solution)/shard_map/ppermute | solution.py:24
  172.6 12.5 %collective-permute-start.13 = (bf16[48,2048]{1,0:T(8,128)(2,1)S(1)}, bf16[48,2048]{1,0:T(8,128)(2,1)S(1)}, u32[]{:S(2)}, u32[]{:S(2)}) collective-permute-start(bf16[48,2048]{1,0:T(8,128)(2,1)S(1)} %slice.184), channel_id=1, source_target_pairs={{0,3},{1,0},{2,1},{3,2},{4,7},{5,4},{6,5},{7,6},{8,11},{9,8},{10,9... | collective-permute-start | bytes 589832 | tf_op jit(solution)/shard_map/ppermute | solution.py:24
  175.1 10.0 %collective-permute-start.11 = (bf16[48,2048]{1,0:T(8,128)(2,1)S(1)}, bf16[48,2048]{1,0:T(8,128)(2,1)S(1)}, u32[]{:S(2)}, u32[]{:S(2)}) collective-permute-start(bf16[48,2048]{1,0:T(8,128)(2,1)S(1)} %slice.183), channel_id=1, source_target_pairs={{0,1},{1,2},{2,3},{3,0},{4,5},{5,6},{6,7},{7,4},{8,9},{9,10},{10,1... | collective-permute-start | bytes 589832 | tf_op jit(solution)/shard_map/ppermute | solution.py:24
  181.6 15.7 %collective-permute-start.15 = (bf16[96,2048]{1,0:T(8,128)(2,1)S(1)}, bf16[96,2048]{1,0:T(8,128)(2,1)}, u32[]{:S(2)}, u32[]{:S(2)}) collective-permute-start(bf16[96,2048]{1,0:T(8,128)(2,1)S(1)} %get-tuple-element.24), channel_id=1, source_target_pairs={{0,1},{1,2},{2,3},{3,0},{4,5},{5,6},{6,7},{7,4},{8,9},{9,10},{10,1... | collective-permute-start | bytes 1179656 | tf_op jit(solution)/shard_map/ppermute | solution.py:24
  181.9 15.4 %collective-permute-start.14 = (bf16[96,2048]{1,0:T(8,128)(2,1)S(1)}, bf16[96,2048]{1,0:T(8,128)(2,1)}, u32[]{:S(2)}, u32[]{:S(2)}) collective-permute-start(bf16[96,2048]{1,0:T(8,128)(2,1)S(1)} %get-tuple-element.28), channel_id=1, source_target_pairs={{0,3},{1,0},{2,1},{3,2},{4,7},{5,4},{6,5},{7,6},{8,11},{9,8},{10,9... | collective-permute-start | bytes 1179656 | tf_op jit(solution)/shard_map/ppermute | solution.py:24
  191.5 13.7 %collective-permute-start.16 = (bf16[96,2048]{1,0:T(8,128)(2,1)S(1)}, bf16[96,2048]{1,0:T(8,128)(2,1)}, u32[]{:S(2)}, u32[]{:S(2)}) collective-permute-start(bf16[96,2048]{1,0:T(8,128)(2,1)S(1)} %get-tuple-element.29), channel_id=1, source_target_pairs={{0,2},{1,3},{2,0},{3,1},{4,6},{5,7},{6,4},{7,5},{8,10},{9,11},{10,... | collective-permute-start | bytes 1179656 | tf_op jit(solution)/shard_map/ppermute | solution.py:24
  195.2 26.0 %collective-permute-start.19 = (bf16[128,2048]{1,0:T(8,128)(2,1)S(1)}, bf16[128,2048]{1,0:T(8,128)(2,1)S(1)}, u32[]{:S(2)}, u32[]{:S(2)}) collective-permute-start(bf16[128,2048]{1,0:T(8,128)(2,1)S(1)} %bitcast.176), channel_id=1, source_target_pairs={{0,3},{1,0},{2,1},{3,2},{4,7},{5,4},{6,5},{7,6},{8,11},{9,8},{10,9... | collective-permute-start | bytes 1572872 | tf_op jit(solution)/shard_map/ppermute | solution.py:24
  196.5 26.7 %collective-permute-start.17 = (bf16[128,2048]{1,0:T(8,128)(2,1)S(1)}, bf16[128,2048]{1,0:T(8,128)(2,1)S(1)}, u32[]{:S(2)}, u32[]{:S(2)}) collective-permute-start(bf16[128,2048]{1,0:T(8,128)(2,1)S(1)} %bitcast.177), channel_id=1, source_target_pairs={{0,1},{1,2},{2,3},{3,0},{4,5},{5,6},{6,7},{7,4},{8,9},{9,10},{10,1... | collective-permute-start | bytes 1572872 | tf_op jit(solution)/shard_map/ppermute | solution.py:24
  207.9 50.9 %all-to-all-start.4 = ((bf16[32,4,1536]{2,1,0:T(4,128)(2,1)}), bf16[32,4,1536]{2,1,0:T(4,128)(2,1)S(1)}, u32[]{:S(2)}, u32[]{:S(2)}) async-start(bf16[32,4,1536]{2,1,0:T(4,128)(2,1)} %copy.60), calls=%async_computation.4 | async-start | bytes 786432 | tf_op jit(solution)/shard_map/all_to_all | solution.py:28
  221.2 12.7 %collective-permute-start.20 = (bf16[64,2048]{1,0:T(8,128)(2,1)S(1)}, bf16[64,2048]{1,0:T(8,128)(2,1)S(1)}, u32[]{:S(2)}, u32[]{:S(2)}) collective-permute-start(bf16[64,2048]{1,0:T(8,128)(2,1)S(1)} %slice.200), channel_id=1, source_target_pairs={{0,3},{1,0},{2,1},{3,2},{4,7},{5,4},{6,5},{7,6},{8,11},{9,8},{10,9... | collective-permute-start | bytes 786440 | tf_op jit(solution)/shard_map/ppermute | solution.py:24
  223.2 10.7 %collective-permute-start.18 = (bf16[64,2048]{1,0:T(8,128)(2,1)S(1)}, bf16[64,2048]{1,0:T(8,128)(2,1)S(1)}, u32[]{:S(2)}, u32[]{:S(2)}) collective-permute-start(bf16[64,2048]{1,0:T(8,128)(2,1)S(1)} %slice.199), channel_id=1, source_target_pairs={{0,1},{1,2},{2,3},{3,0},{4,5},{5,6},{6,7},{7,4},{8,9},{9,10},{10,1... | collective-permute-start | bytes 786440 | tf_op jit(solution)/shard_map/ppermute | solution.py:24
  230.6 15.1 %collective-permute-start.22 = (bf16[128,2048]{1,0:T(8,128)(2,1)S(1)}, bf16[128,2048]{1,0:T(8,128)(2,1)S(1)}, u32[]{:S(2)}, u32[]{:S(2)}) collective-permute-start(bf16[128,2048]{1,0:T(8,128)(2,1)S(1)} %get-tuple-element.33), channel_id=1, source_target_pairs={{0,1},{1,2},{2,3},{3,0},{4,5},{5,6},{6,7},{7,4},{8,9},{9,10},{10,1... | collective-permute-start | bytes 1572872 | tf_op jit(solution)/shard_map/ppermute | solution.py:24
  231.1 24.4 %collective-permute-start.21 = (bf16[128,2048]{1,0:T(8,128)(2,1)S(1)}, bf16[128,2048]{1,0:T(8,128)(2,1)S(1)}, u32[]{:S(2)}, u32[]{:S(2)}) collective-permute-start(bf16[128,2048]{1,0:T(8,128)(2,1)S(1)} %get-tuple-element.37), channel_id=1, source_target_pairs={{0,3},{1,0},{2,1},{3,2},{4,7},{5,4},{6,5},{7,6},{8,11},{9,8},{10,9... | collective-permute-start | bytes 1572872 | tf_op jit(solution)/shard_map/ppermute | solution.py:24
  234.0 8.5 %copy-start.11 = (f32[56,2]{0,1:T(2,128)S(1)}, f32[56,2]{0,1:T(2,128)}, u32[]{:S(2)}) copy-start(f32[56,2]{0,1:T(2,128)} %param.26) | copy-start | bytes 1348
  241.1 16.2 %collective-permute-start.23 = (bf16[128,2048]{1,0:T(8,128)(2,1)S(1)}, bf16[128,2048]{1,0:T(8,128)(2,1)S(1)}, u32[]{:S(2)}, u32[]{:S(2)}) collective-permute-start(bf16[128,2048]{1,0:T(8,128)(2,1)S(1)} %get-tuple-element.38), channel_id=1, source_target_pairs={{0,2},{1,3},{2,0},{3,1},{4,6},{5,7},{6,4},{7,5},{8,10},{9,11},{10,... | collective-permute-start | bytes 1572872 | tf_op jit(solution)/shard_map/ppermute | solution.py:24
  258.8 13.1 %copy-start.2 = (f32[56,2048]{1,0:T(8,128)S(1)}, f32[56,2048]{1,0:T(8,128)}, u32[]{:S(2)}) copy-start(f32[56,2048]{1,0:T(8,128)} %copy-done.1) | copy-start | bytes 1376260
  258.8 13.1 %copy-start.4 = (bf16[56,2048]{1,0:T(8,128)(2,1)S(1)}, bf16[56,2048]{1,0:T(8,128)(2,1)}, u32[]{:S(2)}) copy-start(bf16[56,2048]{1,0:T(8,128)(2,1)} %param.23) | copy-start | bytes 688132
  258.8 46.0 %all-to-all-start.6 = ((bf16[32,4,2048]{2,1,0:T(4,128)(2,1)}), bf16[32,4,2048]{2,1,0:T(4,128)(2,1)S(1)}, u32[]{:S(2)}, u32[]{:S(2)}) async-start(bf16[32,4,2048]{2,1,0:T(4,128)(2,1)} %bitcast.172), calls=%async_computation.6 | async-start | bytes 1048576 | tf_op jit(solution)/shard_map/all_to_all | solution.py:28

commit v5 on v4

--- a/solution.py
+++ b/solution.py
@@ -129,14 +129,14 @@
 
 
 UNIT = 128
-WIDE = 256
-
-
-def expert_body(
-    one_ref, two_ref, gate_hbm, up_hbm, down_hbm, one_out, two_out,
-    gate_ref, up_ref, down_ref, hidden_ref, gate_sem, up_sem, down_sem,
-):
-    units, columns, count = gate_ref.shape[0], down_ref.shape[0], one_ref.shape[0]
+WIDE = 512
+
+
+def expert_body(pieces, *refs):
+    ins, (gate_hbm, up_hbm, down_hbm), refs = refs[:pieces], refs[pieces : pieces + 3], refs[pieces + 3 :]
+    outs, refs = refs[:pieces], refs[pieces:]
+    gate_ref, up_ref, down_ref, hidden_ref, gate_sem, up_sem, down_sem = refs
+    units, columns, count = gate_ref.shape[0], down_ref.shape[0], ins[0].shape[0]
 
     def block(k, size):
         return pl.ds(pl.multiple_of(k * size, size), size)
@@ -158,7 +158,7 @@
         gate_copy(k).wait()
         up_copy(k).wait()
         both = jnp.concatenate([gate_ref[k], up_ref[k]], axis=1)
-        rows = jnp.concatenate([one_ref[...], two_ref[...]], axis=0)
+        rows = jnp.concatenate([ref[...] for ref in ins], axis=0)
         made = jnp.dot(rows, both, preferred_element_type=jnp.float32)
         gate, upward = made[:, :UNIT], made[:, UNIT:]
         hidden = gate / (1.0 + jnp.exp(-gate)) * upward
@@ -168,8 +168,8 @@
         down_copy(k).wait()
         made = jnp.dot(hidden_ref[...], down_ref[k], preferred_element_type=jnp.float32)
         made = made.astype(jnp.bfloat16)
-        one_out[:, block(k, WIDE)] = made[:count]
-        two_out[:, block(k, WIDE)] = made[count:]
+        for n, out_ref in enumerate(outs):
+            out_ref[:, block(k, WIDE)] = made[n * count : (n + 1) * count]
 
     lax.fori_loop(0, units, ask, None)
     lax.fori_loop(0, columns, lambda k, _: down_copy(k).start(), None)
@@ -177,35 +177,35 @@
     lax.fori_loop(0, columns, show, None)
 
 
-def expert_parts(one, two, gate_w, up_w, down_w):
-    count, width = one.shape
+def expert_parts(pieces, gate_w, up_w, down_w):
+    count, width = pieces[0].shape
     inner = gate_w.shape[1]
     units, columns = inner // UNIT, width // WIDE
     whole = pl.BlockSpec(memory_space=pltpu.VMEM)
     stored = pl.BlockSpec(memory_space=pltpu.HBM)
     rows = jax.ShapeDtypeStruct((count, width), jnp.bfloat16)
     return pl.pallas_call(
-        expert_body,
-        in_specs=[whole, whole, stored, stored, stored],
-        out_specs=[whole, whole],
-        out_shape=[rows, rows],
+        lambda *refs: expert_body(len(pieces), *refs),
+        in_specs=[whole] * len(pieces) + [stored] * 3,
+        out_specs=[whole] * len(pieces),
+        out_shape=[rows] * len(pieces),
         scratch_shapes=[
             pltpu.VMEM((units, width, UNIT), jnp.bfloat16),
             pltpu.VMEM((units, width, UNIT), jnp.bfloat16),
             pltpu.VMEM((columns, inner, WIDE), jnp.bfloat16),
-            pltpu.VMEM((2 * count, inner), jnp.bfloat16),
+            pltpu.VMEM((len(pieces) * count, inner), jnp.bfloat16),
             pltpu.SemaphoreType.DMA((units,)),
             pltpu.SemaphoreType.DMA((units,)),
             pltpu.SemaphoreType.DMA((columns,)),
         ],
         compiler_params=pltpu.CompilerParams(vmem_limit_bytes=32 << 20),
         cost_estimate=pl.CostEstimate(
-            flops=12 * count * width * inner,
-            bytes_accessed=6 * width * inner + 8 * count * width,
-            transcendentals=2 * count * inner,
+            flops=6 * len(pieces) * count * width * inner,
+            bytes_accessed=6 * width * inner + 4 * len(pieces) * count * width,
+            transcendentals=len(pieces) * count * inner,
         ),
         name="expert_parts",
-    )(one, two, gate_w, up_w, down_w)
+    )(*pieces, gate_w, up_w, down_w)
 
 
 def packed(by_slot, lines):
@@ -243,11 +243,13 @@
     right = shifted(rows, "tp", size - 1)
     across = [shifted(left[:half], "tp", 1), shifted(right[half:], "tp", size - 1)]
     left, right = lax.optimization_barrier((left, right))
-    from_left, from_right = expert_parts(left, right, *weights)
+    from_left, from_right = expert_parts((left, right), *weights)
     parts = [shifted(from_left, "tp", size - 1), shifted(from_right, "tp", 1)]
-    across, rows, _ = lax.optimization_barrier((jnp.concatenate(across, axis=0), rows, from_right))
-    from_across, own = expert_parts(across, rows, *weights)
-    parts = [own, *parts, shifted(from_across, "tp", 2)]
+    across, _ = lax.optimization_barrier((jnp.concatenate(across, axis=0), from_right))
+    (from_across,) = expert_parts((across,), *weights)
+    parts.append(shifted(from_across, "tp", 2))
+    rows, _ = lax.optimization_barrier((rows, from_across))
+    parts.extend(expert_parts((rows,), *weights))
     made = sum(part.astype(jnp.float32) for part in parts).astype(jnp.bfloat16)
     return made.reshape(by_slot.shape), from_across
 

time: 308 us -> 306 us (level)
  waiting for transfers between devices: 124 us -> 116 us
  Pallas kernels: 27.7 us -> 32.8 us
    ppermute x21, waiting for transfers between devices: 48.5 us -> 38.7 us  [shifted(): return lax.ppermute(x, axis, [(i, (i + by) % size) for i in range(size)])]
    pallas_call x4 -> x6, Pallas kernels: 26.9 us -> 32 us  [expert_parts(): pl.pallas_call(lambda *refs: expert_body(len(pieces), *refs), in_specs=[w...]
  transfers between devices with their start and end apart: 30 -> 30, of which waited for: 13 -> 13; matrix products, arithmetic and copies ran while one was open for 3% -> 3% of each run, Pallas kernels for 9% -> 11%
where the time goes in v5:
time: 306 us; the launch traced here: 304 us
  starting transfers between devices  118 us (39%)
  waiting for transfers between devices  116 us (38%)
  Pallas kernels  32.8 us (11%)
  blocking collectives  15.5 us (5%)
  local copies, waits for them, and re-layouts  7.76 us (3%)
  matrix products  6.76 us (2%)
  other arithmetic  6.36 us (2%)
    all_to_all x6, waiting for transfers between devices, traded(): return lax.all_to_all(x, axis, split_axis=0, concat_axis=0, tiled=True)  76.2 us
    all_to_all x6, starting transfers between devices, traded(): return lax.all_to_all(x, axis, split_axis=0, concat_axis=0, tiled=True)  50 us
    ppermute x21, waiting for transfers between devices, shifted(): return lax.ppermute(x, axis, [(i, (i + by) % size) for i in range(size)])  38.7 us
    ppermute x3, starting transfers between devices, states_before(): lax.ppermute(whole, 'far', [(i, i + back) for i in range(far - back)])  35.1 us
    ppermute x21, starting transfers between devices, shifted(): return lax.ppermute(x, axis, [(i, (i + by) % size) for i in range(size)])  32.6 us
    pallas_call x6, Pallas kernels, expert_parts(): pl.pallas_call(lambda *refs: expert_body(len(pieces), *refs), in_specs=[w...  32 us
    all_to_all x1, blocking collectives, traded(): return lax.all_to_all(x, axis, split_axis=0, concat_axis=0, tiled=True)  15.5 us
  transfers between devices with their start and end apart: 30, of which 13 were waited for; matrix products, arithmetic and copies ran while one was open for 3% of the time, Pallas kernels for 11%

profile of v5, /device:TPU:40, one launch (start us, length us, event | category | flops | bytes accessed | tf_op | source)
XLA Modules:
  0.0 303.9 jit_solution(257792636563062990)
XLA Ops:
  0.0 1.0 copy.50
  1.1 0.8 fusion.36
  2.2 0.9 fusion.68
  3.0 0.8 exponential_bitcast_fusion
  4.2 0.5 fusion.19
  4.9 15.5 %all_to_all.35.parts_ref = f32[8,40,128]{2,1,0:T(8,128)S(1)} all-to-all(f32[8,40,128]{2,1,0:T(8,128)S(1)} %maximum_maximum_fusion), channel_id=1, replica_groups=mesh['grp'=2,'far'=4,'near'=4,'core'=2,'tp'=4] {'near','core'}, dimensions={0} | all-to-all | bytes 327680 | tf_op jit(solution)/shard_map/all_to_all | solution.py:28
  20.5 20.4 %collective-permute-start = (f32[40,128]{1,0:T(8,128)S(1)}, f32[40,128]{1,0:T(8,128)S(1)}, u32[]{:S(2)}, u32[]{:S(2)}) collective-permute-start(f32[40,128]{1,0:T(8,128)S(1)} %group_state.1), channel_id=1, source_target_pairs={{0,96},{1,97},{2,98},{3,99},{4,100},{5,101},{6,102},{7,103},{8,104... | collective-permute-start | bytes 61448 | tf_op jit(solution)/shard_map/ppermute | solution.py:94
  41.0 4.7 %collective-permute-start.4 = (bf16[64,512]{1,0:T(8,128)(2,1)}, bf16[64,512]{1,0:T(8,128)(2,1)S(1)}, u32[]{:S(2)}, u32[]{:S(2)}) collective-permute-start(bf16[64,512]{1,0:T(8,128)(2,1)} %bitcast.226), channel_id=1, source_target_pairs={{0,64},{32,96},{64,0},{96,32},{1,65},{33,97},{65,1},{97,33},{2,66}... | collective-permute-start | bytes 196616 | tf_op jit(solution)/shard_map/ppermute | solution.py:24
  45.7 1.2 collective-permute-start.3
  46.9 12.7 %collective-permute-start.1 = (f32[40,128]{1,0:T(8,128)S(1)}, f32[40,128]{1,0:T(8,128)S(1)}, u32[]{:S(2)}, u32[]{:S(2)}) collective-permute-start(f32[40,128]{1,0:T(8,128)S(1)} %group_state.1), channel_id=1, source_target_pairs={{0,64},{32,96},{1,65},{33,97},{2,66},{34,98},{3,67},{35,99},{4,68}... | collective-permute-start | bytes 61448 | tf_op jit(solution)/shard_map/ppermute | solution.py:94
  59.6 2.1 collective-permute-start.2
  61.7 1.4 collective-permute-done.2.refs_2_
  63.1 0.7 states_before.1
  63.8 3.6 %all-to-all-start.1 = ((f32[8,40,128]{2,1,0:T(8,128)}), f32[8,40,128]{2,1,0:T(8,128)S(1)}, u32[]{:S(2)}, u32[]{:S(2)}) async-start(f32[8,40,128]{2,1,0:T(8,128)} %states_before.1), calls=%async_computation.1 | async-start | bytes 327680 | tf_op jit(solution)/shard_map/all_to_all | solution.py:28
  67.5 5.3 %collective-permute-start.8 = (bf16[4,64,512]{2,1,0:T(8,128)(2,1)S(1)}, bf16[4,64,512]{2,1,0:T(8,128)(2,1)S(1)}, u32[]{:S(2)}, u32[]{:S(2)}) collective-permute-start(bf16[4,64,512]{2,1,0:T(8,128)(2,1)S(1)} %get-tuple-element.48), channel_id=1, source_target_pairs={{0,112},{8,120},{16,0},{24,8},{32,16},{40,24},{48,32},{56,40},{64,... | collective-permute-start | bytes 786440 | tf_op jit(solution)/shard_map/ppermute | solution.py:24
  72.9 0.6 collective-permute-start.7
  73.4 1.5 collective-permute-start.6
  74.9 0.4 fusion.17
  75.5 11.2 %collective-permute-done.8 = bf16[4,64,512]{2,1,0:T(8,128)(2,1)S(1)} collective-permute-done((bf16[4,64,512]{2,1,0:T(8,128)(2,1)S(1)}, bf16[4,64,512]{2,1,0:T(8,128)(2,1)S(1)}, u32[]{:S(2)}, u32[]{:S(2)}) %collective-permute-start.8) | collective-permute-done | bytes 262176 | tf_op jit(solution)/shard_map/ppermute | solution.py:24
  86.6 5.2 %collective-permute-done.7 = bf16[4,64,512]{2,1,0:T(8,128)(2,1)S(1)} collective-permute-done((bf16[4,64,512]{2,1,0:T(8,128)(2,1)S(1)}, bf16[4,64,512]{2,1,0:T(8,128)(2,1)S(1)}, u32[]{:S(2)}, u32[]{:S(2)}) %collective-permute-start.7) | collective-permute-done | bytes 262176 | tf_op jit(solution)/shard_map/ppermute | solution.py:24
  92.4 0.6 fusion.9
  93.0 0.6 multiply_reduce_fusion.1
  93.6 1.1 collective-permute-done.9
  95.4 0.8 fusion.5
  96.1 1.8 convolution_convert_fusion
  97.9 4.7 %all-to-all-start.2 = ((bf16[4,56,2048]{2,1,0:T(8,128)(2,1)}), bf16[4,56,2048]{2,1,0:T(8,128)(2,1)S(1)}, u32[]{:S(2)}, u32[]{:S(2)}) async-start(bf16[4,56,2048]{2,1,0:T(8,128)(2,1)} %bitcast.29), calls=%async_computation.2 | async-start | bytes 1835008 | tf_op jit(solution)/shard_map/all_to_all | solution.py:28
  103.1 13.5 %all-to-all-done.2 = bf16[4,56,2048]{2,1,0:T(8,128)(2,1)S(1)} async-done(((bf16[4,56,2048]{2,1,0:T(8,128)(2,1)}), bf16[4,56,2048]{2,1,0:T(8,128)(2,1)S(1)}, u32[]{:S(2)}, u32[]{:S(2)}) %all-to-all-start.2) | async-done | bytes 917536 | tf_op jit(solution)/shard_map/all_to_all | solution.py:28
  116.9 0.5 convolution_convert_fusion.1
  117.6 1.0 copy.58
  118.7 10.7 %all-to-all-start.3 = ((bf16[32,4,1536]{2,1,0:T(4,128)(2,1)}), bf16[32,4,1536]{2,1,0:T(4,128)(2,1)S(1)}, u32[]{:S(2)}, u32[]{:S(2)}) async-start(bf16[32,4,1536]{2,1,0:T(4,128)(2,1)} %copy.58), calls=%async_computation.3 | async-start | bytes 786432 | tf_op jit(solution)/shard_map/all_to_all | solution.py:28
  129.4 1.2 copy.85
  130.6 26.3 %all-to-all-done.3 = bf16[32,4,1536]{2,1,0:T(4,128)(2,1)S(1)} async-done(((bf16[32,4,1536]{2,1,0:T(4,128)(2,1)}), bf16[32,4,1536]{2,1,0:T(4,128)(2,1)S(1)}, u32[]{:S(2)}, u32[]{:S(2)}) %all-to-all-start.3) | async-done | bytes 393248 | tf_op jit(solution)/shard_map/all_to_all | solution.py:28
  156.9 4.8 %all-to-all-start.5 = ((bf16[32,4,2048]{2,1,0:T(4,128)(2,1)}), bf16[32,4,2048]{2,1,0:T(4,128)(2,1)S(1)}, u32[]{:S(2)}, u32[]{:S(2)}) async-start(bf16[32,4,2048]{2,1,0:T(4,128)(2,1)} %bitcast.173), calls=%async_computation.5 | async-start | bytes 1048576 | tf_op jit(solution)/shard_map/all_to_all | solution.py:28
  162.0 1.3 collective-permute-start.11
  163.2 0.9 collective-permute-start.10
  164.1 8.5 %collective-permute-done.11.refs_1_ = bf16[96,2048]{1,0:T(8,128)(2,1)S(1)} collective-permute-done((bf16[96,2048]{1,0:T(8,128)(2,1)S(1)}, bf16[96,2048]{1,0:T(8,128)(2,1)S(1)}, u32[]{:S(2)}, u32[]{:S(2)}) %collective-permute-start.11) | collective-permute-done | bytes 393248 | tf_op jit(solution)/shard_map/ppermute | solution.py:24
  172.6 2.5 collective-permute-start.15
  175.2 5.7 %expert_parts.6 = (bf16[96,2048]{1,0:T(8,128)(2,1)S(1)}, bf16[96,2048]{1,0:T(8,128)(2,1)S(1)}) custom-call(bf16[96,2048]{1,0:T(8,128)(2,1)S(1)} %collective-permute-done.10.refs_0_, bf16[96,2048]{1,0:T(8,128)(2,1)S(1)} %collective-permute-done.11.refs_1_, bf16[2048,896]{1,0:T(8,128)(2,1)} %bitcast.182, bf16[2048,896]{1,0:T(8,128)(2,1)} %bitcast.188, ...), custom_call_target="tpu_custom_call" | custom-call | flops 2113929216 | bytes 12582912 | tf_op jit(solution)/shard_map/expert_parts/pallas_call | solution.py:187
  181.2 3.2 %collective-permute-start.12 = (bf16[96,2048]{1,0:T(8,128)(2,1)S(1)}, bf16[96,2048]{1,0:T(8,128)(2,1)}, u32[]{:S(2)}, u32[]{:S(2)}) collective-permute-start(bf16[96,2048]{1,0:T(8,128)(2,1)S(1)} %get-tuple-element.20), channel_id=1, source_target_pairs={{0,3},{1,0},{2,1},{3,2},{4,7},{5,4},{6,5},{7,6},{8,11},{9,8},{10,9... | collective-permute-start | bytes 1179656 | tf_op jit(solution)/shard_map/ppermute | solution.py:24
  184.4 5.0 %expert_parts.7 = bf16[96,2048]{1,0:T(8,128)(2,1)S(1)} custom-call(bf16[96,2048]{1,0:T(8,128)(2,1)S(1)} %pad_maximum_fusion.4.refs_0_, bf16[2048,896]{1,0:T(8,128)(2,1)} %bitcast.183, bf16[2048,896]{1,0:T(8,128)(2,1)} %bitcast.189, bf16[896,2048]{1,0:T(8,128)(2,1)} %bitcast.195), custom_call_target="tpu_custom_call" | custom-call | flops 1056964608 | bytes 11796480 | tf_op jit(solution)/shard_map/expert_parts/pallas_call | solution.py:187
  189.4 1.4 collective-permute-start.16
  190.9 3.9 %all-to-all-done.5 = bf16[32,4,2048]{2,1,0:T(4,128)(2,1)S(1)} async-done(((bf16[32,4,2048]{2,1,0:T(4,128)(2,1)}), bf16[32,4,2048]{2,1,0:T(4,128)(2,1)S(1)}, u32[]{:S(2)}, u32[]{:S(2)}) %all-to-all-start.5) | async-done | bytes 524320 | tf_op jit(solution)/shard_map/all_to_all | solution.py:28
  195.2 1.3 collective-permute-start.18
  196.5 0.9 collective-permute-start.17
  197.3 4.9 %expert_parts.8 = bf16[96,2048]{1,0:T(8,128)(2,1)S(1)} custom-call(bf16[96,2048]{1,0:T(8,128)(2,1)S(1)} %bitcast.181, bf16[2048,896]{1,0:T(8,128)(2,1)} %bitcast.184, bf16[2048,896]{1,0:T(8,128)(2,1)} %bitcast.190, bf16[896,2048]{1,0:T(8,128)(2,1)} %bitcast.196), custom_call_target="tpu_custom_call" | custom-call | flops 1056964608 | bytes 11796480 | tf_op jit(solution)/shard_map/expert_parts/pallas_call | solution.py:187
  202.3 0.8 collective-permute-done.16
  203.1 1.5 add_convert_fusion.1
  204.7 1.0 copy.60
  205.8 13.3 %all-to-all-start.4 = ((bf16[32,4,1536]{2,1,0:T(4,128)(2,1)}), bf16[32,4,1536]{2,1,0:T(4,128)(2,1)S(1)}, u32[]{:S(2)}, u32[]{:S(2)}) async-start(bf16[32,4,1536]{2,1,0:T(4,128)(2,1)} %copy.60), calls=%async_computation.4 | async-start | bytes 786432 | tf_op jit(solution)/shard_map/all_to_all | solution.py:28
  219.1 2.2 collective-permute-start.22
  221.3 0.4 collective-permute-start.21
  221.7 6.4 %expert_parts.9 = (bf16[128,2048]{1,0:T(8,128)(2,1)S(1)}, bf16[128,2048]{1,0:T(8,128)(2,1)S(1)}) custom-call(bf16[128,2048]{1,0:T(8,128)(2,1)S(1)} %collective-permute-done.17.refs_0_, bf16[128,2048]{1,0:T(8,128)(2,1)S(1)} %collective-permute-done.18.refs_1_, bf16[2048,896]{1,0:T(8,128)(2,1)} %bitcast.185, bf16[2048,896]{1,0:T(8,128)(2,1)} %bitcast.191, ...), custom_call_target="tpu_custom_call" | custom-call | flops 2818572288 | bytes 13107200 | tf_op jit(solution)/shard_map/expert_parts/pallas_call | solution.py:187
  228.0 2.1 collective-permute-start.20
  230.1 1.2 collective-permute-start.19
  231.4 5.0 %expert_parts.10 = bf16[128,2048]{1,0:T(8,128)(2,1)S(1)} custom-call(bf16[128,2048]{1,0:T(8,128)(2,1)S(1)} %pad_maximum_fusion.2.refs_0_, bf16[2048,896]{1,0:T(8,128)(2,1)} %bitcast.186, bf16[2048,896]{1,0:T(8,128)(2,1)} %bitcast.192, bf16[896,2048]{1,0:T(8,128)(2,1)} %bitcast.198), custom_call_target="tpu_custom_call" | custom-call | flops 1409286144 | bytes 12058624 | tf_op jit(solution)/shard_map/expert_parts/pallas_call | solution.py:187
  236.5 1.3 collective-permute-start.23
  237.9 5.0 %expert_parts.11 = bf16[128,2048]{1,0:T(8,128)(2,1)S(1)} custom-call(bf16[128,2048]{1,0:T(8,128)(2,1)S(1)} %bitcast.178, bf16[2048,896]{1,0:T(8,128)(2,1)} %bitcast.187, bf16[2048,896]{1,0:T(8,128)(2,1)} %bitcast.193, bf16[896,2048]{1,0:T(8,128)(2,1)} %bitcast.199), custom_call_target="tpu_custom_call" | custom-call | flops 1409286144 | bytes 12058624 | tf_op jit(solution)/shard_map/expert_parts/pallas_call | solution.py:187
  242.9 0.6 collective-permute-done.20
  243.5 1.4 collective-permute-done.19
  244.9 9.9 %collective-permute-done.23 = bf16[128,2048]{1,0:T(8,128)(2,1)S(1)} collective-permute-done((bf16[128,2048]{1,0:T(8,128)(2,1)S(1)}, bf16[128,2048]{1,0:T(8,128)(2,1)S(1)}, u32[]{:S(2)}, u32[]{:S(2)}) %collective-permute-start.23) | collective-permute-done | bytes 524320 | tf_op jit(solution)/shard_map/ppermute | solution.py:24
  255.2 1.2 copy.84
  256.4 12.9 %all-to-all-start.6 = ((bf16[32,4,2048]{2,1,0:T(4,128)(2,1)}), bf16[32,4,2048]{2,1,0:T(4,128)(2,1)S(1)}, u32[]{:S(2)}, u32[]{:S(2)}) async-start(bf16[32,4,2048]{2,1,0:T(4,128)(2,1)} %bitcast.172), calls=%async_computation.6 | async-start | bytes 1048576 | tf_op jit(solution)/shard_map/all_to_all | solution.py:28
  269.9 32.4 %all-to-all-done.6 = bf16[32,4,2048]{2,1,0:T(4,128)(2,1)S(1)} async-done(((bf16[32,4,2048]{2,1,0:T(4,128)(2,1)}), bf16[32,4,2048]{2,1,0:T(4,128)(2,1)S(1)}, u32[]{:S(2)}, u32[]{:S(2)}) %all-to-all-start.6) | async-done | bytes 524320 | tf_op jit(solution)/shard_map/all_to_all | solution.py:28
  302.9 1.0 fusion.4
  (116 shorter events, 6.1 us)
Async XLA Ops:
  0.0 4.2 %copy-start = (bf16[224,512]{1,0:T(8,128)(2,1)S(1)}, bf16[224,512]{1,0:T(8,128)(2,1)}, u32[]{:S(2)}) copy-start(bf16[224,512]{1,0:T(8,128)(2,1)} %param.17) | copy-start | bytes 688132
  0.0 74.9 %copy-start.7 = (f32[4,224]{1,0:T(4,128)S(1)}, f32[4,224]{1,0:T(4,128)}, u32[]{:S(2)}) copy-start(f32[4,224]{1,0:T(4,128)} %param.18) | copy-start | bytes 10756
  0.0 67.5 %copy-start.6 = (bf16[512,64]{0,1:T(8,128)(2,1)S(1)}, bf16[512,64]{0,1:T(8,128)(2,1)}, u32[]{:S(2)}) copy-start(bf16[512,64]{0,1:T(8,128)(2,1)} %param.22) | copy-start | bytes 196612
  0.0 75.3 %copy-start.8 = (bf16[2048]{0:T(1024)(128)(2,1)S(1)}, bf16[2048]{0:T(1024)(128)(2,1)}, u32[]{:S(2)}) copy-start(bf16[2048]{0:T(1024)(128)(2,1)} %param.24) | copy-start | bytes 12292
  0.0 75.3 %copy-start.5 = (bf16[224,256]{1,0:T(8,128)(2,1)S(1)}, bf16[224,256]{1,0:T(8,128)(2,1)}, u32[]{:S(2)}) copy-start(bf16[224,256]{1,0:T(8,128)(2,1)} %param.15) | copy-start | bytes 344068
  0.0 75.4 %copy-start.10 = (bf16[512]{0:T(512)(128)(2,1)S(1)}, bf16[512]{0:T(512)(128)(2,1)}, u32[]{:S(2)}) copy-start(bf16[512]{0:T(512)(128)(2,1)} %param.21) | copy-start | bytes 3076
  20.5 39.1 %collective-permute-start = (f32[40,128]{1,0:T(8,128)S(1)}, f32[40,128]{1,0:T(8,128)S(1)}, u32[]{:S(2)}, u32[]{:S(2)}) collective-permute-start(f32[40,128]{1,0:T(8,128)S(1)} %group_state.1), channel_id=1, source_target_pairs={{0,96},{1,97},{2,98},{3,99},{4,100},{5,101},{6,102},{7,103},{8,104... | collective-permute-start | bytes 61448 | tf_op jit(solution)/shard_map/ppermute | solution.py:94
  40.8 26.6 %collective-permute-start.5 = (bf16[64,512]{1,0:T(8,128)(2,1)}, bf16[64,512]{1,0:T(8,128)(2,1)S(1)}, u32[]{:S(2)}, u32[]{:S(2)}) collective-permute-start(bf16[64,512]{1,0:T(8,128)(2,1)} %bitcast.225), channel_id=1, source_target_pairs={{0,32},{32,64},{64,96},{96,0},{1,33},{33,65},{65,97},{97,1},{2,34}... | collective-permute-start | bytes 196616 | tf_op jit(solution)/shard_map/ppermute | solution.py:24
  41.0 26.5 %collective-permute-start.4 = (bf16[64,512]{1,0:T(8,128)(2,1)}, bf16[64,512]{1,0:T(8,128)(2,1)S(1)}, u32[]{:S(2)}, u32[]{:S(2)}) collective-permute-start(bf16[64,512]{1,0:T(8,128)(2,1)} %bitcast.226), channel_id=1, source_target_pairs={{0,64},{32,96},{64,0},{96,32},{1,65},{33,97},{65,1},{97,33},{2,66}... | collective-permute-start | bytes 196616 | tf_op jit(solution)/shard_map/ppermute | solution.py:24
  45.7 21.8 %collective-permute-start.3 = (bf16[64,512]{1,0:T(8,128)(2,1)}, bf16[64,512]{1,0:T(8,128)(2,1)S(1)}, u32[]{:S(2)}, u32[]{:S(2)}) collective-permute-start(bf16[64,512]{1,0:T(8,128)(2,1)} %bitcast.227), channel_id=1, source_target_pairs={{0,96},{32,0},{64,32},{96,64},{1,97},{33,1},{65,33},{97,65},{2,98}... | collective-permute-start | bytes 196616 | tf_op jit(solution)/shard_map/ppermute | solution.py:24
  46.9 14.8 %collective-permute-start.1 = (f32[40,128]{1,0:T(8,128)S(1)}, f32[40,128]{1,0:T(8,128)S(1)}, u32[]{:S(2)}, u32[]{:S(2)}) collective-permute-start(f32[40,128]{1,0:T(8,128)S(1)} %group_state.1), channel_id=1, source_target_pairs={{0,64},{32,96},{1,65},{33,97},{2,66},{34,98},{3,67},{35,99},{4,68}... | collective-permute-start | bytes 61448 | tf_op jit(solution)/shard_map/ppermute | solution.py:94
  59.6 3.6 %collective-permute-start.2 = (f32[40,128]{1,0:T(8,128)S(1)}, f32[40,128]{1,0:T(8,128)S(1)}, u32[]{:S(2)}, u32[]{:S(2)}) collective-permute-start(f32[40,128]{1,0:T(8,128)S(1)} %group_state.1), channel_id=1, source_target_pairs={{0,32},{32,64},{64,96},{1,33},{33,65},{65,97},{2,34},{34,66},{66,9... | collective-permute-start | bytes 61448 | tf_op jit(solution)/shard_map/ppermute | solution.py:94
  63.8 28.2 %all-to-all-start.1 = ((f32[8,40,128]{2,1,0:T(8,128)}), f32[8,40,128]{2,1,0:T(8,128)S(1)}, u32[]{:S(2)}, u32[]{:S(2)}) async-start(f32[8,40,128]{2,1,0:T(8,128)} %states_before.1), calls=%async_computation.1 | async-start | bytes 327680 | tf_op jit(solution)/shard_map/all_to_all | solution.py:28
  67.5 19.1 %collective-permute-start.8 = (bf16[4,64,512]{2,1,0:T(8,128)(2,1)S(1)}, bf16[4,64,512]{2,1,0:T(8,128)(2,1)S(1)}, u32[]{:S(2)}, u32[]{:S(2)}) collective-permute-start(bf16[4,64,512]{2,1,0:T(8,128)(2,1)S(1)} %get-tuple-element.48), channel_id=1, source_target_pairs={{0,112},{8,120},{16,0},{24,8},{32,16},{40,24},{48,32},{56,40},{64,... | collective-permute-start | bytes 786440 | tf_op jit(solution)/shard_map/ppermute | solution.py:24
  72.9 18.9 %collective-permute-start.7 = (bf16[4,64,512]{2,1,0:T(8,128)(2,1)S(1)}, bf16[4,64,512]{2,1,0:T(8,128)(2,1)S(1)}, u32[]{:S(2)}, u32[]{:S(2)}) collective-permute-start(bf16[4,64,512]{2,1,0:T(8,128)(2,1)S(1)} %get-tuple-element.48), channel_id=1, source_target_pairs={{0,120},{8,0},{16,8},{24,16},{32,24},{40,32},{48,40},{56,48},{64,5... | collective-permute-start | bytes 786440 | tf_op jit(solution)/shard_map/ppermute | solution.py:24
  73.4 18.4 %collective-permute-start.6 = (bf16[4,64,512]{2,1,0:T(8,128)(2,1)S(1)}, bf16[4,64,512]{2,1,0:T(8,128)(2,1)S(1)}, u32[]{:S(2)}, u32[]{:S(2)}) collective-permute-start(bf16[4,64,512]{2,1,0:T(8,128)(2,1)S(1)} %get-tuple-element.48), channel_id=1, source_target_pairs={{0,8},{8,16},{16,24},{24,32},{32,40},{40,48},{48,56},{56,64},{64,7... | collective-permute-start | bytes 786440 | tf_op jit(solution)/shard_map/ppermute | solution.py:24
  91.9 2.8 collective-permute-start.9
  96.1 6.5 %copy-start.9 = (s32[56,2]{0,1:T(2,128)S(1)}, s32[56,2]{0,1:T(2,128)}, u32[]{:S(2)}) copy-start(s32[56,2]{0,1:T(2,128)} %param.25) | copy-start | bytes 1348
  97.9 18.9 %copy-start.3 = (bf16[56,2048]{1,0:T(8,128)(2,1)S(1)}, bf16[56,2048]{1,0:T(8,128)(2,1)}, u32[]{:S(2)}) copy-start(bf16[56,2048]{1,0:T(8,128)(2,1)} %param.23) | copy-start | bytes 688132
  97.9 18.7 %all-to-all-start.2 = ((bf16[4,56,2048]{2,1,0:T(8,128)(2,1)}), bf16[4,56,2048]{2,1,0:T(8,128)(2,1)S(1)}, u32[]{:S(2)}, u32[]{:S(2)}) async-start(bf16[4,56,2048]{2,1,0:T(8,128)(2,1)} %bitcast.29), calls=%async_computation.2 | async-start | bytes 1835008 | tf_op jit(solution)/shard_map/all_to_all | solution.py:28
  116.8 0.8 copy-start.1
  118.7 38.3 %all-to-all-start.3 = ((bf16[32,4,1536]{2,1,0:T(4,128)(2,1)}), bf16[32,4,1536]{2,1,0:T(4,128)(2,1)S(1)}, u32[]{:S(2)}, u32[]{:S(2)}) async-start(bf16[32,4,1536]{2,1,0:T(4,128)(2,1)} %copy.58), calls=%async_computation.3 | async-start | bytes 786432 | tf_op jit(solution)/shard_map/all_to_all | solution.py:28
  156.9 38.0 %all-to-all-start.5 = ((bf16[32,4,2048]{2,1,0:T(4,128)(2,1)}), bf16[32,4,2048]{2,1,0:T(4,128)(2,1)S(1)}, u32[]{:S(2)}, u32[]{:S(2)}) async-start(bf16[32,4,2048]{2,1,0:T(4,128)(2,1)} %bitcast.173), calls=%async_computation.5 | async-start | bytes 1048576 | tf_op jit(solution)/shard_map/all_to_all | solution.py:28
  162.0 10.6 %collective-permute-start.11 = (bf16[96,2048]{1,0:T(8,128)(2,1)S(1)}, bf16[96,2048]{1,0:T(8,128)(2,1)S(1)}, u32[]{:S(2)}, u32[]{:S(2)}) collective-permute-start(bf16[96,2048]{1,0:T(8,128)(2,1)S(1)} %bitcast.179), channel_id=1, source_target_pairs={{0,3},{1,0},{2,1},{3,2},{4,7},{5,4},{6,5},{7,6},{8,11},{9,8},{10,9... | collective-permute-start | bytes 1179656 | tf_op jit(solution)/shard_map/ppermute | solution.py:24
  163.2 11.8 %collective-permute-start.10 = (bf16[96,2048]{1,0:T(8,128)(2,1)S(1)}, bf16[96,2048]{1,0:T(8,128)(2,1)S(1)}, u32[]{:S(2)}, u32[]{:S(2)}) collective-permute-start(bf16[96,2048]{1,0:T(8,128)(2,1)S(1)} %bitcast.180), channel_id=1, source_target_pairs={{0,1},{1,2},{2,3},{3,0},{4,5},{5,6},{6,7},{7,4},{8,9},{9,10},{10,1... | collective-permute-start | bytes 1179656 | tf_op jit(solution)/shard_map/ppermute | solution.py:24
  172.6 11.8 %collective-permute-start.15 = (bf16[48,2048]{1,0:T(8,128)(2,1)S(1)}, bf16[48,2048]{1,0:T(8,128)(2,1)S(1)}, u32[]{:S(2)}, u32[]{:S(2)}) collective-permute-start(bf16[48,2048]{1,0:T(8,128)(2,1)S(1)} %slice.184), channel_id=1, source_target_pairs={{0,3},{1,0},{2,1},{3,2},{4,7},{5,4},{6,5},{7,6},{8,11},{9,8},{10,9... | collective-permute-start | bytes 589832 | tf_op jit(solution)/shard_map/ppermute | solution.py:24
  175.1 9.3 %collective-permute-start.14 = (bf16[48,2048]{1,0:T(8,128)(2,1)S(1)}, bf16[48,2048]{1,0:T(8,128)(2,1)S(1)}, u32[]{:S(2)}, u32[]{:S(2)}) collective-permute-start(bf16[48,2048]{1,0:T(8,128)(2,1)S(1)} %slice.183), channel_id=1, source_target_pairs={{0,1},{1,2},{2,3},{3,0},{4,5},{5,6},{6,7},{7,4},{8,9},{9,10},{10,1... | collective-permute-start | bytes 589832 | tf_op jit(solution)/shard_map/ppermute | solution.py:24
  180.9 21.3 %collective-permute-start.13 = (bf16[96,2048]{1,0:T(8,128)(2,1)S(1)}, bf16[96,2048]{1,0:T(8,128)(2,1)}, u32[]{:S(2)}, u32[]{:S(2)}) collective-permute-start(bf16[96,2048]{1,0:T(8,128)(2,1)S(1)} %get-tuple-element.21), channel_id=1, source_target_pairs={{0,1},{1,2},{2,3},{3,0},{4,5},{5,6},{6,7},{7,4},{8,9},{9,10},{10,1... | collective-permute-start | bytes 1179656 | tf_op jit(solution)/shard_map/ppermute | solution.py:24
  181.2 21.0 %collective-permute-start.12 = (bf16[96,2048]{1,0:T(8,128)(2,1)S(1)}, bf16[96,2048]{1,0:T(8,128)(2,1)}, u32[]{:S(2)}, u32[]{:S(2)}) collective-permute-start(bf16[96,2048]{1,0:T(8,128)(2,1)S(1)} %get-tuple-element.20), channel_id=1, source_target_pairs={{0,3},{1,0},{2,1},{3,2},{4,7},{5,4},{6,5},{7,6},{8,11},{9,8},{10,9... | collective-permute-start | bytes 1179656 | tf_op jit(solution)/shard_map/ppermute | solution.py:24
  189.4 13.7 %collective-permute-start.16 = (bf16[96,2048]{1,0:T(8,128)(2,1)S(1)}, bf16[96,2048]{1,0:T(8,128)(2,1)}, u32[]{:S(2)}, u32[]{:S(2)}) collective-permute-start(bf16[96,2048]{1,0:T(8,128)(2,1)S(1)} %expert_parts.7), channel_id=1, source_target_pairs={{0,2},{1,3},{2,0},{3,1},{4,6},{5,7},{6,4},{7,5},{8,10},{9,11},{10,... | collective-permute-start | bytes 1179656 | tf_op jit(solution)/shard_map/ppermute | solution.py:24
  195.2 23.9 %collective-permute-start.18 = (bf16[128,2048]{1,0:T(8,128)(2,1)S(1)}, bf16[128,2048]{1,0:T(8,128)(2,1)S(1)}, u32[]{:S(2)}, u32[]{:S(2)}) collective-permute-start(bf16[128,2048]{1,0:T(8,128)(2,1)S(1)} %bitcast.176), channel_id=1, source_target_pairs={{0,3},{1,0},{2,1},{3,2},{4,7},{5,4},{6,5},{7,6},{8,11},{9,8},{10,9... | collective-permute-start | bytes 1572872 | tf_op jit(solution)/shard_map/ppermute | solution.py:24
  196.5 24.8 %collective-permute-start.17 = (bf16[128,2048]{1,0:T(8,128)(2,1)S(1)}, bf16[128,2048]{1,0:T(8,128)(2,1)S(1)}, u32[]{:S(2)}, u32[]{:S(2)}) collective-permute-start(bf16[128,2048]{1,0:T(8,128)(2,1)S(1)} %bitcast.177), channel_id=1, source_target_pairs={{0,1},{1,2},{2,3},{3,0},{4,5},{5,6},{6,7},{7,4},{8,9},{9,10},{10,1... | collective-permute-start | bytes 1572872 | tf_op jit(solution)/shard_map/ppermute | solution.py:24
  205.8 50.6 %all-to-all-start.4 = ((bf16[32,4,1536]{2,1,0:T(4,128)(2,1)}), bf16[32,4,1536]{2,1,0:T(4,128)(2,1)S(1)}, u32[]{:S(2)}, u32[]{:S(2)}) async-start(bf16[32,4,1536]{2,1,0:T(4,128)(2,1)} %copy.60), calls=%async_computation.4 | async-start | bytes 786432 | tf_op jit(solution)/shard_map/all_to_all | solution.py:28
  219.1 12.3 %collective-permute-start.22 = (bf16[64,2048]{1,0:T(8,128)(2,1)S(1)}, bf16[64,2048]{1,0:T(8,128)(2,1)S(1)}, u32[]{:S(2)}, u32[]{:S(2)}) collective-permute-start(bf16[64,2048]{1,0:T(8,128)(2,1)S(1)} %slice.200), channel_id=1, source_target_pairs={{0,3},{1,0},{2,1},{3,2},{4,7},{5,4},{6,5},{7,6},{8,11},{9,8},{10,9... | collective-permute-start | bytes 786440 | tf_op jit(solution)/shard_map/ppermute | solution.py:24
  221.3 10.1 %collective-permute-start.21 = (bf16[64,2048]{1,0:T(8,128)(2,1)S(1)}, bf16[64,2048]{1,0:T(8,128)(2,1)S(1)}, u32[]{:S(2)}, u32[]{:S(2)}) collective-permute-start(bf16[64,2048]{1,0:T(8,128)(2,1)S(1)} %slice.199), channel_id=1, source_target_pairs={{0,1},{1,2},{2,3},{3,0},{4,5},{5,6},{6,7},{7,4},{8,9},{9,10},{10,1... | collective-permute-start | bytes 786440 | tf_op jit(solution)/shard_map/ppermute | solution.py:24
  228.0 15.5 %collective-permute-start.20 = (bf16[128,2048]{1,0:T(8,128)(2,1)S(1)}, bf16[128,2048]{1,0:T(8,128)(2,1)S(1)}, u32[]{:S(2)}, u32[]{:S(2)}) collective-permute-start(bf16[128,2048]{1,0:T(8,128)(2,1)S(1)} %get-tuple-element.28), channel_id=1, source_target_pairs={{0,1},{1,2},{2,3},{3,0},{4,5},{5,6},{6,7},{7,4},{8,9},{9,10},{10,1... | collective-permute-start | bytes 1572872 | tf_op jit(solution)/shard_map/ppermute | solution.py:24
  230.1 14.8 %collective-permute-start.19 = (bf16[128,2048]{1,0:T(8,128)(2,1)S(1)}, bf16[128,2048]{1,0:T(8,128)(2,1)S(1)}, u32[]{:S(2)}, u32[]{:S(2)}) collective-permute-start(bf16[128,2048]{1,0:T(8,128)(2,1)S(1)} %get-tuple-element.27), channel_id=1, source_target_pairs={{0,3},{1,0},{2,1},{3,2},{4,7},{5,4},{6,5},{7,6},{8,11},{9,8},{10,9... | collective-permute-start | bytes 1572872 | tf_op jit(solution)/shard_map/ppermute | solution.py:24
  231.4 6.4 %copy-start.11 = (f32[56,2]{0,1:T(2,128)S(1)}, f32[56,2]{0,1:T(2,128)}, u32[]{:S(2)}) copy-start(f32[56,2]{0,1:T(2,128)} %param.26) | copy-start | bytes 1348
  236.5 18.3 %collective-permute-start.23 = (bf16[128,2048]{1,0:T(8,128)(2,1)S(1)}, bf16[128,2048]{1,0:T(8,128)(2,1)S(1)}, u32[]{:S(2)}, u32[]{:S(2)}) collective-permute-start(bf16[128,2048]{1,0:T(8,128)(2,1)S(1)} %expert_parts.10), channel_id=1, source_target_pairs={{0,2},{1,3},{2,0},{3,1},{4,6},{5,7},{6,4},{7,5},{8,10},{9,11},{10,... | collective-permute-start | bytes 1572872 | tf_op jit(solution)/shard_map/ppermute | solution.py:24
  256.4 13.1 %copy-start.2 = (f32[56,2048]{1,0:T(8,128)S(1)}, f32[56,2048]{1,0:T(8,128)}, u32[]{:S(2)}) copy-start(f32[56,2048]{1,0:T(8,128)} %copy-done.1) | copy-start | bytes 1376260
  256.4 13.1 %copy-start.4 = (bf16[56,2048]{1,0:T(8,128)(2,1)S(1)}, bf16[56,2048]{1,0:T(8,128)(2,1)}, u32[]{:S(2)}) copy-start(bf16[56,2048]{1,0:T(8,128)(2,1)} %param.23) | copy-start | bytes 688132
  256.4 46.0 %all-to-all-start.6 = ((bf16[32,4,2048]{2,1,0:T(4,128)(2,1)}), bf16[32,4,2048]{2,1,0:T(4,128)(2,1)S(1)}, u32[]{:S(2)}, u32[]{:S(2)}) async-start(bf16[32,4,2048]{2,1,0:T(4,128)(2,1)} %bitcast.172), calls=%async_computation.6 | async-start | bytes 1048576 | tf_op jit(solution)/shard_map/all_to_all | solution.py:28
